TPU v7x, 512 devices: a whole 4x4x16 slice. The times are simulated.
512 devices in a mesh: sp: 32 (over z, core), tp: 16 (over y, x).
Axes of the slice: x: 4, y: 4, z: 16, core: 2. Of those that a mesh axis runs over, the one named last changes fastest.
Arguments:
- queries: bfloat16 [8192, 2048], P('sp', 'tp'), may hold values from -6 to 6
- keys: bfloat16 [8192, 1024], P('sp', 'tp'), may hold values from -6 to 6
- values: bfloat16 [8192, 1024], P('sp', 'tp'), may hold values from -6 to 6
- sink_logit: float32 [32], P('tp'), may hold values from -1 to 6
- out_weight: bfloat16 [2048, 2048], P(None, 'tp'), may hold values from -0.125 to 0.125
- residual: bfloat16 [8192, 2048], P(('sp', 'tp')), may hold values from -1.796875 to 1.796875
- norm_gain: float32 [2048], replicated, may hold values from 0.1 to 1.9
- routes: int32 [8192, 2], P(('sp', 'tp')), may hold values from 0 to 31, all different within a row; in each aligned block of 16 rows (0 to 15, 16 to 31, ...) at most 2 rows name the same one
- route_weights: float32 [8192, 2], P(('sp', 'tp')), may hold values from 0.2 to 1
- gate_weight: bfloat16 [32, 2048, 5120], P('sp', None, 'tp'), may hold values from -0.125 to 0.125
- up_weight: bfloat16 [32, 2048, 5120], P('sp', None, 'tp'), may hold values from -0.125 to 0.125
- down_weight: bfloat16 [32, 5120, 2048], P('sp', 'tp'), may hold values from -0.078125 to 0.078125
Outputs:
- mixed: bfloat16 [8192, 2048], P(('sp', 'tp'))
Inputs may be any that keep to these rules, and one draw needn't show every extreme that they name: `routes`: each row names two different experts. Among the rows of one device no expert is named more than 2 times, and in every draw some expert is named exactly 2 times by the rows of some device.
All inputs are finite; a program needn't handle non-finite values.
Results may differ from a plain program's by a relative error of at most 0.018.
Values may be sent and summed in bfloat16 or wider, within the bound.
No kernel may reach another device: no remote copies, remote signals or barrier semaphores. Data moves between devices by JAX's collectives and lax.ppermute only.
A program may use at most 64 MiB of HBM per device.

v0:
```python
import jax
import jax.numpy as jnp
from jax import lax
from jax.sharding import PartitionSpec as P

HEADS = 32
KV_HEADS = 16
HEAD = 64
WINDOW = 128


EPS = 1e-06
NEGATIVE = -1e30


def with_halo(block, sides, width):
    for axis, dim in sides:
        count = lax.axis_size(axis)
        forward = [(i, i + 1) for i in range(count - 1)]
        backward = [(target, source) for source, target in forward]
        low = lax.ppermute(
            lax.slice_in_dim(block, block.shape[dim] - width, None, axis=dim), axis, forward
        )
        high = lax.ppermute(lax.slice_in_dim(block, 0, width, axis=dim), axis, backward)
        block = jnp.concatenate([low, block, high], axis=dim)
    return block


def sent_to_all(value, axis):
    copies = jnp.broadcast_to(value, (lax.axis_size(axis), *value.shape))
    return lax.all_to_all(copies, axis, split_axis=0, concat_axis=0, tiled=True)


def laid_out(tiles, dim):
    tiles = jnp.moveaxis(tiles, 0, dim)
    lengths = tiles.shape
    return tiles.reshape(*lengths[:dim], lengths[dim] * lengths[dim + 1], *lengths[dim + 2 :])


def gather_directly(value, axis, dim):
    tiles = sent_to_all(value, axis)
    return laid_out(tiles, dim)


def cut_along(value, dim, size):
    lengths = value.shape
    tiles = value.reshape(*lengths[:dim], size, lengths[dim] // size, *lengths[dim + 1 :])
    return jnp.moveaxis(tiles, dim, 0)


def summed_on_arrival(value, axis, dim):
    tiles = cut_along(value, dim, lax.axis_size(axis))
    arrived = lax.all_to_all(tiles, axis, split_axis=0, concat_axis=0, tiled=True)
    return arrived.astype(jnp.float32).sum(axis=0)


def make_band(extended, length):
    blocks = length // WINDOW
    pieces = [
        lax.slice_in_dim(extended, offset * WINDOW, offset * WINDOW + length, axis=0).reshape(
            blocks, WINDOW, -1
        )
        for offset in range(3)
    ]
    return jnp.concatenate(pieces, axis=1)


def attend_local(queries, keys, values, sink_logit):
    length = queries.shape[0]
    groups = keys.shape[1] // HEAD
    repeat = HEADS // KV_HEADS
    blocks = length // WINDOW
    joined = jnp.concatenate([keys, values], axis=1)
    extended = with_halo(joined, (("sp", 0),), WINDOW)
    banded = make_band(extended, length)
    key_band = banded[..., : groups * HEAD].reshape(blocks, 3 * WINDOW, groups, HEAD)
    value_band = banded[..., groups * HEAD :].reshape(blocks, 3 * WINDOW, groups, HEAD)
    query_blocks = queries.reshape(blocks, WINDOW, groups, repeat, HEAD)
    scores = jnp.einsum(
        "nqgrd,nkgd->ngrqk", query_blocks, key_band, preferred_element_type=jnp.float32
    ) * HEAD ** (-0.5)
    near = jnp.abs(jnp.arange(WINDOW)[:, None] + WINDOW - jnp.arange(3 * WINDOW)[None, :]) <= WINDOW
    first_token = lax.axis_index("sp") * length
    key_pos = (
        first_token + (jnp.arange(blocks)[:, None] - 1) * WINDOW + jnp.arange(3 * WINDOW)[None, :]
    )
    inside = (key_pos >= 0) & (key_pos < length * lax.axis_size("sp"))
    valid = near[None, None, None, :, :] & inside[:, None, None, None, :]
    sinks = sink_logit.reshape(1, groups, repeat, 1, 1)
    masked = jnp.where(valid, scores, NEGATIVE)
    top = jnp.maximum(jnp.max(masked, axis=-1, keepdims=True), sinks)
    probs = jnp.exp(masked - top)
    denom = jnp.sum(probs, axis=-1, keepdims=True) + jnp.exp(sinks - top)
    weights = (probs / denom).astype(jnp.bfloat16)
    output = jnp.einsum(
        "ngrqk,nkgd->nqgrd", weights, value_band, preferred_element_type=jnp.float32
    )
    return output.astype(jnp.bfloat16).reshape(length, groups * repeat * HEAD)


def local(
    queries,
    keys,
    values,
    sink_logit,
    out_weight,
    residual,
    norm_gain,
    routes,
    route_weights,
    gate_weight,
    up_weight,
    down_weight,
):
    attention = attend_local(queries, keys, values, sink_logit)
    columns = jnp.dot(
        gather_directly(attention, "tp", 1), out_weight, preferred_element_type=jnp.float32
    )
    projected = lax.all_to_all(
        columns.astype(jnp.bfloat16), "tp", split_axis=0, concat_axis=1, tiled=True
    )
    hidden_state = residual.astype(jnp.float32) + projected.astype(jnp.float32)
    inverse = lax.rsqrt(jnp.mean(hidden_state * hidden_state, axis=-1, keepdims=True) + EPS)
    normed = (hidden_state * inverse * norm_gain).astype(jnp.bfloat16)
    sp_count = lax.axis_size("sp")
    tok_rows = residual.shape[0]
    width = residual.shape[1]
    capacity = max(2, 4 * tok_rows // sp_count)
    slot_total = sp_count * capacity
    expert_ids = routes.reshape(-1)
    onehot = (expert_ids[:, None] == jnp.arange(sp_count, dtype=jnp.int32)[None, :]).astype(
        jnp.int32
    )
    earlier = jnp.cumsum(onehot, axis=0) - onehot
    rank = jnp.sum(earlier * onehot, axis=1)
    slots = expert_ids * capacity + rank
    placing = (slots[:, None] == jnp.arange(slot_total, dtype=jnp.int32)[None, :]).astype(
        jnp.bfloat16
    )
    placing = placing.reshape(tok_rows, 2, slot_total)
    first_place = placing[:, 0]
    second_place = placing[:, 1]
    sending = jnp.einsum(
        "ts,td->sd", first_place + second_place, normed, preferred_element_type=jnp.float32
    )
    sending = sending.astype(jnp.bfloat16).reshape(sp_count, capacity, width)
    piece = lax.all_gather(
        lax.all_to_all(sending, "sp", split_axis=0, concat_axis=0, tiled=True),
        "tp",
        axis=0,
        tiled=True,
    )
    flat = piece.reshape(-1, piece.shape[-1])
    gate = jnp.dot(flat, gate_weight[0], preferred_element_type=jnp.float32)
    upward = jnp.dot(flat, up_weight[0], preferred_element_type=jnp.float32)
    hidden = (jax.nn.silu(gate) * upward).astype(jnp.bfloat16)
    partial_value = jnp.dot(hidden, down_weight[0], preferred_element_type=jnp.float32)
    partial_value = partial_value.reshape(piece.shape[:-1] + (down_weight.shape[-1],))
    returned = lax.all_to_all(
        summed_on_arrival(partial_value.astype(jnp.bfloat16), "tp", 0).astype(jnp.bfloat16),
        "sp",
        split_axis=0,
        concat_axis=0,
        tiled=True,
    )
    gathered_back = returned.reshape(slot_total, width)
    first_pick = jnp.dot(first_place, gathered_back, preferred_element_type=jnp.float32)
    second_pick = jnp.dot(second_place, gathered_back, preferred_element_type=jnp.float32)
    mixture = route_weights[:, 0:1] * first_pick + route_weights[:, 1:2] * second_pick
    return (hidden_state + mixture).astype(jnp.bfloat16)


def solution(mesh):
    in_specs = (
        P("sp", "tp"),
        P("sp", "tp"),
        P("sp", "tp"),
        P("tp"),
        P(None, "tp"),
        P(("sp", "tp"), None),
        P(),
        P(("sp", "tp"), None),
        P(("sp", "tp"), None),
        P("sp", None, "tp"),
        P("sp", None, "tp"),
        P("sp", "tp", None),
    )
    out_specs = P(("sp", "tp"), None)
    return jax.shard_map(local, mesh=mesh, in_specs=in_specs, out_specs=out_specs, check_vma=False)
```

profile of v0, /device:TPU:1, one launch (start us, length us, event | category | flops | bytes accessed | tf_op | source)
XLA Modules:
  0.0 271.8 jit_solution(23323305794079645)
XLA Ops:
  6.5 1.0 copy.92
  7.5 0.9 copy.93
  8.4 0.1 fusion.17
  8.5 4.9 %collective-permute-start = (bf16[128,128]{1,0:T(8,128)(2,1)S(1)}, bf16[128,128]{1,0:T(8,128)(2,1)S(1)}, u32[]{:S(2)}, u32[]{:S(2)}) collective-permute-start(bf16[128,128]{1,0:T(8,128)(2,1)S(1)} %get-tuple-element.8), channel_id=1, source_target_pairs={{0,16},{16,32},{32,48},{48,64},{64,80},{80,96},{96,112},{112,128},... | collective-permute-start | bytes 98312 | tf_op jit(solution)/shard_map/ppermute | solution.py:21
  13.4 5.1 %collective-permute-start.1 = (bf16[128,128]{1,0:T(8,128)(2,1)S(1)}, bf16[128,128]{1,0:T(8,128)(2,1)S(1)}, u32[]{:S(2)}, u32[]{:S(2)}) collective-permute-start(bf16[128,128]{1,0:T(8,128)(2,1)S(1)} %get-tuple-element.9), channel_id=1, source_target_pairs={{16,0},{32,16},{48,32},{64,48},{80,64},{96,80},{112,96},{128,112},... | collective-permute-start | bytes 98312 | tf_op jit(solution)/shard_map/ppermute | solution.py:24
  18.6 0.1 abs_compare_fusion
  18.7 0.1 compare_and_fusion
  18.7 0.2 broadcast_and_fusion
  18.9 0.0 copy-start.6
  18.9 0.9 reshape.197
  19.9 0.0 collective-permute-done
  19.9 0.0 collective-permute-done.1
  19.9 0.1 pad_maximum_fusion.3
  20.0 0.1 copy.94
  20.1 0.1 copy.95
  20.3 0.1 copy.96
  20.4 0.3 fusion.24
  20.8 0.1 broadcast_maximum_fusion
  20.8 0.1 fusion.12
  21.0 0.1 exponential_add_fusion
  21.0 0.3 fusion.10
  21.3 0.1 copy.100
  21.4 1.1 broadcast_in_dim.16
  22.5 5.7 %all-to-all-start = ((bf16[16,256,128]{1,2,0:T(8,128)(2,1)}), bf16[16,256,128]{1,2,0:T(8,128)(2,1)S(1)}, u32[]{:S(2)}, u32[]{:S(2)}) async-start(bf16[16,256,128]{1,2,0:T(8,128)(2,1)} %broadcast_in_dim.16), calls=%async_computation | async-start | bytes 2097152 | tf_op jit(solution)/shard_map/all_to_all | solution.py:31
  28.2 0.0 copy-start.2
  28.2 0.0 copy-start.4
  28.2 0.1 copy.102
  28.3 0.1 eq.30
  28.4 0.1 fusion.19
  28.4 0.1 reduce_window_sum.11
  28.5 0.2 select_reduce_fusion
  28.7 0.1 reduce_sum.43
  28.8 0.1 copy.103
  28.9 15.9 %all-to-all-done = bf16[16,256,128]{1,2,0:T(8,128)(2,1)S(1)} async-done(((bf16[16,256,128]{1,2,0:T(8,128)(2,1)}), bf16[16,256,128]{1,2,0:T(8,128)(2,1)S(1)}, u32[]{:S(2)}, u32[]{:S(2)}) %all-to-all-start) | async-done | bytes 1048608 | tf_op jit(solution)/shard_map/all_to_all | solution.py:31
  44.7 1.1 convolution_convert_fusion.2
  45.8 3.5 %all-to-all-start.1 = ((bf16[16,16,128]{2,1,0:T(8,128)(2,1)}), bf16[16,16,128]{2,1,0:T(8,128)(2,1)S(1)}, u32[]{:S(2)}, u32[]{:S(2)}) async-start(bf16[16,16,128]{2,1,0:T(8,128)(2,1)} %bitcast.14), calls=%async_computation.1 | async-start | bytes 131072 | tf_op jit(solution)/shard_map/all_to_all | solution.py:119
  49.3 0.0 all-gather.2.cloned.1.call-start
  49.4 0.1 iota_compare_fusion
  49.5 6.7 %all-to-all-done.1 = bf16[16,16,128]{2,1,0:T(8,128)(2,1)S(1)} async-done(((bf16[16,16,128]{2,1,0:T(8,128)(2,1)}), bf16[16,16,128]{2,1,0:T(8,128)(2,1)S(1)}, u32[]{:S(2)}, u32[]{:S(2)}) %all-to-all-start.1) | async-done | bytes 65568 | tf_op jit(solution)/shard_map/all_to_all | solution.py:119
  56.1 0.1 multiply_reduce_fusion
  56.3 0.0 copy-done.4
  56.3 0.3 convolution_convert_fusion.1
  56.6 0.2 reshape.189
  56.8 40.8 %all_to_all.33 = bf16[32,2,2048]{2,1,0:T(2,128)(2,1)} all-to-all(bf16[32,2,2048]{2,1,0:T(2,128)(2,1)S(1)} %reshape.189), channel_id=1, replica_groups=mesh['sp'=32,'tp'=16] {'sp'}, dimensions={0} | all-to-all | bytes 524288 | tf_op jit(solution)/shard_map/all_to_all | solution.py:148
  97.6 0.0 all-gather.2.cloned.1.call-update
  97.6 0.0 copy-start.8
  97.6 54.4 %all-gather.2.cloned.1.call-done = bf16[512,2,2048]{2,1,0:T(2,128)(2,1)} async-done(((bf16[32,2,2048]{2,1,0:T(2,128)(2,1)}), bf16[512,2,2048]{2,1,0:T(2,128)(2,1)}) %all-gather.2.cloned.1.call-update) | async-done | bytes 4194320 | tf_op jit(solution)/shard_map/all_gather | solution.py:147
  152.0 7.3 %reshape.190 = bf16[1024,2048]{1,0:T(8,128)(2,1)} reshape(bf16[512,2,2048]{2,1,0:T(2,128)(2,1)} %all-gather.2.cloned.1.call-done) | data formatting | bytes 8388608 | tf_op jit(solution)/shard_map/reshape | solution.py:153
  159.3 4.0 %fusion.6 = f32[1024,320]{0,1:T(8,128)S(1)} fusion(bf16[1024,2048]{1,0:T(8,128)(2,1)} %reshape.190, bf16[1,2048,320]{1,2,0:T(8,128)(2,1)S(1)} %copy-done.8), kind=kOutput, calls=%fused_computation.11 | convolution fusion | flops 1342177280 | bytes 6815744 | tf_op jit(solution)/shard_map/dot_general | solution.py:154
  163.3 0.0 copy-done.1
  163.3 0.0 copy-done.9
  163.3 1.7 fusion.3
  165.0 0.4 copy.104
  165.4 0.3 dot_general.35
  165.7 2.3 convolution_convert_fusion
  168.1 0.6 copy.106
  168.7 54.8 %all_to_all.34 = bf16[16,32,2,2048]{3,1,2,0:T(8,128)(2,1)} all-to-all(bf16[16,32,2,2048]{3,1,2,0:T(8,128)(2,1)S(1)} %copy.106), channel_id=1, replica_groups=mesh['sp'=32,'tp'=16] {'tp'}, dimensions={0} | all-to-all | bytes 8388608 | tf_op jit(solution)/shard_map/all_to_all | solution.py:53
  223.4 3.0 %reduce_sum.45 = bf16[32,2,2048]{2,0,1:T(8,128)(2,1)S(1)} reduce(bf16[16,32,2,2048]{3,1,2,0:T(8,128)(2,1)} %all_to_all.34, bf16[]{:T(256)} %constant.43.clone.1), dimensions={0}, to_apply=%region_5.6 | reduce | flops 1966080 | bytes 4456450 | tf_op jit(solution)/shard_map/reduce_sum | solution.py:54
  226.4 1.0 copy.108
  227.4 14.3 %all-to-all-start.4 = ((bf16[32,2,2048]{2,1,0:T(2,128)(2,1)}), bf16[32,2,2048]{2,1,0:T(2,128)(2,1)S(1)}, u32[]{:S(2)}, u32[]{:S(2)}) async-start(bf16[32,2,2048]{2,1,0:T(2,128)(2,1)} %copy.108), calls=%async_computation.4 | async-start | bytes 524288 | tf_op jit(solution)/shard_map/all_to_all | solution.py:159
  241.7 22.2 %all-to-all-done.4 = bf16[32,2,2048]{2,1,0:T(2,128)(2,1)S(1)} async-done(((bf16[32,2,2048]{2,1,0:T(2,128)(2,1)}), bf16[32,2,2048]{2,1,0:T(2,128)(2,1)S(1)}, u32[]{:S(2)}, u32[]{:S(2)}) %all-to-all-start.4) | async-done | bytes 262176 | tf_op jit(solution)/shard_map/all_to_all | solution.py:159
  263.9 0.1 reshape.192
  264.0 0.2 convolution_multiply_fusion.1
  264.2 0.8 fusion.2
  (20 shorter events, 0.1 us)
Async XLA Ops:
  6.5 159.2 %copy-start = (bf16[1,320,2048]{2,1,0:T(8,128)(2,1)S(1)}, bf16[1,320,2048]{2,1,0:T(8,128)(2,1)}, u32[]{:S(2)}) copy-start(bf16[1,320,2048]{2,1,0:T(8,128)(2,1)} %param.23) | copy-start | bytes 3932164
  8.5 11.4 %collective-permute-start = (bf16[128,128]{1,0:T(8,128)(2,1)S(1)}, bf16[128,128]{1,0:T(8,128)(2,1)S(1)}, u32[]{:S(2)}, u32[]{:S(2)}) collective-permute-start(bf16[128,128]{1,0:T(8,128)(2,1)S(1)} %get-tuple-element.8), channel_id=1, source_target_pairs={{0,16},{16,32},{32,48},{48,64},{64,80},{80,96},{96,112},{112,128},... | collective-permute-start | bytes 98312 | tf_op jit(solution)/shard_map/ppermute | solution.py:21
  13.4 6.5 %collective-permute-start.1 = (bf16[128,128]{1,0:T(8,128)(2,1)S(1)}, bf16[128,128]{1,0:T(8,128)(2,1)S(1)}, u32[]{:S(2)}, u32[]{:S(2)}) collective-permute-start(bf16[128,128]{1,0:T(8,128)(2,1)S(1)} %get-tuple-element.9), channel_id=1, source_target_pairs={{16,0},{32,16},{48,32},{64,48},{80,64},{96,80},{112,96},{128,112},... | collective-permute-start | bytes 98312 | tf_op jit(solution)/shard_map/ppermute | solution.py:24
  18.9 1.8 copy-start.6
  22.5 5.7 %copy-start.5 = (s32[16,2]{0,1:T(2,128)S(1)}, s32[16,2]{0,1:T(2,128)}, u32[]{:S(2)}) copy-start(s32[16,2]{0,1:T(2,128)} %param.19) | copy-start | bytes 388
  22.5 22.2 %copy-start.3 = (bf16[2048,128]{1,0:T(8,128)(2,1)S(1)}, bf16[2048,128]{1,0:T(8,128)(2,1)}, u32[]{:S(2)}) copy-start(bf16[2048,128]{1,0:T(8,128)(2,1)} %param.16) | copy-start | bytes 1572868
  22.5 22.2 %all-to-all-start = ((bf16[16,256,128]{1,2,0:T(8,128)(2,1)}), bf16[16,256,128]{1,2,0:T(8,128)(2,1)S(1)}, u32[]{:S(2)}, u32[]{:S(2)}) async-start(bf16[16,256,128]{1,2,0:T(8,128)(2,1)} %broadcast_in_dim.16), calls=%async_computation | async-start | bytes 2097152 | tf_op jit(solution)/shard_map/all_to_all | solution.py:31
  28.2 28.0 %copy-start.2 = (bf16[16,2048]{1,0:T(8,128)(2,1)S(1)}, bf16[16,2048]{1,0:T(8,128)(2,1)}, u32[]{:S(2)}) copy-start(bf16[16,2048]{1,0:T(8,128)(2,1)} %param.17) | copy-start | bytes 196612
  28.2 28.1 %copy-start.4 = (f32[2048]{0:T(1024)S(1)}, f32[2048]{0:T(1024)}, u32[]{:S(2)}) copy-start(f32[2048]{0:T(1024)} %param.18) | copy-start | bytes 24580
  45.8 10.3 %all-to-all-start.1 = ((bf16[16,16,128]{2,1,0:T(8,128)(2,1)}), bf16[16,16,128]{2,1,0:T(8,128)(2,1)S(1)}, u32[]{:S(2)}, u32[]{:S(2)}) async-start(bf16[16,16,128]{2,1,0:T(8,128)(2,1)} %bitcast.14), calls=%async_computation.1 | async-start | bytes 131072 | tf_op jit(solution)/shard_map/all_to_all | solution.py:119
  49.3 102.7 %all-gather.2.cloned.1.call-start = ((), (), s32[]{:S(2)}) async-start(), calls=%async_computation.5 | async-start | bytes 4456448 | tf_op jit(solution)/shard_map/all_gather | solution.py:147
  97.6 61.6 %copy-start.8 = (bf16[1,2048,320]{1,2,0:T(8,128)(2,1)S(1)}, bf16[1,2048,320]{1,2,0:T(8,128)(2,1)}, u32[]{:S(2)}) copy-start(bf16[1,2048,320]{1,2,0:T(8,128)(2,1)} %param.21) | copy-start | bytes 3932164
  159.3 4.0 %copy-start.1 = (bf16[1024,2048]{1,0:T(8,128)(2,1)S(1)}, bf16[1024,2048]{1,0:T(8,128)(2,1)}, u32[]{:S(2)}) copy-start(bf16[1024,2048]{1,0:T(8,128)(2,1)} %reshape.190) | copy-start | bytes 12582916
  159.3 4.0 %copy-start.9 = (bf16[1,2048,320]{1,2,0:T(8,128)(2,1)S(1)}, bf16[1,2048,320]{1,2,0:T(8,128)(2,1)}, u32[]{:S(2)}) copy-start(bf16[1,2048,320]{1,2,0:T(8,128)(2,1)} %param.22) | copy-start | bytes 3932164
  223.4 18.2 %copy-start.7 = (f32[16,2]{0,1:T(2,128)S(1)}, f32[16,2]{0,1:T(2,128)}, u32[]{:S(2)}) copy-start(f32[16,2]{0,1:T(2,128)} %param.20) | copy-start | bytes 388
  227.4 36.5 %all-to-all-start.4 = ((bf16[32,2,2048]{2,1,0:T(2,128)(2,1)}), bf16[32,2,2048]{2,1,0:T(2,128)(2,1)S(1)}, u32[]{:S(2)}, u32[]{:S(2)}) async-start(bf16[32,2,2048]{2,1,0:T(2,128)(2,1)} %copy.108), calls=%async_computation.4 | async-start | bytes 524288 | tf_op jit(solution)/shard_map/all_to_all | solution.py:159
Sparse Core Ops, SparseCore 0:
  97.7 54.2 all-gather.1
where the time goes:
time: 273 us; the launch traced here: 272 us
  waiting for transfers between devices  99.2 us (36%)
  blocking collectives  95.6 us (35%)
  starting transfers between devices  33.5 us (12%)
  local copies, waits for them, and re-layouts  14.5 us (5%)
  between operations  13.8 us (5%)
  matrix products  10.9 us (4%)
  other arithmetic  4.35 us (2%)
    all_to_all x1, blocking collectives, summed_on_arrival(): lax.all_to_all(tiles, axis, split_axis=0, concat_axis=0, tiled=True)  54.8 us
    all_gather x1, waiting for transfers between devices, local(): lax.all_gather(lax.all_to_all(sending, 'sp', split_axis=0, concat_axis=0,...  54.4 us
    all_to_all x1, blocking collectives, local(): lax.all_to_all(sending, 'sp', split_axis=0, concat_axis=0, tiled=True)  40.8 us
    all_to_all x1, waiting for transfers between devices, local(): lax.all_to_all(summed_on_arrival(partial_value.astype(jnp.bfloat16), 'tp'...  22.2 us
    all_to_all x1, waiting for transfers between devices, sent_to_all(): return lax.all_to_all(copies, axis, split_axis=0, concat_axis=0, tiled=True)  15.9 us
    all_to_all x1, starting transfers between devices, local(): lax.all_to_all(summed_on_arrival(partial_value.astype(jnp.bfloat16), 'tp'...  14.3 us
    reshape x1, local copies, waits for them, and re-layouts, local(): flat = piece.reshape(-1, piece.shape[-1])  7.26 us
    all_to_all x1, waiting for transfers between devices, local(): lax.all_to_all(columns.astype(jnp.bfloat16), 'tp', split_axis=0, concat_a...  6.68 us
  transfers between devices with their start and end apart: 6, of which 4 were waited for; matrix products, arithmetic and copies ran while one was open for 1% of the time, Pallas kernels for 0%

commit v1 on v0

v1 whole, which is shorter than its diff:
```python
import jax
import jax.numpy as jnp
from jax import lax
from jax.sharding import PartitionSpec as P

HEADS = 32
KV_HEADS = 16
HEAD = 64
WINDOW = 128

EPS = 1e-06
NEGATIVE = -1e30


def halo(block, width):
    count = lax.axis_size("sp")
    forward = [(i, i + 1) for i in range(count - 1)]
    backward = [(target, source) for source, target in forward]
    low = lax.ppermute(block[-width:], "sp", forward)
    high = lax.ppermute(block[:width], "sp", backward)
    return jnp.concatenate([low, block, high], axis=0)


def make_band(extended, length):
    blocks = length // WINDOW
    pieces = [
        lax.slice_in_dim(extended, offset * WINDOW, offset * WINDOW + length, axis=0).reshape(
            blocks, WINDOW, -1
        )
        for offset in range(3)
    ]
    return jnp.concatenate(pieces, axis=1)


def attend_local(queries, keys, values, sink_logit):
    length = queries.shape[0]
    groups = keys.shape[1] // HEAD
    repeat = HEADS // KV_HEADS
    blocks = length // WINDOW
    joined = jnp.concatenate([keys, values], axis=1)
    extended = halo(joined, WINDOW)
    banded = make_band(extended, length)
    key_band = banded[..., : groups * HEAD].reshape(blocks, 3 * WINDOW, groups, HEAD)
    value_band = banded[..., groups * HEAD :].reshape(blocks, 3 * WINDOW, groups, HEAD)
    query_blocks = queries.reshape(blocks, WINDOW, groups, repeat, HEAD)
    scores = jnp.einsum(
        "nqgrd,nkgd->ngrqk", query_blocks, key_band, preferred_element_type=jnp.float32
    ) * HEAD ** (-0.5)
    near = jnp.abs(jnp.arange(WINDOW)[:, None] + WINDOW - jnp.arange(3 * WINDOW)[None, :]) <= WINDOW
    first_token = lax.axis_index("sp") * length
    key_pos = (
        first_token + (jnp.arange(blocks)[:, None] - 1) * WINDOW + jnp.arange(3 * WINDOW)[None, :]
    )
    inside = (key_pos >= 0) & (key_pos < length * lax.axis_size("sp"))
    valid = near[None, None, None, :, :] & inside[:, None, None, None, :]
    sinks = sink_logit.reshape(1, groups, repeat, 1, 1)
    masked = jnp.where(valid, scores, NEGATIVE)
    top = jnp.maximum(jnp.max(masked, axis=-1, keepdims=True), sinks)
    probs = jnp.exp(masked - top)
    denom = jnp.sum(probs, axis=-1, keepdims=True) + jnp.exp(sinks - top)
    weights = (probs / denom).astype(jnp.bfloat16)
    output = jnp.einsum(
        "ngrqk,nkgd->nqgrd", weights, value_band, preferred_element_type=jnp.float32
    )
    return output.astype(jnp.bfloat16).reshape(length, groups * repeat * HEAD)


def exchange(value, axis, groups=None):
    return lax.all_to_all(
        value, axis, split_axis=0, concat_axis=0, tiled=True, axis_index_groups=groups
    )


def local(
    queries,
    keys,
    values,
    sink_logit,
    out_weight,
    residual,
    norm_gain,
    routes,
    route_weights,
    gate_weight,
    up_weight,
    down_weight,
):
    n_sp, n_tp = lax.axis_size("sp"), lax.axis_size("tp")
    planes = n_sp // 2
    pairs = n_tp // 2
    tok_rows, width = residual.shape
    cols = width // n_tp
    length = queries.shape[0]
    parity = lax.axis_index("tp") % 2
    same_core = [[plane * 2 + core for plane in range(planes)] for core in range(2)]
    same_parity = [[pair * 2 + side for pair in range(pairs)] for side in range(2)]

    to_server = []
    for plane in range(planes):
        for core in range(2):
            for member in range(n_tp):
                source = (plane * 2 + core) * n_tp + member
                if member % 2 == core:
                    to_server.append((source, source))
                else:
                    to_server.append((source, (plane * 2 + 1 - core) * n_tp + (member ^ 1)))
    swap_core = [(s, s ^ 1) for s in range(n_sp)]
    swap_pair = [(t, t ^ 1) for t in range(n_tp)]
    gate_up = jnp.concatenate(
        [
            gate_weight[0, :, :256],
            up_weight[0, :, :256],
            gate_weight[0, :, 256:],
            up_weight[0, :, 256:],
        ],
        axis=1,
    )
    out_other = lax.ppermute(out_weight, "tp", swap_pair)
    down_one = lax.ppermute(down_weight[0], ("sp", "tp"), to_server)
    gate_up_one = lax.ppermute(gate_up, ("sp", "tp"), to_server)
    down_two = lax.ppermute(down_one, "sp", swap_core)
    gate_up_two = lax.ppermute(gate_up_one, "sp", swap_core)

    expert_ids = routes.reshape(-1)
    onehot = (expert_ids[:, None] == jnp.arange(n_sp, dtype=jnp.int32)[None, :]).astype(jnp.int32)
    earlier = jnp.cumsum(onehot, axis=0) - onehot
    rank = jnp.sum(earlier * onehot, axis=1)
    slots = (expert_ids * 2 + rank).reshape(tok_rows, 2)

    attention = attend_local(queries, keys, values, sink_logit)

    residual_pieces = residual.reshape(tok_rows, pairs, 2, cols).transpose(1, 2, 0, 3)
    residual_pieces = jnp.repeat(residual_pieces.reshape(pairs, 2 * tok_rows, cols), 2, axis=0)
    slot_rows = jnp.pad(slots.astype(jnp.bfloat16), ((0, 0), (0, cols - 2)))
    message = jnp.concatenate(
        [
            jnp.broadcast_to(attention, (n_tp, *attention.shape)),
            residual_pieces,
            jnp.broadcast_to(slot_rows, (n_tp, *slot_rows.shape)),
        ],
        axis=1,
    )
    arrived = exchange(message, "tp")
    attended = arrived[:, :length].transpose(1, 0, 2).reshape(length, width)
    residual_cols = (
        arrived[:, length : length + 2 * tok_rows]
        .reshape(n_tp, 2, tok_rows, cols)
        .transpose(0, 2, 1, 3)
        .reshape(length, 2 * cols)
    )
    slot_all = arrived[:, length + 2 * tok_rows :, :2].reshape(length, 2).astype(jnp.int32)

    own = jnp.dot(attended, out_weight, preferred_element_type=jnp.float32).astype(jnp.bfloat16)
    other = jnp.dot(attended, out_other, preferred_element_type=jnp.float32).astype(jnp.bfloat16)
    projected = jnp.concatenate(
        [jnp.where(parity == 0, own, other), jnp.where(parity == 0, other, own)], axis=1
    )
    hidden_cols = (residual_cols.astype(jnp.float32) + projected.astype(jnp.float32)).astype(
        jnp.bfloat16
    )
    wanted = (2 * jnp.arange(planes)[:, None] + parity) * 2 + jnp.arange(2)[None, :]
    named = jnp.any(slot_all[None, None] == wanted[:, :, None, None], axis=-1)
    mine = (jnp.arange(length) // tok_rows)[None, :] == jnp.arange(n_tp)[:, None]
    placing = (named[:, None] & mine[None, :, None]).astype(jnp.bfloat16)
    sending = jnp.dot(
        placing.reshape(planes * n_tp * 2, length), hidden_cols, preferred_element_type=jnp.float32
    ).astype(jnp.bfloat16)

    dispatched = exchange(sending.reshape(planes, n_tp * 2, 2 * cols), "sp", same_core)
    rows = planes * n_tp * 2
    block = dispatched.reshape(planes, n_tp, 2, 2 * cols).transpose(1, 2, 0, 3)
    block = block.reshape(rows, 2 * cols)
    gathered = exchange(jnp.broadcast_to(block, (pairs, *block.shape)), "tp", same_parity)
    flat = gathered.transpose(1, 0, 2).reshape(rows, width).astype(jnp.float32)
    inverse = lax.rsqrt(jnp.mean(flat * flat, axis=-1, keepdims=True) + EPS)
    normed = (flat * inverse * norm_gain).astype(jnp.bfloat16)

    def hidden_of(weights):
        both = jnp.dot(normed, weights, preferred_element_type=jnp.float32)
        gate = jnp.concatenate([both[:, :256], both[:, 512:576]], axis=1)
        upward = jnp.concatenate([both[:, 256:512], both[:, 576:]], axis=1)
        return (jax.nn.silu(gate) * upward).astype(jnp.bfloat16)

    share = jnp.dot(hidden_of(gate_up_one), down_one, preferred_element_type=jnp.float32)
    share = share + jnp.dot(hidden_of(gate_up_two), down_two, preferred_element_type=jnp.float32)

    pieces = share.astype(jnp.bfloat16).reshape(n_tp, 2 * planes, n_tp, cols).transpose(0, 2, 1, 3)
    pieces = pieces.reshape(n_tp, n_tp * 2 * planes, cols)
    pieces = jnp.concatenate([pieces, own.reshape(n_tp, tok_rows, cols)], axis=1)
    shares = exchange(pieces, "tp")
    main = shares[:, : n_tp * 2 * planes].astype(jnp.float32)
    main = main.reshape(pairs, 2, n_tp, 2, planes, cols).sum(axis=0).astype(jnp.bfloat16)
    own_rows = shares[:, n_tp * 2 * planes :].transpose(1, 0, 2).reshape(tok_rows, width)

    returning = main.transpose(3, 1, 0, 2, 4).reshape(planes, n_tp * 4, cols)
    returned = exchange(returning, "sp", same_core)
    returned = returned.reshape(planes, n_tp, 4, cols).transpose(0, 2, 1, 3).reshape(2 * n_sp, width)
    place = (slots[:, :, None] == jnp.arange(2 * n_sp)[None, None, :]).astype(jnp.bfloat16)
    first = jnp.dot(place[:, 0], returned, preferred_element_type=jnp.float32)
    second = jnp.dot(place[:, 1], returned, preferred_element_type=jnp.float32)
    mixture = route_weights[:, 0:1] * first + route_weights[:, 1:2] * second
    hidden_state = residual.astype(jnp.float32) + own_rows.astype(jnp.float32)
    return (hidden_state + mixture).astype(jnp.bfloat16)


def solution(mesh):
    in_specs = (
        P("sp", "tp"),
        P("sp", "tp"),
        P("sp", "tp"),
        P("tp"),
        P(None, "tp"),
        P(("sp", "tp"), None),
        P(),
        P(("sp", "tp"), None),
        P(("sp", "tp"), None),
        P("sp", None, "tp"),
        P("sp", None, "tp"),
        P("sp", "tp", None),
    )
    out_specs = P(("sp", "tp"), None)
    return jax.shard_map(local, mesh=mesh, in_specs=in_specs, out_specs=out_specs, check_vma=False)
```

time: 273 us -> 212 us (0.78)
  the two profiles are of different devices: /device:TPU:1 before, /device:TPU:32 now
where the time goes in v1:
time: 212 us; the launch traced here: 210 us
  starting transfers between devices  86 us (41%)
  blocking collectives  68 us (32%)
  waiting for transfers between devices  17.5 us (8%)
  matrix products  16 us (8%)
  local copies, waits for them, and re-layouts  13.7 us (6%)
  other arithmetic  7.76 us (4%)
    all_to_all x2, blocking collectives, exchange(): lax.all_to_all(value, axis, split_axis=0, concat_axis=0, tiled=True, axis...  68 us
    ppermute x1, starting transfers between devices, local(): down_two = lax.ppermute(down_one, 'sp', swap_core)  32 us
    ppermute x1, starting transfers between devices, local(): gate_up_one = lax.ppermute(gate_up, ('sp', 'tp'), to_server)  21.2 us
    all_to_all x3, starting transfers between devices, exchange(): lax.all_to_all(value, axis, split_axis=0, concat_axis=0, tiled=True, axis...  20.1 us
    all_to_all x3, waiting for transfers between devices, exchange(): lax.all_to_all(value, axis, split_axis=0, concat_axis=0, tiled=True, axis...  17.5 us
    dot_general x2, matrix products, hidden_of(): both = jnp.dot(normed, weights, preferred_element_type=jnp.float32)  7.24 us
  transfers between devices with their start and end apart: 10, of which 1 were waited for; matrix products, arithmetic and copies ran while one was open for 13% of the time, Pallas kernels for 0%

profile of v1, /device:TPU:32, one launch (start us, length us, event | category | flops | bytes accessed | tf_op | source)
XLA Modules:
  0.0 209.5 jit_solution(5512332750424631834)
XLA Ops:
  0.0 0.9 copy.120
  0.9 0.9 copy.121
  1.8 0.1 fusion.27
  1.9 1.9 collective-permute-start
  3.8 3.6 %collective-permute-start.1 = (bf16[128,128]{1,0:T(8,128)(2,1)S(1)}, bf16[128,128]{1,0:T(8,128)(2,1)S(1)}, u32[]{:S(2)}, u32[]{:S(2)}) collective-permute-start(bf16[128,128]{1,0:T(8,128)(2,1)S(1)} %get-tuple-element.21), channel_id=1, source_target_pairs={{16,0},{32,16},{48,32},{64,48},{80,64},{96,80},{112,96},{128,112},... | collective-permute-start | bytes 98312 | tf_op jit(solution)/shard_map/ppermute | solution.py:20
  7.4 3.4 %collective-permute-start.2 = (bf16[2048,128]{1,0:T(8,128)(2,1)}, bf16[2048,128]{1,0:T(8,128)(2,1)}, u32[]{:S(2)}, u32[]{:S(2)}) collective-permute-start(bf16[2048,128]{1,0:T(8,128)(2,1)} %param.16), channel_id=1, source_target_pairs={{0,1},{1,0},{2,3},{3,2},{4,5},{5,4},{6,7},{7,6},{8,9},{9,8},{10,11... | collective-permute-start | bytes 1572872 | tf_op jit(solution)/shard_map/ppermute | solution.py:118
  11.0 0.8 copy.131
  12.0 0.2 select_reduce_fusion
  12.3 0.1 copy.132
  12.4 0.2 broadcast_and_fusion.1
  12.6 1.7 slice_bitcast_fusion.1
  14.3 0.1 reshape.313
  14.4 0.1 copy.155
  14.6 0.1 pad_maximum_fusion.8
  14.7 0.1 copy.122
  14.9 0.1 copy.123
  15.0 0.1 copy.124
  15.2 0.3 fusion.39
  15.6 0.1 fusion.11
  15.8 0.3 fusion.8
  16.1 0.1 copy.153
  16.2 0.1 reshape.314
  16.3 0.2 broadcast_in_dim.22
  16.6 1.2 pad_maximum_fusion.2
  17.7 6.7 %all-to-all-start = ((bf16[16,304,128]{2,1,0:T(8,128)(2,1)}), bf16[16,304,128]{2,1,0:T(8,128)(2,1)S(1)}, u32[]{:S(2)}, u32[]{:S(2)}) async-start(bf16[16,304,128]{2,1,0:T(8,128)(2,1)} %pad_maximum_fusion.2), calls=%async_computation | async-start | bytes 2490368 | tf_op jit(solution)/shard_map/all_to_all | solution.py:69
  24.5 1.1 slice_bitcast_fusion.3
  25.5 1.7 pad_maximum_fusion
  27.2 21.2 %collective-permute-start.3 = (bf16[2048,640]{0,1:T(8,128)(2,1)}, bf16[2048,640]{0,1:T(8,128)(2,1)}, u32[]{:S(2)}, u32[]{:S(2)}) collective-permute-start(bf16[2048,640]{0,1:T(8,128)(2,1)} %pad_maximum_fusion), channel_id=1, source_target_pairs={{0,0},{1,16},{2,2},{3,18},{4,4},{5,20},{6,6},{7,22},{8,8},{9,24},{... | collective-permute-start | bytes 7864328 | tf_op jit(solution)/shard_map/ppermute | solution.py:120
  48.5 0.1 slice_bitcast_fusion
  48.6 0.5 copy.136
  49.1 1.5 convolution_convert_fusion.2
  50.6 1.5 broadcast_select_fusion.1
  52.2 0.1 reshape.307
  52.4 0.1 copy.139
  52.7 0.3 broadcast_and_fusion
  53.0 0.3 and.77
  53.4 0.2 convolution_convert_fusion
  53.6 31.0 %all_to_all.25 = bf16[16,32,256]{2,1,0:T(8,128)(2,1)S(1)} all-to-all(bf16[16,32,256]{2,1,0:T(8,128)(2,1)S(1)} %bitcast.133), channel_id=1, replica_groups={{0,32,64,96,128,160,192,224,256,288,320,352,384,416,448,480},{16,48,80,..., dimensions={0} | all-to-all | bytes 524288 | tf_op jit(solution)/shard_map/all_to_all | solution.py:69
  84.6 0.1 copy.140
  84.7 0.1 copy.141
  84.9 1.5 broadcast_in_dim.25
  86.4 7.1 %all-to-all-start.2 = ((bf16[8,512,256]{1,2,0:T(8,128)(2,1)}), bf16[8,512,256]{1,2,0:T(8,128)(2,1)S(1)}, u32[]{:S(2)}, u32[]{:S(2)}) async-start(bf16[8,512,256]{1,2,0:T(8,128)(2,1)} %broadcast_in_dim.25), calls=%async_computation.2 | async-start | bytes 4194304 | tf_op jit(solution)/shard_map/all_to_all | solution.py:69
  93.5 1.8 collective-permute-start.4
  95.3 1.9 collective-permute-start.5
  97.3 32.0 %collective-permute-start.6 = (bf16[320,2048]{1,0:T(8,128)(2,1)}, bf16[320,2048]{1,0:T(8,128)(2,1)S(1)}, u32[]{:S(2)}, u32[]{:S(2)}) collective-permute-start(bf16[320,2048]{1,0:T(8,128)(2,1)} %collective-permute-done.4), channel_id=1, source_target_pairs={{0,16},{16,0},{32,48},{48,32},{64,80},{80,64},{96,112},{112,96},{1... | collective-permute-start | bytes 3932168 | tf_op jit(solution)/shard_map/ppermute | solution.py:121
  129.3 0.5 multiply_reduce_fusion
  129.8 0.5 fusion.1
  130.4 3.6 %fusion.40 = f32[512,640]{1,0:T(8,128)S(1)} fusion(bf16[512,2048]{0,1:T(8,128)(2,1)S(1)} %fusion.1, bf16[2048,640]{0,1:T(8,128)(2,1)} %collective-permute-done.3), kind=kOutput, calls=%fused_computation.106 | convolution fusion | flops 1342177280 | bytes 6029312 | tf_op jit(solution)/shard_map/dot_general | solution.py:179
  134.0 0.1 fusion.38
  134.2 2.6 %fusion.13 = f32[512,2048]{1,0:T(8,128)S(1)} fusion(bf16[320,2048]{1,0:T(8,128)(2,1)} %collective-permute-done.4, f32[512,64]{1,0:T(8,128)S(1)} %get-tuple-element.14, f32[512,256]{1,0:T(8,128)S(1)} %get-tuple-element.12, f32[512,64]{1,0:T(8,128)S(1)} %get-tuple-element.13, f32[512,256]{1,0:T(8,128)S(1)} %get-tuple-element.11), kind=kOutput, calls=%fused_computation.35 | convolution fusion | flops 672399360 | bytes 6815744 | tf_op jit(solution)/shard_map/dot_general | solution.py:184
  136.8 3.6 %fusion.41 = f32[512,640]{1,0:T(8,128)S(1)} fusion(bf16[512,2048]{0,1:T(8,128)(2,1)S(1)} %fusion.1, bf16[2048,640]{0,1:T(8,128)(2,1)} %collective-permute-done.5), kind=kOutput, calls=%fused_computation.107 | convolution fusion | flops 1342177280 | bytes 6029312 | tf_op jit(solution)/shard_map/dot_general | solution.py:179
  140.5 0.1 fusion.36
  140.7 1.3 fusion.5
  142.0 0.6 copy.158
  142.6 0.5 copy.142
  143.2 0.2 pad_maximum_fusion.1
  143.4 37.0 %all_to_all.26 = bf16[16,528,128]{2,1,0:T(8,128)(2,1)S(1)} all-to-all(bf16[16,528,128]{2,1,0:T(8,128)(2,1)S(1)} %pad_maximum_fusion.1), channel_id=1, replica_groups=mesh['sp'=32,'tp'=16] {'tp'}, dimensions={0} | all-to-all | bytes 4325376 | tf_op jit(solution)/shard_map/all_to_all | solution.py:69
  180.3 1.5 slice.129
  181.9 2.0 reduce.4
  183.9 0.8 copy.145
  184.6 6.3 %all-to-all-start.4 = ((bf16[16,64,128]{2,1,0:T(8,128)(2,1)}), bf16[16,64,128]{2,1,0:T(8,128)(2,1)S(1)}, u32[]{:S(2)}, u32[]{:S(2)}) async-start(bf16[16,64,128]{2,1,0:T(8,128)(2,1)} %copy.145), calls=%async_computation.4 | async-start | bytes 524288 | tf_op jit(solution)/shard_map/all_to_all | solution.py:69
  191.0 17.5 %all-to-all-done.4 = bf16[16,64,128]{2,1,0:T(8,128)(2,1)S(1)} async-done(((bf16[16,64,128]{2,1,0:T(8,128)(2,1)}), bf16[16,64,128]{2,1,0:T(8,128)(2,1)S(1)}, u32[]{:S(2)}, u32[]{:S(2)}) %all-to-all-start.4) | async-done | bytes 262176 | tf_op jit(solution)/shard_map/all_to_all | solution.py:69
  208.6 0.2 convolution_multiply_fusion.1
  208.7 0.8 fusion.4
  (59 shorter events, 1.4 us)
Async XLA Ops:
  1.9 12.8 %collective-permute-start = (bf16[128,128]{1,0:T(8,128)(2,1)S(1)}, bf16[128,128]{1,0:T(8,128)(2,1)S(1)}, u32[]{:S(2)}, u32[]{:S(2)}) collective-permute-start(bf16[128,128]{1,0:T(8,128)(2,1)S(1)} %get-tuple-element.20), channel_id=1, source_target_pairs={{0,16},{16,32},{32,48},{48,64},{64,80},{80,96},{96,112},{112,128},... | collective-permute-start | bytes 98312 | tf_op jit(solution)/shard_map/ppermute | solution.py:19
  3.8 10.8 %collective-permute-start.1 = (bf16[128,128]{1,0:T(8,128)(2,1)S(1)}, bf16[128,128]{1,0:T(8,128)(2,1)S(1)}, u32[]{:S(2)}, u32[]{:S(2)}) collective-permute-start(bf16[128,128]{1,0:T(8,128)(2,1)S(1)} %get-tuple-element.21), channel_id=1, source_target_pairs={{16,0},{32,16},{48,32},{64,48},{80,64},{96,80},{112,96},{128,112},... | collective-permute-start | bytes 98312 | tf_op jit(solution)/shard_map/ppermute | solution.py:20
  7.4 43.2 %collective-permute-start.2 = (bf16[2048,128]{1,0:T(8,128)(2,1)}, bf16[2048,128]{1,0:T(8,128)(2,1)}, u32[]{:S(2)}, u32[]{:S(2)}) collective-permute-start(bf16[2048,128]{1,0:T(8,128)(2,1)} %param.16), channel_id=1, source_target_pairs={{0,1},{1,0},{2,3},{3,2},{4,5},{5,4},{6,7},{7,6},{8,9},{9,8},{10,11... | collective-permute-start | bytes 1572872 | tf_op jit(solution)/shard_map/ppermute | solution.py:118
  12.4 1.9 copy-start.3
  12.4 2.0 copy-start.1
  12.6 2.0 copy-start
  14.3 1.2 copy-start.4
  17.7 30.7 %all-to-all-start = ((bf16[16,304,128]{2,1,0:T(8,128)(2,1)}), bf16[16,304,128]{2,1,0:T(8,128)(2,1)S(1)}, u32[]{:S(2)}, u32[]{:S(2)}) async-start(bf16[16,304,128]{2,1,0:T(8,128)(2,1)} %pad_maximum_fusion.2), calls=%async_computation | async-start | bytes 2490368 | tf_op jit(solution)/shard_map/all_to_all | solution.py:69
  27.2 68.1 %collective-permute-start.3 = (bf16[2048,640]{0,1:T(8,128)(2,1)}, bf16[2048,640]{0,1:T(8,128)(2,1)}, u32[]{:S(2)}, u32[]{:S(2)}) collective-permute-start(bf16[2048,640]{0,1:T(8,128)(2,1)} %pad_maximum_fusion), channel_id=1, source_target_pairs={{0,0},{1,16},{2,2},{3,18},{4,4},{5,20},{6,6},{7,22},{8,8},{9,24},{... | collective-permute-start | bytes 7864328 | tf_op jit(solution)/shard_map/ppermute | solution.py:120
  86.4 7.1 %copy-start.6 = (bf16[1,320,2048]{2,1,0:T(8,128)(2,1)S(1)}, bf16[1,320,2048]{2,1,0:T(8,128)(2,1)}, u32[]{:S(2)}) copy-start(bf16[1,320,2048]{2,1,0:T(8,128)(2,1)} %param.23) | copy-start | bytes 3932164
  86.4 43.4 %copy-start.2 = (f32[2048]{0:T(1024)S(1)}, f32[2048]{0:T(1024)}, u32[]{:S(2)}) copy-start(f32[2048]{0:T(1024)} %param.18) | copy-start | bytes 24580
  86.4 42.9 %all-to-all-start.2 = ((bf16[8,512,256]{1,2,0:T(8,128)(2,1)}), bf16[8,512,256]{1,2,0:T(8,128)(2,1)S(1)}, u32[]{:S(2)}, u32[]{:S(2)}) async-start(bf16[8,512,256]{1,2,0:T(8,128)(2,1)} %broadcast_in_dim.25), calls=%async_computation.2 | async-start | bytes 4194304 | tf_op jit(solution)/shard_map/all_to_all | solution.py:69
  93.5 3.7 %collective-permute-start.4 = (bf16[320,2048]{1,0:T(8,128)(2,1)S(1)}, bf16[320,2048]{1,0:T(8,128)(2,1)}, u32[]{:S(2)}, u32[]{:S(2)}) collective-permute-start(bf16[320,2048]{1,0:T(8,128)(2,1)S(1)} %bitcast.145), channel_id=1, source_target_pairs={{0,0},{1,16},{2,2},{3,18},{4,4},{5,20},{6,6},{7,22},{8,8},{9,24},{... | collective-permute-start | bytes 3932168 | tf_op jit(solution)/shard_map/ppermute | solution.py:119
  95.3 41.5 %collective-permute-start.5 = (bf16[2048,640]{0,1:T(8,128)(2,1)}, bf16[2048,640]{0,1:T(8,128)(2,1)}, u32[]{:S(2)}, u32[]{:S(2)}) collective-permute-start(bf16[2048,640]{0,1:T(8,128)(2,1)} %collective-permute-done.3), channel_id=1, source_target_pairs={{0,16},{16,0},{32,48},{48,32},{64,80},{80,64},{96,112},{112,96},{1... | collective-permute-start | bytes 7864328 | tf_op jit(solution)/shard_map/ppermute | solution.py:122
  97.3 43.4 %collective-permute-start.6 = (bf16[320,2048]{1,0:T(8,128)(2,1)}, bf16[320,2048]{1,0:T(8,128)(2,1)S(1)}, u32[]{:S(2)}, u32[]{:S(2)}) collective-permute-start(bf16[320,2048]{1,0:T(8,128)(2,1)} %collective-permute-done.4), channel_id=1, source_target_pairs={{0,16},{16,0},{32,48},{48,32},{64,80},{80,64},{96,112},{112,96},{1... | collective-permute-start | bytes 3932168 | tf_op jit(solution)/shard_map/ppermute | solution.py:121
  181.9 9.1 %copy-start.5 = (f32[16,2]{0,1:T(2,128)S(1)}, f32[16,2]{0,1:T(2,128)}, u32[]{:S(2)}) copy-start(f32[16,2]{0,1:T(2,128)} %param.20) | copy-start | bytes 388
  184.6 23.9 %all-to-all-start.4 = ((bf16[16,64,128]{2,1,0:T(8,128)(2,1)}), bf16[16,64,128]{2,1,0:T(8,128)(2,1)S(1)}, u32[]{:S(2)}, u32[]{:S(2)}) async-start(bf16[16,64,128]{2,1,0:T(8,128)(2,1)} %copy.145), calls=%async_computation.4 | async-start | bytes 524288 | tf_op jit(solution)/shard_map/all_to_all | solution.py:69

commit v2 on v1

--- a/solution.py
+++ b/solution.py
@@ -1,7 +1,10 @@
 import jax
 import jax.numpy as jnp
 from jax import lax
+from jax.experimental import pallas as pl
+from jax.experimental.pallas import tpu as pltpu
 from jax.sharding import PartitionSpec as P
+
 
 HEADS = 32
 KV_HEADS = 16
@@ -69,6 +72,156 @@
     return lax.all_to_all(
         value, axis, split_axis=0, concat_axis=0, tiled=True, axis_index_groups=groups
     )
+
+
+def expert_kernel(
+    serves,
+    gathered,
+    own,
+    gain,
+    gate_own,
+    up_own,
+    down_own,
+    gate_one,
+    up_one,
+    down_one,
+    gate_two,
+    up_two,
+    down_two,
+    out,
+    gate,
+    up,
+    down,
+    normed,
+    sems,
+):
+    half = gate_own.shape[0]
+    width = gate_own.shape[1]
+    pairs, rows, piece = gathered.shape
+    members = out.shape[0]
+    each = rows // members
+    tiles = width // 128
+    lower = [
+        pltpu.make_async_copy(source, target.at[pl.ds(0, half)], sems.at[i])
+        for i, (source, target) in enumerate(((gate_one, gate), (up_one, up), (down_one, down)))
+    ]
+    for copy in lower:
+        copy.start()
+
+    def upper(sources):
+        return [
+            pltpu.make_async_copy(source, target.at[pl.ds(half, half)], sems.at[3 + i])
+            for i, (source, target) in enumerate(zip(sources, (gate, up, down)))
+        ]
+
+    @pl.when(serves[0] == 1)
+    def _():
+        for copy in upper((gate_own, up_own, down_own)):
+            copy.start()
+
+    @pl.when(serves[0] != 1)
+    def _():
+        for copy in upper((gate_two, up_two, down_two)):
+            copy.start()
+
+    total = jnp.zeros((rows, 1), jnp.float32)
+    for k in range(pairs):
+        part = gathered[k].astype(jnp.float32)
+        total = total + jnp.sum(part * part, axis=-1, keepdims=True)
+    inverse = lax.rsqrt(total * (1.0 / width) + EPS)
+    for k in range(pairs):
+        part = gathered[k].astype(jnp.float32)
+        scaled = part * inverse * gain[:, k * piece : (k + 1) * piece]
+        normed[:, k * piece : (k + 1) * piece] = scaled.astype(jnp.bfloat16)
+    for t in range(members):
+        out[t, each * tiles :, :] = own[t * 16 : (t + 1) * 16, :]
+    others = upper((gate_two, up_two, down_two))
+    for copy in (lower[0], others[0], lower[1], others[1]):
+        copy.wait()
+    contract = (((1,), (1,)), ((), ()))
+    hidden = []
+    for start, size in ((0, 256), (256, 256), (512, 128)):
+        g = lax.dot_general(
+            normed[...], gate[pl.ds(start, size), :], contract, preferred_element_type=jnp.float32
+        )
+        u = lax.dot_general(
+            normed[...], up[pl.ds(start, size), :], contract, preferred_element_type=jnp.float32
+        )
+        hidden.append((g / (1.0 + jnp.exp(-g)) * u).astype(jnp.bfloat16))
+    hidden = jnp.concatenate(hidden, axis=1)
+    lower[2].wait()
+    others[2].wait()
+    for chunk in range(width // 256):
+        share = jnp.dot(
+            hidden, down[:, pl.ds(chunk * 256, 256)], preferred_element_type=jnp.float32
+        ).astype(jnp.bfloat16)
+        for t in range(members):
+            for side in range(2):
+                tile = chunk * 2 + side
+                out[t, tile * each : (tile + 1) * each, :] = share[
+                    t * each : (t + 1) * each, side * 128 : (side + 1) * 128
+                ]
+
+
+def run_expert(serves, gathered, own, norm_gain, owned, first, second):
+    pairs, rows, _ = gathered.shape
+    half, width = owned[0].shape
+    members = 2 * pairs
+    vmem = pl.BlockSpec(memory_space=pltpu.VMEM)
+    anywhere = pl.BlockSpec(memory_space=pl.ANY)
+    return pl.pallas_call(
+        expert_kernel,
+        out_shape=jax.ShapeDtypeStruct(
+            (members, rows // members * (width // 128) + 16, 128), jnp.bfloat16
+        ),
+        in_specs=[pl.BlockSpec(memory_space=pltpu.SMEM), vmem, vmem, vmem] + [anywhere] * 9,
+        out_specs=vmem,
+        scratch_shapes=[pltpu.VMEM((2 * half, width), jnp.bfloat16) for _ in range(3)]
+        + [pltpu.VMEM((rows, width), jnp.bfloat16), pltpu.SemaphoreType.DMA((6,))],
+        cost_estimate=pl.CostEstimate(
+            flops=12 * rows * half * width,
+            bytes_accessed=12 * half * width + 4 * rows * width,
+            transcendentals=2 * rows * half,
+        ),
+        compiler_params=pltpu.CompilerParams(vmem_limit_bytes=28 * 2**20),
+        name="expert",
+    )(serves, gathered, own, norm_gain.reshape(1, -1), *owned, *first, *second)
+
+
+def sum_kernel(shares, out, acc):
+    members, rows, _ = shares.shape
+    planes = out.shape[0]
+    tiles = (rows - 16) // (2 * planes)
+    for side in range(2):
+        for block in range(2):
+            lo, size = block * (rows - 16) // 2, (rows - 16) // 2
+            total = shares[side, pl.ds(lo, size), :].astype(jnp.float32)
+            for k in range(1, members // 2):
+                total = total + shares[2 * k + side, pl.ds(lo, size), :].astype(jnp.float32)
+            acc[pl.ds(lo, size), :] = total
+        for rank in range(2):
+            for plane in range(planes):
+                rows_of = acc[pl.ds(rank * planes + plane, tiles, stride=2 * planes), :]
+                at = (side * 2 + rank) * tiles
+                out[plane, at : at + tiles, :] = rows_of.astype(jnp.bfloat16)
+
+
+def sum_shares(shares, planes):
+    members, rows, lanes = shares.shape
+    tiles = (rows - 16) // (2 * planes)
+    vmem = pl.BlockSpec(memory_space=pltpu.VMEM)
+    return pl.pallas_call(
+        sum_kernel,
+        out_shape=jax.ShapeDtypeStruct((planes, 4 * tiles, lanes), jnp.bfloat16),
+        in_specs=[vmem],
+        out_specs=vmem,
+        scratch_shapes=[pltpu.VMEM((rows - 16, lanes), jnp.float32)],
+        cost_estimate=pl.CostEstimate(
+            flops=members * rows * lanes, bytes_accessed=2 * members * rows * lanes, transcendentals=0
+        ),
+        compiler_params=pltpu.CompilerParams(vmem_limit_bytes=8 * 2**20),
+        name="shares",
+    )(shares)
 
 
 def local(
@@ -95,31 +248,27 @@
     same_core = [[plane * 2 + core for plane in range(planes)] for core in range(2)]
     same_parity = [[pair * 2 + side for pair in range(pairs)] for side in range(2)]
 
-    to_server = []
+    swap_pair = [(t, t ^ 1) for t in range(n_tp)]
+    first_moves, second_moves = [], []
     for plane in range(planes):
         for core in range(2):
             for member in range(n_tp):
                 source = (plane * 2 + core) * n_tp + member
+                across = (plane * 2 + 1 - core) * n_tp + member
                 if member % 2 == core:
-                    to_server.append((source, source))
+                    first_moves.append((source, across))
+                    second_moves.append((source, across))
                 else:
-                    to_server.append((source, (plane * 2 + 1 - core) * n_tp + (member ^ 1)))
-    swap_core = [(s, s ^ 1) for s in range(n_sp)]
-    swap_pair = [(t, t ^ 1) for t in range(n_tp)]
-    gate_up = jnp.concatenate(
-        [
-            gate_weight[0, :, :256],
-            up_weight[0, :, :256],
-            gate_weight[0, :, 256:],
-            up_weight[0, :, 256:],
-        ],
-        axis=1,
-    )
+                    first_moves.append((source, source ^ 1))
+    serves = (lax.axis_index("sp") % 2 == parity).astype(jnp.int32).reshape(1)
+    gate_own, up_own, down_own = gate_weight[0].T, up_weight[0].T, down_weight[0]
     out_other = lax.ppermute(out_weight, "tp", swap_pair)
-    down_one = lax.ppermute(down_weight[0], ("sp", "tp"), to_server)
-    gate_up_one = lax.ppermute(gate_up, ("sp", "tp"), to_server)
-    down_two = lax.ppermute(down_one, "sp", swap_core)
-    gate_up_two = lax.ppermute(gate_up_one, "sp", swap_core)
+    gate_one = lax.ppermute(gate_own, ("sp", "tp"), first_moves)
+    up_one = lax.ppermute(up_own, ("sp", "tp"), first_moves)
+    down_one = lax.ppermute(down_own, ("sp", "tp"), first_moves)
+    gate_two = lax.ppermute(gate_one, ("sp", "tp"), second_moves)
+    up_two = lax.ppermute(up_one, ("sp", "tp"), second_moves)
+    down_two = lax.ppermute(down_one, ("sp", "tp"), second_moves)
 
     expert_ids = routes.reshape(-1)
     onehot = (expert_ids[:, None] == jnp.arange(n_sp, dtype=jnp.int32)[None, :]).astype(jnp.int32)
@@ -171,30 +320,22 @@
     block = dispatched.reshape(planes, n_tp, 2, 2 * cols).transpose(1, 2, 0, 3)
     block = block.reshape(rows, 2 * cols)
     gathered = exchange(jnp.broadcast_to(block, (pairs, *block.shape)), "tp", same_parity)
-    flat = gathered.transpose(1, 0, 2).reshape(rows, width).astype(jnp.float32)
-    inverse = lax.rsqrt(jnp.mean(flat * flat, axis=-1, keepdims=True) + EPS)
-    normed = (flat * inverse * norm_gain).astype(jnp.bfloat16)
-
-    def hidden_of(weights):
-        both = jnp.dot(normed, weights, preferred_element_type=jnp.float32)
-        gate = jnp.concatenate([both[:, :256], both[:, 512:576]], axis=1)
-        upward = jnp.concatenate([both[:, 256:512], both[:, 576:]], axis=1)
-        return (jax.nn.silu(gate) * upward).astype(jnp.bfloat16)
-
-    share = jnp.dot(hidden_of(gate_up_one), down_one, preferred_element_type=jnp.float32)
-    share = share + jnp.dot(hidden_of(gate_up_two), down_two, preferred_element_type=jnp.float32)
-
-    pieces = share.astype(jnp.bfloat16).reshape(n_tp, 2 * planes, n_tp, cols).transpose(0, 2, 1, 3)
-    pieces = pieces.reshape(n_tp, n_tp * 2 * planes, cols)
-    pieces = jnp.concatenate([pieces, own.reshape(n_tp, tok_rows, cols)], axis=1)
+    pieces = run_expert(
+        serves,
+        gathered,
+        own,
+        norm_gain,
+        (gate_own, up_own, down_own),
+        (gate_one, up_one, down_one),
+        (gate_two, up_two, down_two),
+    )
+
     shares = exchange(pieces, "tp")
-    main = shares[:, : n_tp * 2 * planes].astype(jnp.float32)
-    main = main.reshape(pairs, 2, n_tp, 2, planes, cols).sum(axis=0).astype(jnp.bfloat16)
-    own_rows = shares[:, n_tp * 2 * planes :].transpose(1, 0, 2).reshape(tok_rows, width)
-
-    returning = main.transpose(3, 1, 0, 2, 4).reshape(planes, n_tp * 4, cols)
+    own_rows = shares[:, 2 * n_tp * planes :].transpose(1, 0, 2).reshape(tok_rows, width)
+    returning = sum_shares(shares, planes)
+
     returned = exchange(returning, "sp", same_core)
-    returned = returned.reshape(planes, n_tp, 4, cols).transpose(0, 2, 1, 3).reshape(2 * n_sp, width)
+    returned = returned.reshape(planes * 4, width)
     place = (slots[:, :, None] == jnp.arange(2 * n_sp)[None, None, :]).astype(jnp.bfloat16)
     first = jnp.dot(place[:, 0], returned, preferred_element_type=jnp.float32)
     second = jnp.dot(place[:, 1], returned, preferred_element_type=jnp.float32)
@@ -219,4 +360,5 @@
         P("sp", "tp", None),
     )
     out_specs = P(("sp", "tp"), None)
+
     return jax.shard_map(local, mesh=mesh, in_specs=in_specs, out_specs=out_specs, check_vma=False)

time: 212 us -> 215 us (1.014)
  waiting for transfers between devices: 17.5 us -> 77.8 us
  blocking collectives: 68 us -> 43.5 us
  starting transfers between devices: 86 us -> 64.7 us
  matrix products: 16 us -> 4.48 us
  Pallas kernels: 0 us -> 9.13 us
  other arithmetic: 7.76 us -> 3.54 us
  local copies, waits for them, and re-layouts: 13.7 us -> 10.6 us
    ppermute x4 -> x6, starting transfers between devices: 56.9 us -> 14.1 us  [the longest x1 2.49 us: local(): down_one = lax.ppermute(down_own, ('sp', 'tp'), first_moves)]
    all_to_all x3 -> x4, waiting for transfers between devices: 17.5 us -> 46.6 us  [exchange(): lax.all_to_all(value, axis, split_axis=0, concat_axis=0, tiled=True, axis...]
    ppermute x4 -> x6, waiting for transfers between devices: 0.01 us -> 28.5 us  [the longest x1 18.4 us: local(): down_one = lax.ppermute(down_own, ('sp', 'tp'), first_moves)]
    all_to_all x2 -> x1, blocking collectives: 68 us -> 43.5 us  [exchange(): lax.all_to_all(value, axis, split_axis=0, concat_axis=0, tiled=True, axis...]
    all_to_all x3 -> x4, starting transfers between devices: 20.1 us -> 41.2 us  [exchange(): lax.all_to_all(value, axis, split_axis=0, concat_axis=0, tiled=True, axis...]
    dot_general x4 -> x0, matrix products: 11.1 us -> none  [the longest x2 7.24 us: hidden_of(): both = jnp.dot(normed, weights, preferred_element_type=jnp.float32)]
    pallas_call x0 -> x2, Pallas kernels: none -> 9.13 us  [the longest x1 7.84 us: run_expert(): pl.pallas_call(expert_kernel, out_shape=jax.ShapeDtypeStruct((members, ro...]
    squeeze x2 -> x0, local copies, waits for them, and re-layouts: 2.78 us -> none  [the longest x1 1.71 us: local(): up_weight[0, :, :256]]
  transfers between devices with their start and end apart: 10 -> 13, of which waited for: 1 -> 7; matrix products, arithmetic and copies ran while one was open for 13% -> 4% of each run, Pallas kernels for 0% -> 0%
where the time goes in v2:
time: 215 us; the launch traced here: 214 us
  waiting for transfers between devices  77.8 us (36%)
  starting transfers between devices  64.7 us (30%)
  blocking collectives  43.5 us (20%)
  local copies, waits for them, and re-layouts  10.6 us (5%)
  Pallas kernels  9.13 us (4%)
  matrix products  4.48 us (2%)
  other arithmetic  3.54 us (2%)
    all_to_all x4, waiting for transfers between devices, exchange(): lax.all_to_all(value, axis, split_axis=0, concat_axis=0, tiled=True, axis...  46.6 us
    all_to_all x1, blocking collectives, exchange(): lax.all_to_all(value, axis, split_axis=0, concat_axis=0, tiled=True, axis...  43.5 us
    all_to_all x4, starting transfers between devices, exchange(): lax.all_to_all(value, axis, split_axis=0, concat_axis=0, tiled=True, axis...  41.2 us
    ppermute x1, waiting for transfers between devices, local(): down_one = lax.ppermute(down_own, ('sp', 'tp'), first_moves)  18.4 us
    ppermute x1, waiting for transfers between devices, local(): up_one = lax.ppermute(up_own, ('sp', 'tp'), first_moves)  8.24 us
    pallas_call x1, Pallas kernels, run_expert(): pl.pallas_call(expert_kernel, out_shape=jax.ShapeDtypeStruct((members, ro...  7.84 us
  transfers between devices with their start and end apart: 13, of which 7 were waited for; matrix products, arithmetic and copies ran while one was open for 4% of the time, Pallas kernels for 0%

profile of v2, /device:TPU:32, one launch (start us, length us, event | category | flops | bytes accessed | tf_op | source)
XLA Modules:
  0.0 214.2 jit_solution(1195108580180633058)
XLA Ops:
  0.0 0.9 copy.87
  0.9 0.9 copy.88
  1.8 0.1 fusion.13
  1.9 1.9 collective-permute-start
  3.8 3.6 %collective-permute-start.1 = (bf16[128,128]{1,0:T(8,128)(2,1)S(1)}, bf16[128,128]{1,0:T(8,128)(2,1)S(1)}, u32[]{:S(2)}, u32[]{:S(2)}) collective-permute-start(bf16[128,128]{1,0:T(8,128)(2,1)S(1)} %get-tuple-element.13), channel_id=1, source_target_pairs={{16,0},{32,16},{48,32},{64,48},{80,64},{96,80},{112,96},{128,112},... | collective-permute-start | bytes 98312 | tf_op jit(solution)/shard_map/ppermute | solution.py:23
  7.5 0.1 compare_and_fusion
  7.6 0.8 copy.98
  8.4 0.1 eq.69
  8.6 0.2 select_reduce_fusion
  8.8 0.1 reduce_sum.22
  8.9 0.1 copy.99
  8.9 0.2 broadcast_and_fusion.1
  9.1 0.7 fusion.16
  9.8 0.9 reshape.285
  10.8 0.1 copy.120
  10.9 0.9 reshape.268
  11.8 0.1 pad_maximum_fusion.4
  11.9 0.1 copy.89
  12.1 0.1 copy.90
  12.2 0.1 copy.91
  12.4 0.3 fusion.17
  12.8 0.1 fusion.6
  12.9 0.1 exponential_add_fusion
  13.0 0.3 fusion.5
  13.3 0.1 copy.117
  13.4 0.1 reshape.286
  13.5 0.2 broadcast_in_dim.22
  13.8 1.2 pad_maximum_fusion
  14.9 7.2 %all-to-all-start = ((bf16[16,304,128]{2,1,0:T(8,128)(2,1)}), bf16[16,304,128]{2,1,0:T(8,128)(2,1)S(1)}, u32[]{:S(2)}, u32[]{:S(2)}) async-start(bf16[16,304,128]{2,1,0:T(8,128)(2,1)} %pad_maximum_fusion), calls=%async_computation | async-start | bytes 2490368 | tf_op jit(solution)/shard_map/all_to_all | solution.py:72
  22.1 3.8 %collective-permute-start.2 = (bf16[2048,128]{1,0:T(8,128)(2,1)S(1)}, bf16[2048,128]{1,0:T(8,128)(2,1)}, u32[]{:S(2)}, u32[]{:S(2)}) collective-permute-start(bf16[2048,128]{1,0:T(8,128)(2,1)S(1)} %copy-done.2), channel_id=1, source_target_pairs={{0,1},{1,0},{2,3},{3,2},{4,5},{5,4},{6,7},{7,6},{8,9},{9,8},{10,11... | collective-permute-start | bytes 1572872 | tf_op jit(solution)/shard_map/ppermute | solution.py:265
  26.0 17.9 %all-to-all-done = bf16[16,304,128]{2,1,0:T(8,128)(2,1)S(1)} async-done(((bf16[16,304,128]{2,1,0:T(8,128)(2,1)}), bf16[16,304,128]{2,1,0:T(8,128)(2,1)S(1)}, u32[]{:S(2)}, u32[]{:S(2)}) %all-to-all-start) | async-done | bytes 1245216 | tf_op jit(solution)/shard_map/all_to_all | solution.py:72
  43.9 1.1 slice_bitcast_fusion
  45.0 1.5 copy.103
  46.5 0.5 convolution_convert_fusion.2.own
  47.0 2.7 %collective-permute-done.2 = bf16[2048,128]{1,0:T(8,128)(2,1)} collective-permute-done((bf16[2048,128]{1,0:T(8,128)(2,1)S(1)}, bf16[2048,128]{1,0:T(8,128)(2,1)}, u32[]{:S(2)}, u32[]{:S(2)}) %collective-permute-start.2) | collective-permute-done | bytes 524320 | tf_op jit(solution)/shard_map/ppermute | solution.py:265
  49.7 1.5 broadcast_select_fusion.1
  51.3 0.1 reshape.280
  51.5 0.1 copy.107
  51.7 0.1 compare_reduce_fusion
  51.8 0.3 broadcast_and_fusion
  52.1 0.3 and.82
  52.4 0.9 convolution_convert_fusion
  53.4 14.1 %all-to-all-start.1 = ((bf16[16,32,256]{2,1,0:T(8,128)(2,1)}), bf16[16,32,256]{2,1,0:T(8,128)(2,1)S(1)}, u32[]{:S(2)}, u32[]{:S(2)}) async-start(bf16[16,32,256]{2,1,0:T(8,128)(2,1)} %bitcast.21), calls=%async_computation.1 | async-start | bytes 524288 | tf_op jit(solution)/shard_map/all_to_all | solution.py:72
  67.5 1.9 collective-permute-start.3
  69.5 2.4 %collective-permute-start.4 = (bf16[320,2048]{1,0:T(8,128)(2,1)}, bf16[320,2048]{1,0:T(8,128)(2,1)}, u32[]{:S(2)}, u32[]{:S(2)}) collective-permute-start(bf16[320,2048]{1,0:T(8,128)(2,1)} %bitcast.29.up_own), channel_id=1, source_target_pairs={{0,16},{1,0},{2,18},{3,2},{4,20},{5,4},{6,22},{7,6},{8,24},{9,8},{... | collective-permute-start | bytes 3932168 | tf_op jit(solution)/shard_map/ppermute | solution.py:267
  71.9 2.5 %collective-permute-start.5 = (bf16[320,2048]{1,0:T(8,128)(2,1)}, bf16[320,2048]{1,0:T(8,128)(2,1)}, u32[]{:S(2)}, u32[]{:S(2)}) collective-permute-start(bf16[320,2048]{1,0:T(8,128)(2,1)} %bitcast.30.down_own), channel_id=1, source_target_pairs={{0,16},{1,0},{2,18},{3,2},{4,20},{5,4},{6,22},{7,6},{8,24},{9,8},{... | collective-permute-start | bytes 3932168 | tf_op jit(solution)/shard_map/ppermute | solution.py:268
  74.4 11.2 %all-to-all-done.1 = bf16[16,32,256]{2,1,0:T(8,128)(2,1)S(1)} async-done(((bf16[16,32,256]{2,1,0:T(8,128)(2,1)}), bf16[16,32,256]{2,1,0:T(8,128)(2,1)S(1)}, u32[]{:S(2)}, u32[]{:S(2)}) %all-to-all-start.1) | async-done | bytes 262176 | tf_op jit(solution)/shard_map/all_to_all | solution.py:72
  85.6 0.1 copy.118
  85.7 1.5 broadcast_in_dim.25
  87.2 7.8 %all-to-all-start.2 = ((bf16[8,512,256]{2,1,0:T(8,128)(2,1)}), bf16[8,512,256]{2,1,0:T(8,128)(2,1)S(1)}, u32[]{:S(2)}, u32[]{:S(2)}) async-start(bf16[8,512,256]{2,1,0:T(8,128)(2,1)} %broadcast_in_dim.25), calls=%async_computation.2 | async-start | bytes 4194304 | tf_op jit(solution)/shard_map/all_to_all | solution.py:72
  95.0 2.4 %collective-permute-start.6 = (bf16[320,2048]{1,0:T(8,128)(2,1)}, bf16[320,2048]{1,0:T(8,128)(2,1)}, u32[]{:S(2)}, u32[]{:S(2)}) collective-permute-start(bf16[320,2048]{1,0:T(8,128)(2,1)} %collective-permute-done.3.gate_one), channel_id=1, source_target_pairs={{0,16},{2,18},{4,20},{6,22},{8,24},{10,26},{12,28},{14,30},{17,1},... | collective-permute-start | bytes 3932168 | tf_op jit(solution)/shard_map/ppermute | solution.py:269
  97.4 8.2 %collective-permute-done.4.up_one = bf16[320,2048]{1,0:T(8,128)(2,1)} collective-permute-done((bf16[320,2048]{1,0:T(8,128)(2,1)}, bf16[320,2048]{1,0:T(8,128)(2,1)}, u32[]{:S(2)}, u32[]{:S(2)}) %collective-permute-start.4) | collective-permute-done | bytes 1310752 | tf_op jit(solution)/shard_map/ppermute | solution.py:267
  105.6 2.4 %collective-permute-start.7 = (bf16[320,2048]{1,0:T(8,128)(2,1)}, bf16[320,2048]{1,0:T(8,128)(2,1)}, u32[]{:S(2)}, u32[]{:S(2)}) collective-permute-start(bf16[320,2048]{1,0:T(8,128)(2,1)} %collective-permute-done.4.up_one), channel_id=1, source_target_pairs={{0,16},{2,18},{4,20},{6,22},{8,24},{10,26},{12,28},{14,30},{17,1},... | collective-permute-start | bytes 3932168 | tf_op jit(solution)/shard_map/ppermute | solution.py:270
  108.1 18.4 %collective-permute-done.5.down_one = bf16[320,2048]{1,0:T(8,128)(2,1)} collective-permute-done((bf16[320,2048]{1,0:T(8,128)(2,1)}, bf16[320,2048]{1,0:T(8,128)(2,1)}, u32[]{:S(2)}, u32[]{:S(2)}) %collective-permute-start.5) | collective-permute-done | bytes 1310752 | tf_op jit(solution)/shard_map/ppermute | solution.py:268
  126.5 2.4 %collective-permute-start.8 = (bf16[320,2048]{1,0:T(8,128)(2,1)}, bf16[320,2048]{1,0:T(8,128)(2,1)}, u32[]{:S(2)}, u32[]{:S(2)}) collective-permute-start(bf16[320,2048]{1,0:T(8,128)(2,1)} %collective-permute-done.5.down_one), channel_id=1, source_target_pairs={{0,16},{2,18},{4,20},{6,22},{8,24},{10,26},{12,28},{14,30},{17,1},... | collective-permute-start | bytes 3932168 | tf_op jit(solution)/shard_map/ppermute | solution.py:271
  128.9 1.9 collective-permute-done.8.down_two
  130.7 7.8 %expert.1 = bf16[16,528,128]{2,1,0:T(8,128)(2,1)S(1)} custom-call(s32[1]{0:T(128)} %bitcast.serves, bf16[8,512,256]{2,1,0:T(8,128)(2,1)S(1)} %all-to-all-done.2.gathered, bf16[256,128]{1,0:T(8,128)(2,1)S(1)} %convolution_convert_fusion.2.own, f32[1,2048]{1,0:T(1,128)S(1)} %bitcast.94, bf16[320,2048]{1,0:T(8,128)(2,1)S(1)} %bitcast.93, ...), custom_call_target="tpu_custom_call" | custom-call | flops 4026531840 | bytes 12058624 | tf_op jit(solution)/shard_map/expert/pallas_call | solution.py:172
  138.6 43.5 %all_to_all.25.shares = bf16[16,528,128]{2,1,0:T(8,128)(2,1)S(1)} all-to-all(bf16[16,528,128]{2,1,0:T(8,128)(2,1)S(1)} %expert.1), channel_id=1, replica_groups=mesh['sp'=32,'tp'=16] {'tp'}, dimensions={0} | all-to-all | bytes 4325376 | tf_op jit(solution)/shard_map/all_to_all | solution.py:72
  182.1 1.3 shares.1
  183.4 12.2 %all-to-all-start.4 = ((bf16[16,64,128]{2,1,0:T(8,128)(2,1)}), bf16[16,64,128]{2,1,0:T(8,128)(2,1)S(1)}, u32[]{:S(2)}, u32[]{:S(2)}) async-start(bf16[16,64,128]{2,1,0:T(8,128)(2,1)} %shares.1), calls=%async_computation.4 | async-start | bytes 524288 | tf_op jit(solution)/shard_map/all_to_all | solution.py:72
  195.6 17.5 %all-to-all-done.4 = bf16[16,64,128]{2,1,0:T(8,128)(2,1)S(1)} async-done(((bf16[16,64,128]{2,1,0:T(8,128)(2,1)}), bf16[16,64,128]{2,1,0:T(8,128)(2,1)S(1)}, u32[]{:S(2)}, u32[]{:S(2)}) %all-to-all-start.4) | async-done | bytes 262176 | tf_op jit(solution)/shard_map/all_to_all | solution.py:72
  213.1 0.1 reshape.276
  213.2 0.2 convolution_multiply_fusion.1
  213.4 0.8 fusion.2
  (42 shorter events, 0.7 us)
Async XLA Ops:
  1.9 9.9 %collective-permute-start = (bf16[128,128]{1,0:T(8,128)(2,1)S(1)}, bf16[128,128]{1,0:T(8,128)(2,1)S(1)}, u32[]{:S(2)}, u32[]{:S(2)}) collective-permute-start(bf16[128,128]{1,0:T(8,128)(2,1)S(1)} %get-tuple-element.12), channel_id=1, source_target_pairs={{0,16},{16,32},{32,48},{48,64},{64,80},{80,96},{96,112},{112,128},... | collective-permute-start | bytes 98312 | tf_op jit(solution)/shard_map/ppermute | solution.py:22
  3.8 8.0 %collective-permute-start.1 = (bf16[128,128]{1,0:T(8,128)(2,1)S(1)}, bf16[128,128]{1,0:T(8,128)(2,1)S(1)}, u32[]{:S(2)}, u32[]{:S(2)}) collective-permute-start(bf16[128,128]{1,0:T(8,128)(2,1)S(1)} %get-tuple-element.13), channel_id=1, source_target_pairs={{16,0},{32,16},{48,32},{64,48},{80,64},{96,80},{112,96},{128,112},... | collective-permute-start | bytes 98312 | tf_op jit(solution)/shard_map/ppermute | solution.py:23
  10.9 1.8 copy-start.4
  14.9 7.2 %copy-start.2 = (bf16[2048,128]{1,0:T(8,128)(2,1)S(1)}, bf16[2048,128]{1,0:T(8,128)(2,1)}, u32[]{:S(2)}) copy-start(bf16[2048,128]{1,0:T(8,128)(2,1)} %param.16) | copy-start | bytes 1572868
  14.9 29.0 %all-to-all-start = ((bf16[16,304,128]{2,1,0:T(8,128)(2,1)}), bf16[16,304,128]{2,1,0:T(8,128)(2,1)S(1)}, u32[]{:S(2)}, u32[]{:S(2)}) async-start(bf16[16,304,128]{2,1,0:T(8,128)(2,1)} %pad_maximum_fusion), calls=%async_computation | async-start | bytes 2490368 | tf_op jit(solution)/shard_map/all_to_all | solution.py:72
  22.1 27.6 %collective-permute-start.2 = (bf16[2048,128]{1,0:T(8,128)(2,1)S(1)}, bf16[2048,128]{1,0:T(8,128)(2,1)}, u32[]{:S(2)}, u32[]{:S(2)}) collective-permute-start(bf16[2048,128]{1,0:T(8,128)(2,1)S(1)} %copy-done.2), channel_id=1, source_target_pairs={{0,1},{1,0},{2,3},{3,2},{4,5},{5,4},{6,7},{7,6},{8,9},{9,8},{10,11... | collective-permute-start | bytes 1572872 | tf_op jit(solution)/shard_map/ppermute | solution.py:265
  51.5 16.1 %copy-start = (bf16[1,2048,320]{1,2,0:T(8,128)(2,1)S(1)}, bf16[1,2048,320]{1,2,0:T(8,128)(2,1)}, u32[]{:S(2)}) copy-start(bf16[1,2048,320]{1,2,0:T(8,128)(2,1)} %param.21) | copy-start | bytes 3932164
  53.4 32.2 %all-to-all-start.1 = ((bf16[16,32,256]{2,1,0:T(8,128)(2,1)}), bf16[16,32,256]{2,1,0:T(8,128)(2,1)S(1)}, u32[]{:S(2)}, u32[]{:S(2)}) async-start(bf16[16,32,256]{2,1,0:T(8,128)(2,1)} %bitcast.21), calls=%async_computation.1 | async-start | bytes 524288 | tf_op jit(solution)/shard_map/all_to_all | solution.py:72
  67.5 27.5 %collective-permute-start.3 = (bf16[320,2048]{1,0:T(8,128)(2,1)S(1)}, bf16[320,2048]{1,0:T(8,128)(2,1)}, u32[]{:S(2)}, u32[]{:S(2)}) collective-permute-start(bf16[320,2048]{1,0:T(8,128)(2,1)S(1)} %bitcast.92), channel_id=1, source_target_pairs={{0,16},{1,0},{2,18},{3,2},{4,20},{5,4},{6,22},{7,6},{8,24},{9,8},{... | collective-permute-start | bytes 3932168 | tf_op jit(solution)/shard_map/ppermute | solution.py:266
  69.5 36.2 %collective-permute-start.4 = (bf16[320,2048]{1,0:T(8,128)(2,1)}, bf16[320,2048]{1,0:T(8,128)(2,1)}, u32[]{:S(2)}, u32[]{:S(2)}) collective-permute-start(bf16[320,2048]{1,0:T(8,128)(2,1)} %bitcast.29.up_own), channel_id=1, source_target_pairs={{0,16},{1,0},{2,18},{3,2},{4,20},{5,4},{6,22},{7,6},{8,24},{9,8},{... | collective-permute-start | bytes 3932168 | tf_op jit(solution)/shard_map/ppermute | solution.py:267
  71.9 54.6 %collective-permute-start.5 = (bf16[320,2048]{1,0:T(8,128)(2,1)}, bf16[320,2048]{1,0:T(8,128)(2,1)}, u32[]{:S(2)}, u32[]{:S(2)}) collective-permute-start(bf16[320,2048]{1,0:T(8,128)(2,1)} %bitcast.30.down_own), channel_id=1, source_target_pairs={{0,16},{1,0},{2,18},{3,2},{4,20},{5,4},{6,22},{7,6},{8,24},{9,8},{... | collective-permute-start | bytes 3932168 | tf_op jit(solution)/shard_map/ppermute | solution.py:268
  87.2 43.5 %copy-start.1 = (f32[2048]{0:T(1024)S(1)}, f32[2048]{0:T(1024)}, u32[]{:S(2)}) copy-start(f32[2048]{0:T(1024)} %param.18) | copy-start | bytes 24580
  87.2 43.5 %all-to-all-start.2 = ((bf16[8,512,256]{2,1,0:T(8,128)(2,1)}), bf16[8,512,256]{2,1,0:T(8,128)(2,1)S(1)}, u32[]{:S(2)}, u32[]{:S(2)}) async-start(bf16[8,512,256]{2,1,0:T(8,128)(2,1)} %broadcast_in_dim.25), calls=%async_computation.2 | async-start | bytes 4194304 | tf_op jit(solution)/shard_map/all_to_all | solution.py:72
  95.0 33.9 %collective-permute-start.6 = (bf16[320,2048]{1,0:T(8,128)(2,1)}, bf16[320,2048]{1,0:T(8,128)(2,1)}, u32[]{:S(2)}, u32[]{:S(2)}) collective-permute-start(bf16[320,2048]{1,0:T(8,128)(2,1)} %collective-permute-done.3.gate_one), channel_id=1, source_target_pairs={{0,16},{2,18},{4,20},{6,22},{8,24},{10,26},{12,28},{14,30},{17,1},... | collective-permute-start | bytes 3932168 | tf_op jit(solution)/shard_map/ppermute | solution.py:269
  105.6 23.2 %collective-permute-start.7 = (bf16[320,2048]{1,0:T(8,128)(2,1)}, bf16[320,2048]{1,0:T(8,128)(2,1)}, u32[]{:S(2)}, u32[]{:S(2)}) collective-permute-start(bf16[320,2048]{1,0:T(8,128)(2,1)} %collective-permute-done.4.up_one), channel_id=1, source_target_pairs={{0,16},{2,18},{4,20},{6,22},{8,24},{10,26},{12,28},{14,30},{17,1},... | collective-permute-start | bytes 3932168 | tf_op jit(solution)/shard_map/ppermute | solution.py:270
  126.5 4.3 %collective-permute-start.8 = (bf16[320,2048]{1,0:T(8,128)(2,1)}, bf16[320,2048]{1,0:T(8,128)(2,1)}, u32[]{:S(2)}, u32[]{:S(2)}) collective-permute-start(bf16[320,2048]{1,0:T(8,128)(2,1)} %collective-permute-done.5.down_one), channel_id=1, source_target_pairs={{0,16},{2,18},{4,20},{6,22},{8,24},{10,26},{12,28},{14,30},{17,1},... | collective-permute-start | bytes 3932168 | tf_op jit(solution)/shard_map/ppermute | solution.py:271
  182.1 13.5 %copy-start.5 = (f32[16,2]{0,1:T(2,128)S(1)}, f32[16,2]{0,1:T(2,128)}, u32[]{:S(2)}) copy-start(f32[16,2]{0,1:T(2,128)} %param.20) | copy-start | bytes 388
  183.4 30.0 %copy-start.3 = (bf16[16,2048]{1,0:T(8,128)(2,1)S(1)}, bf16[16,2048]{1,0:T(8,128)(2,1)}, u32[]{:S(2)}) copy-start(bf16[16,2048]{1,0:T(8,128)(2,1)} %param.17) | copy-start | bytes 196612
  183.4 29.8 %all-to-all-start.4 = ((bf16[16,64,128]{2,1,0:T(8,128)(2,1)}), bf16[16,64,128]{2,1,0:T(8,128)(2,1)S(1)}, u32[]{:S(2)}, u32[]{:S(2)}) async-start(bf16[16,64,128]{2,1,0:T(8,128)(2,1)} %shares.1), calls=%async_computation.4 | async-start | bytes 524288 | tf_op jit(solution)/shard_map/all_to_all | solution.py:72

commit v3 on v2

--- a/solution.py
+++ b/solution.py
@@ -6,8 +6,6 @@
 from jax.sharding import PartitionSpec as P
 
 
-HEADS = 32
-KV_HEADS = 16
 HEAD = 64
 WINDOW = 128
 
@@ -15,57 +13,150 @@
 NEGATIVE = -1e30
 
 
-def halo(block, width):
-    count = lax.axis_size("sp")
-    forward = [(i, i + 1) for i in range(count - 1)]
-    backward = [(target, source) for source, target in forward]
-    low = lax.ppermute(block[-width:], "sp", forward)
-    high = lax.ppermute(block[:width], "sp", backward)
-    return jnp.concatenate([low, block, high], axis=0)
-
-
-def make_band(extended, length):
-    blocks = length // WINDOW
-    pieces = [
-        lax.slice_in_dim(extended, offset * WINDOW, offset * WINDOW + length, axis=0).reshape(
-            blocks, WINDOW, -1
+VMEM = pl.BlockSpec(memory_space=pltpu.VMEM)
+SMEM = pl.BlockSpec(memory_space=pltpu.SMEM)
+ANYWHERE = pl.BlockSpec(memory_space=pl.ANY)
+
+
+def attend_kernel(place, sink, queries, low, own, high, residual, slots, out):
+    members = out.shape[0]
+    length, both = queries.shape
+    tok_rows = residual.shape[0]
+    total = place[1] * length
+    band = jnp.concatenate([low[...], own[...], high[...]], axis=1)
+    row = lax.broadcasted_iota(jnp.int32, (WINDOW, 3 * WINDOW), 0)
+    col = lax.broadcasted_iota(jnp.int32, (WINDOW, 3 * WINDOW), 1)
+    near = jnp.abs(row + WINDOW - col) <= WINDOW
+    for block in range(length // WINDOW):
+        position = place[0] * length + (block - 1) * WINDOW + col
+        valid = near & (position >= 0) & (position < total)
+        keys = band[:HEAD, block * WINDOW : (block + 3) * WINDOW]
+        values = band[HEAD:, block * WINDOW : (block + 3) * WINDOW]
+        heads = []
+        for head in range(both // HEAD):
+            asked = queries[block * WINDOW : (block + 1) * WINDOW, head * HEAD : (head + 1) * HEAD]
+            scores = jnp.dot(asked, keys, preferred_element_type=jnp.float32) * HEAD ** (-0.5)
+            masked = jnp.where(valid, scores, NEGATIVE)
+            top = jnp.maximum(jnp.max(masked, axis=-1, keepdims=True), sink[head])
+            probs = jnp.exp(masked - top)
+            denom = jnp.sum(probs, axis=-1, keepdims=True) + jnp.exp(sink[head] - top)
+            weights = (probs / denom).astype(jnp.bfloat16)
+            heads.append(
+                lax.dot_general(
+                    weights, values, (((1,), (1,)), ((), ())), preferred_element_type=jnp.float32
+                )
+            )
+        attended = jnp.concatenate(heads, axis=1).astype(jnp.bfloat16)
+        for t in range(members):
+            out[t, block * WINDOW : (block + 1) * WINDOW, :] = attended
+    for t in range(members):
+        out[t, length : length + tok_rows, :] = residual[:, t * 128 : (t + 1) * 128]
+        out[t, length + tok_rows :, :] = slots[...]
+
+
+def run_attention(place, sink, queries, low, own, high, residual, slots, members):
+    length, both = queries.shape
+    tok_rows = residual.shape[0]
+    return pl.pallas_call(
+        attend_kernel,
+        out_shape=jax.ShapeDtypeStruct((members, length + 2 * tok_rows, 128), jnp.bfloat16),
+        in_specs=[SMEM, SMEM] + [VMEM] * 6,
+        out_specs=VMEM,
+        cost_estimate=pl.CostEstimate(
+            flops=4 * length * both * 3 * WINDOW,
+            bytes_accessed=4 * members * length * 128,
+            transcendentals=6 * length * WINDOW,
+        ),
+        compiler_params=pltpu.CompilerParams(vmem_limit_bytes=10 * 2**20),
+        name="attend",
+    )(place, sink, queries, low, own, high, residual, slots)
+
+
+def project_kernel(arrived, weight, projected, sending):
+    members = arrived.shape[0]
+    length = projected.shape[0]
+    tok_rows = length // members
+    planes, per_plane, lanes = sending.shape
+    total = jnp.zeros((length, lanes), jnp.float32)
+    for k in range(members // 2):
+        part = jnp.concatenate(
+            [arrived[2 * k, :length, :], arrived[2 * k + 1, :length, :]], axis=1
         )
-        for offset in range(3)
-    ]
-    return jnp.concatenate(pieces, axis=1)
-
-
-def attend_local(queries, keys, values, sink_logit):
-    length = queries.shape[0]
-    groups = keys.shape[1] // HEAD
-    repeat = HEADS // KV_HEADS
-    blocks = length // WINDOW
-    joined = jnp.concatenate([keys, values], axis=1)
-    extended = halo(joined, WINDOW)
-    banded = make_band(extended, length)
-    key_band = banded[..., : groups * HEAD].reshape(blocks, 3 * WINDOW, groups, HEAD)
-    value_band = banded[..., groups * HEAD :].reshape(blocks, 3 * WINDOW, groups, HEAD)
-    query_blocks = queries.reshape(blocks, WINDOW, groups, repeat, HEAD)
-    scores = jnp.einsum(
-        "nqgrd,nkgd->ngrqk", query_blocks, key_band, preferred_element_type=jnp.float32
-    ) * HEAD ** (-0.5)
-    near = jnp.abs(jnp.arange(WINDOW)[:, None] + WINDOW - jnp.arange(3 * WINDOW)[None, :]) <= WINDOW
-    first_token = lax.axis_index("sp") * length
-    key_pos = (
-        first_token + (jnp.arange(blocks)[:, None] - 1) * WINDOW + jnp.arange(3 * WINDOW)[None, :]
+        total = total + jnp.dot(
+            part, weight[k * 256 : (k + 1) * 256, :], preferred_element_type=jnp.float32
+        )
+    rounded = total.astype(jnp.bfloat16)
+    projected[...] = rounded
+    base = jnp.concatenate(
+        [arrived[t, length : length + tok_rows, :] for t in range(members)], axis=0
     )
-    inside = (key_pos >= 0) & (key_pos < length * lax.axis_size("sp"))
-    valid = near[None, None, None, :, :] & inside[:, None, None, None, :]
-    sinks = sink_logit.reshape(1, groups, repeat, 1, 1)
-    masked = jnp.where(valid, scores, NEGATIVE)
-    top = jnp.maximum(jnp.max(masked, axis=-1, keepdims=True), sinks)
-    probs = jnp.exp(masked - top)
-    denom = jnp.sum(probs, axis=-1, keepdims=True) + jnp.exp(sinks - top)
-    weights = (probs / denom).astype(jnp.bfloat16)
-    output = jnp.einsum(
-        "ngrqk,nkgd->nqgrd", weights, value_band, preferred_element_type=jnp.float32
-    )
-    return output.astype(jnp.bfloat16).reshape(length, groups * repeat * HEAD)
+    hidden = (base.astype(jnp.float32) + rounded.astype(jnp.float32)).astype(jnp.bfloat16)
+    slots = jnp.concatenate([arrived[t, length + tok_rows :, :] for t in range(members)], axis=0)
+    slots = slots.astype(jnp.float32)
+    lines = planes * per_plane
+    place = lax.broadcasted_iota(jnp.int32, (1, lines), 1)
+    named = place // per_plane * 4 + place // (per_plane // 2) % 2 * 2 + place % 2
+    wanted = (named + place // 2 % members * (4 * planes)).astype(jnp.float32)
+    device = lax.broadcasted_iota(jnp.int32, (length, 1), 0) // tok_rows * (4 * planes)
+    device = device.astype(jnp.float32)
+    taken = (slots[:, 0:1] + device == wanted) | (slots[:, 1:2] + device == wanted)
+    placing = jnp.where(taken, 1.0, 0.0).astype(jnp.bfloat16)
+    rows = lax.dot_general(
+        placing, hidden, (((0,), (0,)), ((), ())), preferred_element_type=jnp.float32
+    ).astype(jnp.bfloat16)
+    for plane in range(planes):
+        sending[plane] = rows[plane * per_plane : (plane + 1) * per_plane, :]
+
+
+def project(arrived, weight, planes, length):
+    members = arrived.shape[0]
+    width, lanes = weight.shape
+    return pl.pallas_call(
+        project_kernel,
+        out_shape=(
+            jax.ShapeDtypeStruct((length, lanes), jnp.bfloat16),
+            jax.ShapeDtypeStruct((planes, 4 * members, lanes), jnp.bfloat16),
+        ),
+        in_specs=[VMEM, VMEM],
+        out_specs=(VMEM, VMEM),
+        cost_estimate=pl.CostEstimate(
+            flops=2 * length * width * lanes,
+            bytes_accessed=4 * width * lanes + 2 * members * length * lanes,
+            transcendentals=0,
+        ),
+        compiler_params=pltpu.CompilerParams(vmem_limit_bytes=12 * 2**20),
+        name="project",
+    )(arrived, weight)
+
+
+def spread_kernel(dispatched, out, rows):
+    planes, lines, _ = dispatched.shape
+    members = out.shape[0]
+    for plane in range(planes):
+        rows[plane * lines : (plane + 1) * lines, :] = dispatched[plane].astype(jnp.float32)
+    for line in range(lines):
+        side, at = line // (lines // 2), line % (lines // 2)
+        group = rows[pl.ds(line, planes, stride=lines), :].astype(jnp.bfloat16)
+        for k in range(members // 2):
+            out[2 * k + side, at * planes : (at + 1) * planes, :] = group
+
+
+def spread(dispatched, members):
+    planes, lines, lanes = dispatched.shape
+    return pl.pallas_call(
+        spread_kernel,
+        out_shape=jax.ShapeDtypeStruct((members, planes * lines // 2, lanes), jnp.bfloat16),
+        in_specs=[VMEM],
+        out_specs=VMEM,
+        scratch_shapes=[pltpu.VMEM((planes * lines, lanes), jnp.float32)],
+        cost_estimate=pl.CostEstimate(
+            flops=planes * lines * lanes,
+            bytes_accessed=members * planes * lines * lanes,
+            transcendentals=0,
+        ),
+        compiler_params=pltpu.CompilerParams(vmem_limit_bytes=8 * 2**20),
+        name="spread",
+    )(dispatched)
 
 
 def exchange(value, axis, groups=None):
@@ -166,16 +257,14 @@
 def run_expert(serves, gathered, own, norm_gain, owned, first, second):
     pairs, rows, _ = gathered.shape
     half, width = owned[0].shape
-    members = 2 * pairs
-    vmem = pl.BlockSpec(memory_space=pltpu.VMEM)
-    anywhere = pl.BlockSpec(memory_space=pl.ANY)
+    members = pairs
     return pl.pallas_call(
         expert_kernel,
         out_shape=jax.ShapeDtypeStruct(
             (members, rows // members * (width // 128) + 16, 128), jnp.bfloat16
         ),
-        in_specs=[pl.BlockSpec(memory_space=pltpu.SMEM), vmem, vmem, vmem] + [anywhere] * 9,
-        out_specs=vmem,
+        in_specs=[SMEM, VMEM, VMEM, VMEM] + [ANYWHERE] * 9,
+        out_specs=VMEM,
         scratch_shapes=[pltpu.VMEM((2 * half, width), jnp.bfloat16) for _ in range(3)]
         + [pltpu.VMEM((rows, width), jnp.bfloat16), pltpu.SemaphoreType.DMA((6,))],
         cost_estimate=pl.CostEstimate(
@@ -209,12 +298,11 @@
 def sum_shares(shares, planes):
     members, rows, lanes = shares.shape
     tiles = (rows - 16) // (2 * planes)
-    vmem = pl.BlockSpec(memory_space=pltpu.VMEM)
     return pl.pallas_call(
         sum_kernel,
         out_shape=jax.ShapeDtypeStruct((planes, 4 * tiles, lanes), jnp.bfloat16),
-        in_specs=[vmem],
-        out_specs=vmem,
+        in_specs=[VMEM],
+        out_specs=VMEM,
         scratch_shapes=[pltpu.VMEM((rows - 16, lanes), jnp.float32)],
         cost_estimate=pl.CostEstimate(
             flops=members * rows * lanes, bytes_accessed=2 * members * rows * lanes, transcendentals=0
@@ -240,15 +328,12 @@
 ):
     n_sp, n_tp = lax.axis_size("sp"), lax.axis_size("tp")
     planes = n_sp // 2
-    pairs = n_tp // 2
     tok_rows, width = residual.shape
     cols = width // n_tp
     length = queries.shape[0]
     parity = lax.axis_index("tp") % 2
     same_core = [[plane * 2 + core for plane in range(planes)] for core in range(2)]
-    same_parity = [[pair * 2 + side for pair in range(pairs)] for side in range(2)]
-
-    swap_pair = [(t, t ^ 1) for t in range(n_tp)]
+
     first_moves, second_moves = [], []
     for plane in range(planes):
         for core in range(2):
@@ -262,7 +347,6 @@
                     first_moves.append((source, source ^ 1))
     serves = (lax.axis_index("sp") % 2 == parity).astype(jnp.int32).reshape(1)
     gate_own, up_own, down_own = gate_weight[0].T, up_weight[0].T, down_weight[0]
-    out_other = lax.ppermute(out_weight, "tp", swap_pair)
     gate_one = lax.ppermute(gate_own, ("sp", "tp"), first_moves)
     up_one = lax.ppermute(up_own, ("sp", "tp"), first_moves)
     down_one = lax.ppermute(down_own, ("sp", "tp"), first_moves)
@@ -271,55 +355,29 @@
     down_two = lax.ppermute(down_one, ("sp", "tp"), second_moves)
 
     expert_ids = routes.reshape(-1)
-    onehot = (expert_ids[:, None] == jnp.arange(n_sp, dtype=jnp.int32)[None, :]).astype(jnp.int32)
-    earlier = jnp.cumsum(onehot, axis=0) - onehot
-    rank = jnp.sum(earlier * onehot, axis=1)
+    count = expert_ids.shape[0]
+    before = jnp.arange(count)[None, :] < jnp.arange(count)[:, None]
+    same = (expert_ids[:, None] == expert_ids[None, :]) & before
+    rank = jnp.sum(same.astype(jnp.int32), axis=1)
     slots = (expert_ids * 2 + rank).reshape(tok_rows, 2)
-
-    attention = attend_local(queries, keys, values, sink_logit)
-
-    residual_pieces = residual.reshape(tok_rows, pairs, 2, cols).transpose(1, 2, 0, 3)
-    residual_pieces = jnp.repeat(residual_pieces.reshape(pairs, 2 * tok_rows, cols), 2, axis=0)
     slot_rows = jnp.pad(slots.astype(jnp.bfloat16), ((0, 0), (0, cols - 2)))
-    message = jnp.concatenate(
-        [
-            jnp.broadcast_to(attention, (n_tp, *attention.shape)),
-            residual_pieces,
-            jnp.broadcast_to(slot_rows, (n_tp, *slot_rows.shape)),
-        ],
-        axis=1,
+
+    joined = jnp.concatenate([keys.T, values.T], axis=0)
+    forward = [(i, i + 1) for i in range(n_sp - 1)]
+    backward = [(i + 1, i) for i in range(n_sp - 1)]
+    low = lax.ppermute(joined[:, length - WINDOW :], "sp", forward)
+    high = lax.ppermute(joined[:, :WINDOW], "sp", backward)
+    where = jnp.stack([lax.axis_index("sp"), jnp.int32(n_sp)]).astype(jnp.int32)
+    message = run_attention(
+        where, sink_logit, queries, low, joined, high, residual, slot_rows, n_tp
     )
+
     arrived = exchange(message, "tp")
-    attended = arrived[:, :length].transpose(1, 0, 2).reshape(length, width)
-    residual_cols = (
-        arrived[:, length : length + 2 * tok_rows]
-        .reshape(n_tp, 2, tok_rows, cols)
-        .transpose(0, 2, 1, 3)
-        .reshape(length, 2 * cols)
-    )
-    slot_all = arrived[:, length + 2 * tok_rows :, :2].reshape(length, 2).astype(jnp.int32)
-
-    own = jnp.dot(attended, out_weight, preferred_element_type=jnp.float32).astype(jnp.bfloat16)
-    other = jnp.dot(attended, out_other, preferred_element_type=jnp.float32).astype(jnp.bfloat16)
-    projected = jnp.concatenate(
-        [jnp.where(parity == 0, own, other), jnp.where(parity == 0, other, own)], axis=1
-    )
-    hidden_cols = (residual_cols.astype(jnp.float32) + projected.astype(jnp.float32)).astype(
-        jnp.bfloat16
-    )
-    wanted = (2 * jnp.arange(planes)[:, None] + parity) * 2 + jnp.arange(2)[None, :]
-    named = jnp.any(slot_all[None, None] == wanted[:, :, None, None], axis=-1)
-    mine = (jnp.arange(length) // tok_rows)[None, :] == jnp.arange(n_tp)[:, None]
-    placing = (named[:, None] & mine[None, :, None]).astype(jnp.bfloat16)
-    sending = jnp.dot(
-        placing.reshape(planes * n_tp * 2, length), hidden_cols, preferred_element_type=jnp.float32
-    ).astype(jnp.bfloat16)
-
-    dispatched = exchange(sending.reshape(planes, n_tp * 2, 2 * cols), "sp", same_core)
-    rows = planes * n_tp * 2
-    block = dispatched.reshape(planes, n_tp, 2, 2 * cols).transpose(1, 2, 0, 3)
-    block = block.reshape(rows, 2 * cols)
-    gathered = exchange(jnp.broadcast_to(block, (pairs, *block.shape)), "tp", same_parity)
+    own, sending = project(arrived, out_weight, planes, length)
+
+    dispatched = exchange(sending, "sp", same_core)
+    to_servers = spread(dispatched, n_tp)
+    gathered = exchange(to_servers, "tp")
     pieces = run_expert(
         serves,
         gathered,

time: 215 us -> 197 us (0.916)
  the two profiles are of different devices: /device:TPU:32 before, /device:TPU:8 now
where the time goes in v3:
time: 197 us; the launch traced here: 196 us
  waiting for transfers between devices  64.2 us (33%)
  blocking collectives  59.6 us (30%)
  starting transfers between devices  50.2 us (25%)
  Pallas kernels  13 us (7%)
  local copies, waits for them, and re-layouts  4.89 us (2%)
  other arithmetic  2.58 us (1%)
    all_to_all x2, blocking collectives, exchange(): lax.all_to_all(value, axis, split_axis=0, concat_axis=0, tiled=True, axis...  59.6 us
    all_to_all x3, waiting for transfers between devices, exchange(): lax.all_to_all(value, axis, split_axis=0, concat_axis=0, tiled=True, axis...  33.1 us
    all_to_all x3, starting transfers between devices, exchange(): lax.all_to_all(value, axis, split_axis=0, concat_axis=0, tiled=True, axis...  32.2 us
    ppermute x1, waiting for transfers between devices, local(): up_one = lax.ppermute(up_own, ('sp', 'tp'), first_moves)  17.6 us
    ppermute x1, waiting for transfers between devices, local(): down_one = lax.ppermute(down_own, ('sp', 'tp'), first_moves)  11.6 us
    pallas_call x1, Pallas kernels, run_expert(): pl.pallas_call(expert_kernel, out_shape=jax.ShapeDtypeStruct((members, ro...  7.84 us
    unnamed x19, local copies, waits for them, and re-layouts  4.44 us
  transfers between devices with their start and end apart: 11, of which 6 were waited for; matrix products, arithmetic and copies ran while one was open for 1% of the time, Pallas kernels for 0%

profile of v3, /device:TPU:8, one launch (start us, length us, event | category | flops | bytes accessed | tf_op | source)
XLA Modules:
  0.0 195.7 jit_solution(4552045319723758522)
XLA Ops:
  0.0 0.8 fusion.4
  0.8 1.3 collective-permute-start.1
  2.1 3.0 %collective-permute-start = (bf16[128,128]{1,0:T(8,128)(2,1)S(1)}, bf16[128,128]{1,0:T(8,128)(2,1)S(1)}, u32[]{:S(2)}, u32[]{:S(2)}) collective-permute-start(bf16[128,128]{1,0:T(8,128)(2,1)S(1)} %get-tuple-element.12), channel_id=1, source_target_pairs={{0,16},{16,32},{32,48},{48,64},{64,80},{80,96},{96,112},{112,128},... | collective-permute-start | bytes 98312 | tf_op jit(solution)/shard_map/ppermute | solution.py:368
  5.1 0.7 broadcast_multiply_fusion
  5.8 0.8 copy.26
  6.5 0.8 pad_maximum_fusion.own
  7.3 0.1 copy.27
  7.4 0.1 eq.35
  7.5 0.2 convert_reduce_fusion
  7.7 0.1 reduce_sum.12
  7.8 0.1 pad_add_fusion.place
  7.9 0.0 collective-permute-done.1.high
  7.9 0.0 collective-permute-done.low
  7.9 0.0 copy-start.3
  7.9 0.8 copy-done.3
  8.7 0.0 copy-start.5
  8.7 0.8 copy-done.5
  9.6 0.0 copy-start.7
  9.6 0.7 copy-done.7
  10.2 2.1 %attend.1 = bf16[16,288,128]{2,1,0:T(8,128)(2,1)S(1)} custom-call(s32[2]{0:T(128)S(1)} %pad_add_fusion.place, f32[2]{0:T(128)S(1)} %copy-done.7, bf16[256,128]{1,0:T(8,128)(2,1)S(1)} %copy-done.5, bf16[128,128]{1,0:T(8,128)(2,1)S(1)} %collective-permute-done.low, bf16[128,256]{1,0:T(8,128)(2,1)S(1)} %pad_maximum_fusion.own, ...), custom_call_target="tpu_custom_call" | custom-call | flops 50331648 | bytes 2097152 | tf_op jit(solution)/shard_map/attend/pallas_call | solution.py:60
  12.3 0.0 copy-start.2
  12.4 25.9 %all_to_all.25.arrived = bf16[16,288,128]{2,1,0:T(8,128)(2,1)S(1)} all-to-all(bf16[16,288,128]{2,1,0:T(8,128)(2,1)S(1)} %attend.1), channel_id=1, replica_groups=mesh['sp'=32,'tp'=16] {'tp'}, dimensions={0} | all-to-all | bytes 2359296 | tf_op jit(solution)/shard_map/all_to_all | solution.py:163
  38.3 0.0 copy-done.2
  38.3 0.0 copy-start.1
  38.3 1.4 project.1
  39.7 14.7 %all-to-all-start.1 = ((bf16[16,64,128]{2,1,0:T(8,128)(2,1)}), bf16[16,64,128]{2,1,0:T(8,128)(2,1)S(1)}, u32[]{:S(2)}, u32[]{:S(2)}) async-start(bf16[16,64,128]{2,1,0:T(8,128)(2,1)} %get-tuple-element.7), calls=%async_computation.1 | async-start | bytes 524288 | tf_op jit(solution)/shard_map/all_to_all | solution.py:163
  54.4 0.0 copy-done.1
  54.4 1.9 collective-permute-start.2
  56.4 1.9 collective-permute-start.3
  58.3 2.7 %collective-permute-start.4 = (bf16[320,2048]{1,0:T(8,128)(2,1)}, bf16[320,2048]{1,0:T(8,128)(2,1)}, u32[]{:S(2)}, u32[]{:S(2)}) collective-permute-start(bf16[320,2048]{1,0:T(8,128)(2,1)} %bitcast.9.down_own), channel_id=1, source_target_pairs={{0,16},{1,0},{2,18},{3,2},{4,20},{5,4},{6,22},{7,6},{8,24},{9,8},{... | collective-permute-start | bytes 3932168 | tf_op jit(solution)/shard_map/ppermute | solution.py:352
  61.0 11.4 %all-to-all-done.1.dispatched = bf16[16,64,128]{2,1,0:T(8,128)(2,1)S(1)} async-done(((bf16[16,64,128]{2,1,0:T(8,128)(2,1)}), bf16[16,64,128]{2,1,0:T(8,128)(2,1)S(1)}, u32[]{:S(2)}, u32[]{:S(2)}) %all-to-all-start.1) | async-done | bytes 262176 | tf_op jit(solution)/shard_map/all_to_all | solution.py:163
  72.3 0.4 spread.1
  72.7 0.0 copy-start
  72.7 1.3 copy-done
  74.1 0.0 copy-start.6
  74.1 5.6 %all-to-all-start.2 = ((bf16[16,512,128]{2,1,0:T(8,128)(2,1)}), bf16[16,512,128]{2,1,0:T(8,128)(2,1)S(1)}, u32[]{:S(2)}, u32[]{:S(2)}) async-start(bf16[16,512,128]{2,1,0:T(8,128)(2,1)} %copy-done), calls=%async_computation.2 | async-start | bytes 4194304 | tf_op jit(solution)/shard_map/all_to_all | solution.py:163
  79.7 0.0 collective-permute-done.2.gate_one
  79.7 2.4 %collective-permute-start.5 = (bf16[320,2048]{1,0:T(8,128)(2,1)}, bf16[320,2048]{1,0:T(8,128)(2,1)}, u32[]{:S(2)}, u32[]{:S(2)}) collective-permute-start(bf16[320,2048]{1,0:T(8,128)(2,1)} %collective-permute-done.2.gate_one), channel_id=1, source_target_pairs={{0,16},{2,18},{4,20},{6,22},{8,24},{10,26},{12,28},{14,30},{17,1},... | collective-permute-start | bytes 3932168 | tf_op jit(solution)/shard_map/ppermute | solution.py:353
  82.1 17.6 %collective-permute-done.3.up_one = bf16[320,2048]{1,0:T(8,128)(2,1)} collective-permute-done((bf16[320,2048]{1,0:T(8,128)(2,1)}, bf16[320,2048]{1,0:T(8,128)(2,1)}, u32[]{:S(2)}, u32[]{:S(2)}) %collective-permute-start.3) | collective-permute-done | bytes 1310752 | tf_op jit(solution)/shard_map/ppermute | solution.py:351
  99.6 2.4 %collective-permute-start.6 = (bf16[320,2048]{1,0:T(8,128)(2,1)}, bf16[320,2048]{1,0:T(8,128)(2,1)}, u32[]{:S(2)}, u32[]{:S(2)}) collective-permute-start(bf16[320,2048]{1,0:T(8,128)(2,1)} %collective-permute-done.3.up_one), channel_id=1, source_target_pairs={{0,16},{2,18},{4,20},{6,22},{8,24},{10,26},{12,28},{14,30},{17,1},... | collective-permute-start | bytes 3932168 | tf_op jit(solution)/shard_map/ppermute | solution.py:354
  102.1 11.6 %collective-permute-done.4.down_one = bf16[320,2048]{1,0:T(8,128)(2,1)} collective-permute-done((bf16[320,2048]{1,0:T(8,128)(2,1)}, bf16[320,2048]{1,0:T(8,128)(2,1)}, u32[]{:S(2)}, u32[]{:S(2)}) %collective-permute-start.4) | collective-permute-done | bytes 1310752 | tf_op jit(solution)/shard_map/ppermute | solution.py:352
  113.7 2.4 %collective-permute-start.7 = (bf16[320,2048]{1,0:T(8,128)(2,1)}, bf16[320,2048]{1,0:T(8,128)(2,1)}, u32[]{:S(2)}, u32[]{:S(2)}) collective-permute-start(bf16[320,2048]{1,0:T(8,128)(2,1)} %collective-permute-done.4.down_one), channel_id=1, source_target_pairs={{0,16},{2,18},{4,20},{6,22},{8,24},{10,26},{12,28},{14,30},{17,1},... | collective-permute-start | bytes 3932168 | tf_op jit(solution)/shard_map/ppermute | solution.py:355
  116.1 0.0 collective-permute-done.5.gate_two
  116.1 0.0 collective-permute-done.6.up_two
  116.1 1.9 collective-permute-done.7.down_two
  118.0 5.5 %all-to-all-done.2.gathered = bf16[16,512,128]{2,1,0:T(8,128)(2,1)S(1)} async-done(((bf16[16,512,128]{2,1,0:T(8,128)(2,1)}), bf16[16,512,128]{2,1,0:T(8,128)(2,1)S(1)}, u32[]{:S(2)}, u32[]{:S(2)}) %all-to-all-start.2) | async-done | bytes 2097184 | tf_op jit(solution)/shard_map/all_to_all | solution.py:163
  123.4 0.0 copy-done.6
  123.4 7.8 %expert.1 = bf16[16,528,128]{2,1,0:T(8,128)(2,1)S(1)} custom-call(s32[1]{0:T(128)} %bitcast.serves, bf16[16,512,128]{2,1,0:T(8,128)(2,1)S(1)} %all-to-all-done.2.gathered, bf16[256,128]{1,0:T(8,128)(2,1)S(1)} %get-tuple-element.8.own, f32[1,2048]{1,0:T(1,128)S(1)} %bitcast.34, bf16[320,2048]{1,0:T(8,128)(2,1)S(1)} %bitcast.33, ...), custom_call_target="tpu_custom_call" | custom-call | flops 4026531840 | bytes 12058624 | tf_op jit(solution)/shard_map/expert/pallas_call | solution.py:261
  131.3 33.7 %all_to_all.26.shares = bf16[16,528,128]{2,1,0:T(8,128)(2,1)S(1)} all-to-all(bf16[16,528,128]{2,1,0:T(8,128)(2,1)S(1)} %expert.1), channel_id=1, replica_groups=mesh['sp'=32,'tp'=16] {'tp'}, dimensions={0} | all-to-all | bytes 4325376 | tf_op jit(solution)/shard_map/all_to_all | solution.py:163
  165.0 0.0 copy-start.8
  165.0 1.3 shares.1
  166.3 0.0 copy-start.4
  166.3 11.9 %all-to-all-start.4 = ((bf16[16,64,128]{2,1,0:T(8,128)(2,1)}), bf16[16,64,128]{2,1,0:T(8,128)(2,1)S(1)}, u32[]{:S(2)}, u32[]{:S(2)}) async-start(bf16[16,64,128]{2,1,0:T(8,128)(2,1)} %shares.1), calls=%async_computation.4 | async-start | bytes 524288 | tf_op jit(solution)/shard_map/all_to_all | solution.py:163
  178.1 0.1 copy.29
  178.2 0.0 copy-done.8
  178.2 0.1 iota_compare_fusion
  178.3 16.3 %all-to-all-done.4 = bf16[16,64,128]{2,1,0:T(8,128)(2,1)S(1)} async-done(((bf16[16,64,128]{2,1,0:T(8,128)(2,1)}), bf16[16,64,128]{2,1,0:T(8,128)(2,1)S(1)}, u32[]{:S(2)}, u32[]{:S(2)}) %all-to-all-start.4) | async-done | bytes 262176 | tf_op jit(solution)/shard_map/all_to_all | solution.py:163
  194.6 0.1 reshape.28
  194.7 0.2 convolution_multiply_fusion.1
  194.9 0.0 copy-done.4
  194.9 0.8 fusion.2
  (3 shorter events, 0.0 us)
Async XLA Ops:
  0.8 7.1 %collective-permute-start.1 = (bf16[128,128]{1,0:T(8,128)(2,1)S(1)}, bf16[128,128]{1,0:T(8,128)(2,1)S(1)}, u32[]{:S(2)}, u32[]{:S(2)}) collective-permute-start(bf16[128,128]{1,0:T(8,128)(2,1)S(1)} %get-tuple-element.11), channel_id=1, source_target_pairs={{16,0},{32,16},{48,32},{64,48},{80,64},{96,80},{112,96},{128,112},... | collective-permute-start | bytes 98312 | tf_op jit(solution)/shard_map/ppermute | solution.py:369
  2.1 5.8 %collective-permute-start = (bf16[128,128]{1,0:T(8,128)(2,1)S(1)}, bf16[128,128]{1,0:T(8,128)(2,1)S(1)}, u32[]{:S(2)}, u32[]{:S(2)}) collective-permute-start(bf16[128,128]{1,0:T(8,128)(2,1)S(1)} %get-tuple-element.12), channel_id=1, source_target_pairs={{0,16},{16,32},{32,48},{48,64},{64,80},{80,96},{96,112},{112,128},... | collective-permute-start | bytes 98312 | tf_op jit(solution)/shard_map/ppermute | solution.py:368
  7.9 0.8 copy-start.3
  8.7 0.8 copy-start.5
  9.6 0.7 copy-start.7
  12.3 25.9 %copy-start.2 = (bf16[2048,128]{1,0:T(8,128)(2,1)S(1)}, bf16[2048,128]{1,0:T(8,128)(2,1)}, u32[]{:S(2)}) copy-start(bf16[2048,128]{1,0:T(8,128)(2,1)} %weight.1) | copy-start | bytes 1572868
  38.3 16.1 %copy-start.1 = (bf16[1,2048,320]{1,2,0:T(8,128)(2,1)S(1)}, bf16[1,2048,320]{1,2,0:T(8,128)(2,1)}, u32[]{:S(2)}) copy-start(bf16[1,2048,320]{1,2,0:T(8,128)(2,1)} %param.21) | copy-start | bytes 3932164
  39.7 32.6 %all-to-all-start.1 = ((bf16[16,64,128]{2,1,0:T(8,128)(2,1)}), bf16[16,64,128]{2,1,0:T(8,128)(2,1)S(1)}, u32[]{:S(2)}, u32[]{:S(2)}) async-start(bf16[16,64,128]{2,1,0:T(8,128)(2,1)} %get-tuple-element.7), calls=%async_computation.1 | async-start | bytes 524288 | tf_op jit(solution)/shard_map/all_to_all | solution.py:163
  54.4 25.3 %collective-permute-start.2 = (bf16[320,2048]{1,0:T(8,128)(2,1)S(1)}, bf16[320,2048]{1,0:T(8,128)(2,1)}, u32[]{:S(2)}, u32[]{:S(2)}) collective-permute-start(bf16[320,2048]{1,0:T(8,128)(2,1)S(1)} %bitcast.32), channel_id=1, source_target_pairs={{0,16},{1,0},{2,18},{3,2},{4,20},{5,4},{6,22},{7,6},{8,24},{9,8},{... | collective-permute-start | bytes 3932168 | tf_op jit(solution)/shard_map/ppermute | solution.py:350
  56.4 43.3 %collective-permute-start.3 = (bf16[320,2048]{1,0:T(8,128)(2,1)}, bf16[320,2048]{1,0:T(8,128)(2,1)}, u32[]{:S(2)}, u32[]{:S(2)}) collective-permute-start(bf16[320,2048]{1,0:T(8,128)(2,1)} %bitcast.8.up_own), channel_id=1, source_target_pairs={{0,16},{1,0},{2,18},{3,2},{4,20},{5,4},{6,22},{7,6},{8,24},{9,8},{... | collective-permute-start | bytes 3932168 | tf_op jit(solution)/shard_map/ppermute | solution.py:351
  58.3 55.4 %collective-permute-start.4 = (bf16[320,2048]{1,0:T(8,128)(2,1)}, bf16[320,2048]{1,0:T(8,128)(2,1)}, u32[]{:S(2)}, u32[]{:S(2)}) collective-permute-start(bf16[320,2048]{1,0:T(8,128)(2,1)} %bitcast.9.down_own), channel_id=1, source_target_pairs={{0,16},{1,0},{2,18},{3,2},{4,20},{5,4},{6,22},{7,6},{8,24},{9,8},{... | collective-permute-start | bytes 3932168 | tf_op jit(solution)/shard_map/ppermute | solution.py:352
  72.7 1.3 copy-start
  74.1 49.3 %copy-start.6 = (f32[2048]{0:T(1024)S(1)}, f32[2048]{0:T(1024)}, u32[]{:S(2)}) copy-start(f32[2048]{0:T(1024)} %param.18) | copy-start | bytes 24580
  74.1 49.3 %all-to-all-start.2 = ((bf16[16,512,128]{2,1,0:T(8,128)(2,1)}), bf16[16,512,128]{2,1,0:T(8,128)(2,1)S(1)}, u32[]{:S(2)}, u32[]{:S(2)}) async-start(bf16[16,512,128]{2,1,0:T(8,128)(2,1)} %copy-done), calls=%async_computation.2 | async-start | bytes 4194304 | tf_op jit(solution)/shard_map/all_to_all | solution.py:163
  79.7 36.3 %collective-permute-start.5 = (bf16[320,2048]{1,0:T(8,128)(2,1)}, bf16[320,2048]{1,0:T(8,128)(2,1)}, u32[]{:S(2)}, u32[]{:S(2)}) collective-permute-start(bf16[320,2048]{1,0:T(8,128)(2,1)} %collective-permute-done.2.gate_one), channel_id=1, source_target_pairs={{0,16},{2,18},{4,20},{6,22},{8,24},{10,26},{12,28},{14,30},{17,1},... | collective-permute-start | bytes 3932168 | tf_op jit(solution)/shard_map/ppermute | solution.py:353
  99.6 16.4 %collective-permute-start.6 = (bf16[320,2048]{1,0:T(8,128)(2,1)}, bf16[320,2048]{1,0:T(8,128)(2,1)}, u32[]{:S(2)}, u32[]{:S(2)}) collective-permute-start(bf16[320,2048]{1,0:T(8,128)(2,1)} %collective-permute-done.3.up_one), channel_id=1, source_target_pairs={{0,16},{2,18},{4,20},{6,22},{8,24},{10,26},{12,28},{14,30},{17,1},... | collective-permute-start | bytes 3932168 | tf_op jit(solution)/shard_map/ppermute | solution.py:354
  113.7 4.3 %collective-permute-start.7 = (bf16[320,2048]{1,0:T(8,128)(2,1)}, bf16[320,2048]{1,0:T(8,128)(2,1)}, u32[]{:S(2)}, u32[]{:S(2)}) collective-permute-start(bf16[320,2048]{1,0:T(8,128)(2,1)} %collective-permute-done.4.down_one), channel_id=1, source_target_pairs={{0,16},{2,18},{4,20},{6,22},{8,24},{10,26},{12,28},{14,30},{17,1},... | collective-permute-start | bytes 3932168 | tf_op jit(solution)/shard_map/ppermute | solution.py:355
  165.0 13.2 %copy-start.8 = (f32[16,2]{0,1:T(2,128)S(1)}, f32[16,2]{0,1:T(2,128)}, u32[]{:S(2)}) copy-start(f32[16,2]{0,1:T(2,128)} %param.20) | copy-start | bytes 388
  166.3 28.6 %copy-start.4 = (bf16[16,2048]{1,0:T(8,128)(2,1)S(1)}, bf16[16,2048]{1,0:T(8,128)(2,1)}, u32[]{:S(2)}) copy-start(bf16[16,2048]{1,0:T(8,128)(2,1)} %residual.1) | copy-start | bytes 196612
  166.3 28.3 %all-to-all-start.4 = ((bf16[16,64,128]{2,1,0:T(8,128)(2,1)}), bf16[16,64,128]{2,1,0:T(8,128)(2,1)S(1)}, u32[]{:S(2)}, u32[]{:S(2)}) async-start(bf16[16,64,128]{2,1,0:T(8,128)(2,1)} %shares.1), calls=%async_computation.4 | async-start | bytes 524288 | tf_op jit(solution)/shard_map/all_to_all | solution.py:163

commit v4 on v3

--- a/solution.py
+++ b/solution.py
@@ -15,7 +15,82 @@
 
 VMEM = pl.BlockSpec(memory_space=pltpu.VMEM)
 SMEM = pl.BlockSpec(memory_space=pltpu.SMEM)
-ANYWHERE = pl.BlockSpec(memory_space=pl.ANY)
+ANYWHERE = pl.BlockSpec(memory_space=pltpu.HBM)
+
+
+def in_hbm(values):
+    return [pltpu.with_memory_space_constraint(value, pltpu.HBM) for value in values]
+
+
+def served_side(member):
+    return (member + member // 4) % 2
+
+
+def prep_kernel(
+    keys, values, queries, residual, sink, routes, low, high, own, asked, base, sinks, slots,
+    named, sems,
+):
+    head, length = keys.shape
+    copies = [
+        pltpu.make_async_copy(source, target, sems.at[i])
+        for i, (source, target) in enumerate(
+            (
+                (keys, own.at[pl.ds(0, head)]),
+                (values, own.at[pl.ds(head, head)]),
+                (queries, asked),
+                (residual, base),
+                (sink, sinks),
+                (routes, named),
+            )
+        )
+    ]
+    for copy in copies:
+        copy.start()
+    for copy in copies:
+        copy.wait()
+    low[...] = own[:, length - WINDOW :]
+    high[...] = own[:, :WINDOW]
+    ways, count = named.shape
+    flat = named[...].astype(jnp.float32)
+    row = lax.broadcasted_iota(jnp.int32, (count, count), 0)
+    col = lax.broadcasted_iota(jnp.int32, (count, count), 1)
+    eye = jnp.where(row == col, 1.0, 0.0)
+    upright = lax.dot_general(
+        eye, flat, (((1,), (1,)), ((), ())), preferred_element_type=jnp.float32
+    )
+    lane = lax.broadcasted_iota(jnp.int32, slots.shape, 1)
+    result = jnp.zeros(slots.shape, jnp.float32)
+    for way in range(ways):
+        mine = upright[:, way : way + 1]
+        rank = jnp.zeros((count, 1), jnp.float32)
+        for other in range(ways):
+            same = (flat[other : other + 1, :] == mine) & (col < row)
+            rank = rank + jnp.sum(jnp.where(same, 1.0, 0.0), axis=1, keepdims=True)
+        result = jnp.where(lane == way, mine * 2.0 + rank, result)
+    slots[...] = result.astype(jnp.bfloat16)
+
+
+def prepare(keys, values, queries, residual, sink, routes):
+    head, length = keys.shape
+    tok_rows = residual.shape[0]
+    bf16 = jnp.bfloat16
+    return pl.pallas_call(
+        prep_kernel,
+        out_shape=(
+            jax.ShapeDtypeStruct((2 * head, WINDOW), bf16),
+            jax.ShapeDtypeStruct((2 * head, WINDOW), bf16),
+            jax.ShapeDtypeStruct((2 * head, length), bf16),
+            jax.ShapeDtypeStruct(queries.shape, bf16),
+            jax.ShapeDtypeStruct(residual.shape, bf16),
+            jax.ShapeDtypeStruct(sink.shape, jnp.float32),
+            jax.ShapeDtypeStruct((tok_rows, 128), bf16),
+        ),
+        in_specs=[ANYWHERE] * 6,
+        out_specs=(VMEM,) * 7,
+        scratch_shapes=[pltpu.VMEM(routes.shape, jnp.int32), pltpu.SemaphoreType.DMA((6,))],
+        compiler_params=pltpu.CompilerParams(vmem_limit_bytes=4 * 2**20),
+        name="prepare",
+    )(*in_hbm((keys, values, queries, residual, sink, routes)))
 
 
 def attend_kernel(place, sink, queries, low, own, high, residual, slots, out):
@@ -37,9 +112,10 @@
             asked = queries[block * WINDOW : (block + 1) * WINDOW, head * HEAD : (head + 1) * HEAD]
             scores = jnp.dot(asked, keys, preferred_element_type=jnp.float32) * HEAD ** (-0.5)
             masked = jnp.where(valid, scores, NEGATIVE)
-            top = jnp.maximum(jnp.max(masked, axis=-1, keepdims=True), sink[head])
+            bound = sink[:, head : head + 1]
+            top = jnp.maximum(jnp.max(masked, axis=-1, keepdims=True), bound)
             probs = jnp.exp(masked - top)
-            denom = jnp.sum(probs, axis=-1, keepdims=True) + jnp.exp(sink[head] - top)
+            denom = jnp.sum(probs, axis=-1, keepdims=True) + jnp.exp(bound - top)
             weights = (probs / denom).astype(jnp.bfloat16)
             heads.append(
                 lax.dot_general(
@@ -60,7 +136,7 @@
     return pl.pallas_call(
         attend_kernel,
         out_shape=jax.ShapeDtypeStruct((members, length + 2 * tok_rows, 128), jnp.bfloat16),
-        in_specs=[SMEM, SMEM] + [VMEM] * 6,
+        in_specs=[SMEM] + [VMEM] * 7,
         out_specs=VMEM,
         cost_estimate=pl.CostEstimate(
             flops=4 * length * both * 3 * WINDOW,
@@ -129,26 +205,38 @@
     )(arrived, weight)
 
 
-def spread_kernel(dispatched, out, rows):
+def spread_kernel(dispatched, out, rows, block, sems):
     planes, lines, _ = dispatched.shape
     members = out.shape[0]
     for plane in range(planes):
         rows[plane * lines : (plane + 1) * lines, :] = dispatched[plane].astype(jnp.float32)
-    for line in range(lines):
-        side, at = line // (lines // 2), line % (lines // 2)
-        group = rows[pl.ds(line, planes, stride=lines), :].astype(jnp.bfloat16)
-        for k in range(members // 2):
-            out[2 * k + side, at * planes : (at + 1) * planes, :] = group
+    copies = [
+        pltpu.make_async_copy(block.at[served_side(t)], out.at[t], sems.at[t])
+        for t in range(members)
+    ]
+    for side in range(2):
+        for at in range(lines // 2):
+            group = rows[pl.ds(side * (lines // 2) + at, planes, stride=lines), :]
+            block[side, at * planes : (at + 1) * planes, :] = group.astype(jnp.bfloat16)
+        for t in range(members):
+            if served_side(t) == side:
+                copies[t].start()
+    for copy in copies:
+        copy.wait()
 
 
 def spread(dispatched, members):
     planes, lines, lanes = dispatched.shape
     return pl.pallas_call(
         spread_kernel,
-        out_shape=jax.ShapeDtypeStruct((members, planes * lines // 2, lanes), jnp.bfloat16),
+        out_shape=pltpu.HBM((members, planes * lines // 2, lanes), jnp.bfloat16),
         in_specs=[VMEM],
-        out_specs=VMEM,
-        scratch_shapes=[pltpu.VMEM((planes * lines, lanes), jnp.float32)],
+        out_specs=ANYWHERE,
+        scratch_shapes=[
+            pltpu.VMEM((planes * lines, lanes), jnp.float32),
+            pltpu.VMEM((2, planes * lines // 2, lanes), jnp.bfloat16),
+            pltpu.SemaphoreType.DMA((members,)),
+        ],
         cost_estimate=pl.CostEstimate(
             flops=planes * lines * lanes,
             bytes_accessed=members * planes * lines * lanes,
@@ -166,69 +254,58 @@
 
 
 def expert_kernel(
-    serves,
-    gathered,
-    own,
-    gain,
-    gate_own,
-    up_own,
-    down_own,
-    gate_one,
-    up_one,
-    down_one,
-    gate_two,
-    up_two,
-    down_two,
-    out,
-    gate,
-    up,
-    down,
-    normed,
-    sems,
+    serves, gathered, own, gain,
+    gate_own, up_own, down_own,
+    gate_x, up_x, down_x, gate_y, up_y, down_y,
+    gate_fx, up_fx, down_fx, gate_fy, up_fy, down_fy,
+    out, gate, up, down, normed, sems,
 ):
-    half = gate_own.shape[0]
-    width = gate_own.shape[1]
+    half, width = gate_own.shape
+    part = half // 2
     pairs, rows, piece = gathered.shape
     members = out.shape[0]
     each = rows // members
     tiles = width // 128
-    lower = [
-        pltpu.make_async_copy(source, target.at[pl.ds(0, half)], sems.at[i])
-        for i, (source, target) in enumerate(((gate_one, gate), (up_one, up), (down_one, down)))
-    ]
-    for copy in lower:
+    targets = (gate, up, down)
+
+    def placed(sources, start, size, base):
+        return [
+            pltpu.make_async_copy(source, target.at[pl.ds(start, size)], sems.at[base + i])
+            for i, (source, target) in enumerate(zip(sources, targets))
+        ]
+
+    received_x = placed((gate_x, up_x, down_x), 0, part, 0)
+    received_y = placed((gate_y, up_y, down_y), part, part, 3)
+    held = placed((gate_own, up_own, down_own), half, half, 6)
+    forwarded_x = placed((gate_fx, up_fx, down_fx), half, part, 6)
+    forwarded_y = placed((gate_fy, up_fy, down_fy), half + part, part, 6)
+    for copy in received_x + received_y:
         copy.start()
-
-    def upper(sources):
-        return [
-            pltpu.make_async_copy(source, target.at[pl.ds(half, half)], sems.at[3 + i])
-            for i, (source, target) in enumerate(zip(sources, (gate, up, down)))
-        ]
 
     @pl.when(serves[0] == 1)
     def _():
-        for copy in upper((gate_own, up_own, down_own)):
+        for copy in held:
             copy.start()
 
     @pl.when(serves[0] != 1)
     def _():
-        for copy in upper((gate_two, up_two, down_two)):
+        for copy in forwarded_x + forwarded_y:
             copy.start()
 
     total = jnp.zeros((rows, 1), jnp.float32)
     for k in range(pairs):
-        part = gathered[k].astype(jnp.float32)
-        total = total + jnp.sum(part * part, axis=-1, keepdims=True)
+        block = gathered[k].astype(jnp.float32)
+        total = total + jnp.sum(block * block, axis=-1, keepdims=True)
     inverse = lax.rsqrt(total * (1.0 / width) + EPS)
     for k in range(pairs):
-        part = gathered[k].astype(jnp.float32)
-        scaled = part * inverse * gain[:, k * piece : (k + 1) * piece]
+        block = gathered[k].astype(jnp.float32)
+        scaled = block * inverse * gain[:, k * piece : (k + 1) * piece]
         normed[:, k * piece : (k + 1) * piece] = scaled.astype(jnp.bfloat16)
     for t in range(members):
         out[t, each * tiles :, :] = own[t * 16 : (t + 1) * 16, :]
-    others = upper((gate_two, up_two, down_two))
-    for copy in (lower[0], others[0], lower[1], others[1]):
-        copy.wait()
+    for i in range(2):
+        for copy in (received_x[i], received_y[i], held[i]):
+            copy.wait()
     contract = (((1,), (1,)), ((), ()))
     hidden = []
     for start, size in ((0, 256), (256, 256), (512, 128)):
@@ -240,8 +317,8 @@
         )
         hidden.append((g / (1.0 + jnp.exp(-g)) * u).astype(jnp.bfloat16))
     hidden = jnp.concatenate(hidden, axis=1)
-    lower[2].wait()
-    others[2].wait()
+    for copy in (received_x[2], received_y[2], held[2]):
+        copy.wait()
     for chunk in range(width // 256):
         share = jnp.dot(
             hidden, down[:, pl.ds(chunk * 256, 256)], preferred_element_type=jnp.float32
@@ -254,7 +331,7 @@
                 ]
 
 
-def run_expert(serves, gathered, own, norm_gain, owned, first, second):
+def run_expert(serves, gathered, own, norm_gain, owned, moved):
     pairs, rows, _ = gathered.shape
     half, width = owned[0].shape
     members = pairs
@@ -263,10 +340,10 @@
         out_shape=jax.ShapeDtypeStruct(
             (members, rows // members * (width // 128) + 16, 128), jnp.bfloat16
         ),
-        in_specs=[SMEM, VMEM, VMEM, VMEM] + [ANYWHERE] * 9,
+        in_specs=[SMEM, VMEM, VMEM, VMEM] + [ANYWHERE] * 15,
         out_specs=VMEM,
         scratch_shapes=[pltpu.VMEM((2 * half, width), jnp.bfloat16) for _ in range(3)]
-        + [pltpu.VMEM((rows, width), jnp.bfloat16), pltpu.SemaphoreType.DMA((6,))],
+        + [pltpu.VMEM((rows, width), jnp.bfloat16), pltpu.SemaphoreType.DMA((9,))],
         cost_estimate=pl.CostEstimate(
             flops=12 * rows * half * width,
             bytes_accessed=12 * half * width + 4 * rows * width,
@@ -274,19 +351,20 @@
         ),
         compiler_params=pltpu.CompilerParams(vmem_limit_bytes=28 * 2**20),
         name="expert",
-    )(serves, gathered, own, norm_gain.reshape(1, -1), *owned, *first, *second)
+    )(serves, gathered, own, norm_gain.reshape(1, -1), *in_hbm(owned), *in_hbm(moved))
 
 
 def sum_kernel(shares, out, acc):
-    members, rows, _ = shares.shape
+    members, rows, lanes = shares.shape
     planes = out.shape[0]
     tiles = (rows - 16) // (2 * planes)
     for side in range(2):
         for block in range(2):
             lo, size = block * (rows - 16) // 2, (rows - 16) // 2
-            total = shares[side, pl.ds(lo, size), :].astype(jnp.float32)
-            for k in range(1, members // 2):
-                total = total + shares[2 * k + side, pl.ds(lo, size), :].astype(jnp.float32)
+            total = jnp.zeros((size, lanes), jnp.float32)
+            for t in range(members):
+                if served_side(t) == side:
+                    total = total + shares[t, pl.ds(lo, size), :].astype(jnp.float32)
             acc[pl.ds(lo, size), :] = total
         for rank in range(2):
             for plane in range(planes):
@@ -329,48 +407,42 @@
     n_sp, n_tp = lax.axis_size("sp"), lax.axis_size("tp")
     planes = n_sp // 2
     tok_rows, width = residual.shape
-    cols = width // n_tp
     length = queries.shape[0]
-    parity = lax.axis_index("tp") % 2
     same_core = [[plane * 2 + core for plane in range(planes)] for core in range(2)]
 
-    first_moves, second_moves = [], []
+    moves_x, moves_y, passes = [], [], []
     for plane in range(planes):
         for core in range(2):
             for member in range(n_tp):
                 source = (plane * 2 + core) * n_tp + member
                 across = (plane * 2 + 1 - core) * n_tp + member
-                if member % 2 == core:
-                    first_moves.append((source, across))
-                    second_moves.append((source, across))
+                if served_side(member) == core:
+                    for moves in (moves_x, moves_y, passes):
+                        moves.append((source, across))
                 else:
-                    first_moves.append((source, source ^ 1))
-    serves = (lax.axis_index("sp") % 2 == parity).astype(jnp.int32).reshape(1)
-    gate_own, up_own, down_own = gate_weight[0].T, up_weight[0].T, down_weight[0]
-    gate_one = lax.ppermute(gate_own, ("sp", "tp"), first_moves)
-    up_one = lax.ppermute(up_own, ("sp", "tp"), first_moves)
-    down_one = lax.ppermute(down_own, ("sp", "tp"), first_moves)
-    gate_two = lax.ppermute(gate_one, ("sp", "tp"), second_moves)
-    up_two = lax.ppermute(up_one, ("sp", "tp"), second_moves)
-    down_two = lax.ppermute(down_one, ("sp", "tp"), second_moves)
-
-    expert_ids = routes.reshape(-1)
-    count = expert_ids.shape[0]
-    before = jnp.arange(count)[None, :] < jnp.arange(count)[:, None]
-    same = (expert_ids[:, None] == expert_ids[None, :]) & before
-    rank = jnp.sum(same.astype(jnp.int32), axis=1)
-    slots = (expert_ids * 2 + rank).reshape(tok_rows, 2)
-    slot_rows = jnp.pad(slots.astype(jnp.bfloat16), ((0, 0), (0, cols - 2)))
-
-    joined = jnp.concatenate([keys.T, values.T], axis=0)
+                    moves_x.append((source, source ^ 1))
+                    moves_y.append((source, source ^ 4))
+    core_index = lax.axis_index("sp") % 2
+    serves = (core_index == served_side(lax.axis_index("tp"))).astype(jnp.int32).reshape(1)
+    owned = (gate_weight[0].T, up_weight[0].T, down_weight[0])
+    part = owned[0].shape[0] // 2
+    received, forwarded = [], []
+    for direction, moves in (("x", moves_x), ("y", moves_y)):
+        lo = 0 if direction == "x" else part
+        for weight in owned:
+            piece = weight[lo : lo + part]
+            received.append(lax.ppermute(piece, ("sp", "tp"), moves))
+            forwarded.append(lax.ppermute(received[-1], ("sp", "tp"), passes))
+
+    low, high, joined, asked, base, sinks, slot_rows = prepare(
+        keys.T, values.T, queries, residual, sink_logit.reshape(1, -1), routes.T
+    )
     forward = [(i, i + 1) for i in range(n_sp - 1)]
     backward = [(i + 1, i) for i in range(n_sp - 1)]
-    low = lax.ppermute(joined[:, length - WINDOW :], "sp", forward)
-    high = lax.ppermute(joined[:, :WINDOW], "sp", backward)
+    low = lax.ppermute(low, "sp", forward)
+    high = lax.ppermute(high, "sp", backward)
     where = jnp.stack([lax.axis_index("sp"), jnp.int32(n_sp)]).astype(jnp.int32)
-    message = run_attention(
-        where, sink_logit, queries, low, joined, high, residual, slot_rows, n_tp
-    )
+    message = run_attention(where, sinks, asked, low, joined, high, base, slot_rows, n_tp)
 
     arrived = exchange(message, "tp")
     own, sending = project(arrived, out_weight, planes, length)
@@ -378,15 +450,7 @@
     dispatched = exchange(sending, "sp", same_core)
     to_servers = spread(dispatched, n_tp)
     gathered = exchange(to_servers, "tp")
-    pieces = run_expert(
-        serves,
-        gathered,
-        own,
-        norm_gain,
-        (gate_own, up_own, down_own),
-        (gate_one, up_one, down_one),
-        (gate_two, up_two, down_two),
-    )
+    pieces = run_expert(serves, gathered, own, norm_gain, owned, (*received, *forwarded))
 
     shares = exchange(pieces, "tp")
     own_rows = shares[:, 2 * n_tp * planes :].transpose(1, 0, 2).reshape(tok_rows, width)
@@ -394,6 +458,7 @@
 
     returned = exchange(returning, "sp", same_core)
     returned = returned.reshape(planes * 4, width)
+    slots = slot_rows[:, :2].astype(jnp.int32)
     place = (slots[:, :, None] == jnp.arange(2 * n_sp)[None, None, :]).astype(jnp.bfloat16)
     first = jnp.dot(place[:, 0], returned, preferred_element_type=jnp.float32)
     second = jnp.dot(place[:, 1], returned, preferred_element_type=jnp.float32)

time: 197 us -> 208 us (1.056)
  the two profiles are of different devices: /device:TPU:8 before, /device:TPU:64 now
where the time goes in v4:
time: 208 us; the launch traced here: 207 us
  starting transfers between devices  65.5 us (31%)
  blocking collectives  62.1 us (30%)
  waiting for transfers between devices  58.3 us (28%)
  Pallas kernels  16.7 us (8%)
  local copies, waits for them, and re-layouts  2.81 us (1%)
    all_to_all x2, blocking collectives, exchange(): lax.all_to_all(value, axis, split_axis=0, concat_axis=0, tiled=True, axis...  62.1 us
    all_to_all x3, starting transfers between devices, exchange(): lax.all_to_all(value, axis, split_axis=0, concat_axis=0, tiled=True, axis...  31.4 us
    all_to_all x3, waiting for transfers between devices, exchange(): lax.all_to_all(value, axis, split_axis=0, concat_axis=0, tiled=True, axis...  29.7 us
    ppermute x6, waiting for transfers between devices, local(): received.append(lax.ppermute(piece, ('sp', 'tp'), moves))  26.1 us
    ppermute x6, starting transfers between devices, local(): forwarded.append(lax.ppermute(received[-1], ('sp', 'tp'), passes))  14.8 us
    ppermute x6, starting transfers between devices, local(): received.append(lax.ppermute(piece, ('sp', 'tp'), moves))  13.7 us
    pallas_call x1, Pallas kernels, run_expert(): pl.pallas_call(expert_kernel, out_shape=jax.ShapeDtypeStruct((members, ro...  8.26 us
  transfers between devices with their start and end apart: 17, of which 7 were waited for; matrix products, arithmetic and copies ran while one was open for 1% of the time, Pallas kernels for 1%

profile of v4, /device:TPU:64, one launch (start us, length us, event | category | flops | bytes accessed | tf_op | source)
XLA Modules:
  0.0 206.8 jit_solution(15333540730165483101)
XLA Ops:
  0.0 1.3 prepare.1
  1.3 1.9 collective-permute-start
  3.3 3.6 %collective-permute-start.1 = (bf16[128,128]{1,0:T(8,128)(2,1)S(1)}, bf16[128,128]{1,0:T(8,128)(2,1)S(1)}, u32[]{:S(2)}, u32[]{:S(2)}) collective-permute-start(bf16[128,128]{1,0:T(8,128)(2,1)S(1)} %get-tuple-element.18), channel_id=1, source_target_pairs={{16,0},{32,16},{48,32},{64,48},{80,64},{96,80},{112,96},{128,112},... | collective-permute-start | bytes 98312 | tf_op jit(solution)/shard_map/ppermute | solution.py:443
  6.9 0.1 pad_add_fusion.place
  7.0 0.0 collective-permute-done.low
  7.0 1.5 collective-permute-done.1.high
  8.5 2.7 %attend.1 = bf16[16,288,128]{2,1,0:T(8,128)(2,1)S(1)} custom-call(s32[2]{0:T(128)S(1)} %pad_add_fusion.place, f32[1,2]{1,0:T(1,128)S(1)} %get-tuple-element.14.sink, bf16[256,128]{1,0:T(8,128)(2,1)S(1)} %get-tuple-element.15.queries, bf16[128,128]{1,0:T(8,128)(2,1)S(1)} %collective-permute-done.low, bf16[128,256]{1,0:T(8,128)(2,1)S(1)} %get-tuple-element.17.own, ...), custom_call_target="tpu_custom_call" | custom-call | flops 50331648 | bytes 2097152 | tf_op jit(solution)/shard_map/attend/pallas_call | solution.py:136
  11.2 0.0 copy-start
  11.2 26.2 %all_to_all.25.arrived = bf16[16,288,128]{2,1,0:T(8,128)(2,1)S(1)} all-to-all(bf16[16,288,128]{2,1,0:T(8,128)(2,1)S(1)} %attend.1), channel_id=1, replica_groups=mesh['sp'=32,'tp'=16] {'tp'}, dimensions={0} | all-to-all | bytes 2359296 | tf_op jit(solution)/shard_map/all_to_all | solution.py:251
  37.4 0.0 copy-done
  37.4 1.4 project.1
  38.8 15.5 %all-to-all-start.1 = ((bf16[16,64,128]{2,1,0:T(8,128)(2,1)}), bf16[16,64,128]{2,1,0:T(8,128)(2,1)S(1)}, u32[]{:S(2)}, u32[]{:S(2)}) async-start(bf16[16,64,128]{2,1,0:T(8,128)(2,1)} %get-tuple-element.21), calls=%async_computation.1 | async-start | bytes 524288 | tf_op jit(solution)/shard_map/all_to_all | solution.py:251
  54.3 0.0 copy-done.2
  54.3 0.0 copy-start.3
  54.4 1.2 fusion.4
  55.6 1.9 collective-permute-start.5
  57.5 0.0 copy-done.3
  57.5 1.2 fusion.3
  58.7 1.9 collective-permute-start.6
  60.6 11.6 %all-to-all-done.1.dispatched = bf16[16,64,128]{2,1,0:T(8,128)(2,1)S(1)} async-done(((bf16[16,64,128]{2,1,0:T(8,128)(2,1)}), bf16[16,64,128]{2,1,0:T(8,128)(2,1)S(1)}, u32[]{:S(2)}, u32[]{:S(2)}) %all-to-all-start.1) | async-done | bytes 262176 | tf_op jit(solution)/shard_map/all_to_all | solution.py:251
  72.3 1.7 spread.1
  74.0 0.0 copy-start.4
  74.0 3.9 %all-to-all-start.2 = ((bf16[16,512,128]{2,1,0:T(8,128)(2,1)}), bf16[16,512,128]{2,1,0:T(8,128)(2,1)S(1)}, u32[]{:S(2)}, u32[]{:S(2)}) async-start(bf16[16,512,128]{2,1,0:T(8,128)(2,1)} %spread.1), calls=%async_computation.2 | async-start | bytes 4194304 | tf_op jit(solution)/shard_map/all_to_all | solution.py:251
  77.9 1.9 collective-permute-start.2
  79.8 0.0 copy-start.1
  79.8 1.9 collective-permute-start.3
  81.7 0.0 copy-done.4
  81.7 0.1 slice_bitcast_fusion
  81.9 3.9 %collective-permute-start.4 = (bf16[160,2048]{1,0:T(8,128)(2,1)S(1)}, bf16[160,2048]{1,0:T(8,128)(2,1)S(1)}, u32[]{:S(2)}, u32[]{:S(2)}) collective-permute-start(bf16[160,2048]{1,0:T(8,128)(2,1)S(1)} %get-tuple-element.24), channel_id=1, source_target_pairs={{0,16},{1,0},{2,18},{3,2},{4,5},{5,21},{6,7},{7,23},{8,24},{9,8},{... | collective-permute-start | bytes 1966088 | tf_op jit(solution)/shard_map/ppermute | solution.py:434
  85.8 0.0 collective-permute-done.5.gate_y
  85.8 2.1 %collective-permute-start.7 = (bf16[160,2048]{1,0:T(8,128)(2,1)S(1)}, bf16[160,2048]{1,0:T(8,128)(2,1)S(1)}, u32[]{:S(2)}, u32[]{:S(2)}) collective-permute-start(bf16[160,2048]{1,0:T(8,128)(2,1)S(1)} %get-tuple-element.23), channel_id=1, source_target_pairs={{0,16},{1,5},{2,18},{3,7},{4,0},{5,21},{6,2},{7,23},{8,24},{9,13},... | collective-permute-start | bytes 1966088 | tf_op jit(solution)/shard_map/ppermute | solution.py:434
  88.0 0.0 collective-permute-done.6.up_y
  88.0 4.1 %collective-permute-start.11 = (bf16[160,2048]{1,0:T(8,128)(2,1)}, bf16[160,2048]{1,0:T(8,128)(2,1)}, u32[]{:S(2)}, u32[]{:S(2)}) collective-permute-start(bf16[160,2048]{1,0:T(8,128)(2,1)} %collective-permute-done.5.gate_y), channel_id=1, source_target_pairs={{0,16},{2,18},{5,21},{7,23},{8,24},{10,26},{13,29},{15,31},{17,1},... | collective-permute-start | bytes 1966088 | tf_op jit(solution)/shard_map/ppermute | solution.py:435
  92.0 16.5 %collective-permute-done.2.gate_x = bf16[160,2048]{1,0:T(8,128)(2,1)} collective-permute-done((bf16[160,2048]{1,0:T(8,128)(2,1)}, bf16[160,2048]{1,0:T(8,128)(2,1)}, u32[]{:S(2)}, u32[]{:S(2)}) %collective-permute-start.2) | collective-permute-done | bytes 655392 | tf_op jit(solution)/shard_map/ppermute | solution.py:434
  108.5 2.2 %collective-permute-start.12 = (bf16[160,2048]{1,0:T(8,128)(2,1)}, bf16[160,2048]{1,0:T(8,128)(2,1)}, u32[]{:S(2)}, u32[]{:S(2)}) collective-permute-start(bf16[160,2048]{1,0:T(8,128)(2,1)} %collective-permute-done.6.up_y), channel_id=1, source_target_pairs={{0,16},{2,18},{5,21},{7,23},{8,24},{10,26},{13,29},{15,31},{17,1},... | collective-permute-start | bytes 1966088 | tf_op jit(solution)/shard_map/ppermute | solution.py:435
  110.7 4.9 %collective-permute-done.3.up_x = bf16[160,2048]{1,0:T(8,128)(2,1)} collective-permute-done((bf16[160,2048]{1,0:T(8,128)(2,1)}, bf16[160,2048]{1,0:T(8,128)(2,1)}, u32[]{:S(2)}, u32[]{:S(2)}) %collective-permute-start.3) | collective-permute-done | bytes 655392 | tf_op jit(solution)/shard_map/ppermute | solution.py:434
  115.6 2.2 %collective-permute-start.8 = (bf16[160,2048]{1,0:T(8,128)(2,1)}, bf16[160,2048]{1,0:T(8,128)(2,1)}, u32[]{:S(2)}, u32[]{:S(2)}) collective-permute-start(bf16[160,2048]{1,0:T(8,128)(2,1)} %collective-permute-done.2.gate_x), channel_id=1, source_target_pairs={{0,16},{2,18},{5,21},{7,23},{8,24},{10,26},{13,29},{15,31},{17,1},... | collective-permute-start | bytes 1966088 | tf_op jit(solution)/shard_map/ppermute | solution.py:435
  117.7 4.7 %collective-permute-done.4.down_x = bf16[160,2048]{1,0:T(8,128)(2,1)S(1)} collective-permute-done((bf16[160,2048]{1,0:T(8,128)(2,1)S(1)}, bf16[160,2048]{1,0:T(8,128)(2,1)S(1)}, u32[]{:S(2)}, u32[]{:S(2)}) %collective-permute-start.4) | collective-permute-done | bytes 655392 | tf_op jit(solution)/shard_map/ppermute | solution.py:434
  122.5 2.2 %collective-permute-start.9 = (bf16[160,2048]{1,0:T(8,128)(2,1)}, bf16[160,2048]{1,0:T(8,128)(2,1)}, u32[]{:S(2)}, u32[]{:S(2)}) collective-permute-start(bf16[160,2048]{1,0:T(8,128)(2,1)} %collective-permute-done.3.up_x), channel_id=1, source_target_pairs={{0,16},{2,18},{5,21},{7,23},{8,24},{10,26},{13,29},{15,31},{17,1},... | collective-permute-start | bytes 1966088 | tf_op jit(solution)/shard_map/ppermute | solution.py:435
  124.6 0.0 collective-permute-done.7.down_y
  124.7 2.2 %collective-permute-start.10 = (bf16[160,2048]{1,0:T(8,128)(2,1)S(1)}, bf16[160,2048]{1,0:T(8,128)(2,1)}, u32[]{:S(2)}, u32[]{:S(2)}) collective-permute-start(bf16[160,2048]{1,0:T(8,128)(2,1)S(1)} %collective-permute-done.4.down_x), channel_id=1, source_target_pairs={{0,16},{2,18},{5,21},{7,23},{8,24},{10,26},{13,29},{15,31},{17,1},... | collective-permute-start | bytes 1966088 | tf_op jit(solution)/shard_map/ppermute | solution.py:435
  126.8 0.0 collective-permute-done.11.gate_fy
  126.8 2.1 %collective-permute-start.13 = (bf16[160,2048]{1,0:T(8,128)(2,1)S(1)}, bf16[160,2048]{1,0:T(8,128)(2,1)}, u32[]{:S(2)}, u32[]{:S(2)}) collective-permute-start(bf16[160,2048]{1,0:T(8,128)(2,1)S(1)} %collective-permute-done.7.down_y), channel_id=1, source_target_pairs={{0,16},{2,18},{5,21},{7,23},{8,24},{10,26},{13,29},{15,31},{17,1},... | collective-permute-start | bytes 1966088 | tf_op jit(solution)/shard_map/ppermute | solution.py:435
  128.9 0.0 collective-permute-done.12.up_fy
  128.9 0.0 collective-permute-done.8.gate_fx
  128.9 0.0 collective-permute-done.9.up_fx
  128.9 0.0 collective-permute-done.10.down_fx
  128.9 1.0 collective-permute-done.13.down_fy
  129.9 0.0 all-to-all-done.2.gathered
  129.9 0.0 copy-done.5
  129.9 0.0 copy-done.6
  129.9 0.0 copy-done.1
  130.0 8.3 %expert.1 = bf16[16,528,128]{2,1,0:T(8,128)(2,1)S(1)} custom-call(s32[1]{0:T(128)} %bitcast.serves, bf16[16,512,128]{2,1,0:T(8,128)(2,1)S(1)} %all-to-all-done.2.gathered, bf16[256,128]{1,0:T(8,128)(2,1)S(1)} %get-tuple-element.22.own, f32[1,2048]{1,0:T(1,128)S(1)} %bitcast.38, bf16[320,2048]{1,0:T(8,128)(2,1)} %bitcast.39, bf16[320,2048]{1,0:T(8,128)(2,1)} %bitcast.41, ...), custom_call_target="tpu_custom_call" | custom-call | flops 4026531840 | bytes 12058624 | tf_op jit(solution)/shard_map/expert/pallas_call | solution.py:338
  138.2 35.9 %all_to_all.26.shares = bf16[16,528,128]{2,1,0:T(8,128)(2,1)S(1)} all-to-all(bf16[16,528,128]{2,1,0:T(8,128)(2,1)S(1)} %expert.1), channel_id=1, replica_groups=mesh['sp'=32,'tp'=16] {'tp'}, dimensions={0} | all-to-all | bytes 4325376 | tf_op jit(solution)/shard_map/all_to_all | solution.py:251
  174.2 1.3 shares.1
  175.5 12.0 %all-to-all-start.4 = ((bf16[16,64,128]{2,1,0:T(8,128)(2,1)}), bf16[16,64,128]{2,1,0:T(8,128)(2,1)S(1)}, u32[]{:S(2)}, u32[]{:S(2)}) async-start(bf16[16,64,128]{2,1,0:T(8,128)(2,1)} %shares.1), calls=%async_computation.4 | async-start | bytes 524288 | tf_op jit(solution)/shard_map/all_to_all | solution.py:251
  187.5 0.1 copy.16
  187.6 0.0 copy-done.8
  187.6 0.1 iota_compare_fusion
  187.6 18.1 %all-to-all-done.4 = bf16[16,64,128]{2,1,0:T(8,128)(2,1)S(1)} async-done(((bf16[16,64,128]{2,1,0:T(8,128)(2,1)}), bf16[16,64,128]{2,1,0:T(8,128)(2,1)S(1)}, u32[]{:S(2)}, u32[]{:S(2)}) %all-to-all-start.4) | async-done | bytes 262176 | tf_op jit(solution)/shard_map/all_to_all | solution.py:251
  205.7 0.1 reshape.24
  205.8 0.2 convolution_multiply_fusion.1
  206.0 0.0 copy-done.7
  206.0 0.8 fusion.2
  (7 shorter events, 0.0 us)
Async XLA Ops:
  1.3 5.7 %collective-permute-start = (bf16[128,128]{1,0:T(8,128)(2,1)S(1)}, bf16[128,128]{1,0:T(8,128)(2,1)S(1)}, u32[]{:S(2)}, u32[]{:S(2)}) collective-permute-start(bf16[128,128]{1,0:T(8,128)(2,1)S(1)} %get-tuple-element.16), channel_id=1, source_target_pairs={{0,16},{16,32},{32,48},{48,64},{64,80},{80,96},{96,112},{112,128},... | collective-permute-start | bytes 98312 | tf_op jit(solution)/shard_map/ppermute | solution.py:442
  3.3 5.2 %collective-permute-start.1 = (bf16[128,128]{1,0:T(8,128)(2,1)S(1)}, bf16[128,128]{1,0:T(8,128)(2,1)S(1)}, u32[]{:S(2)}, u32[]{:S(2)}) collective-permute-start(bf16[128,128]{1,0:T(8,128)(2,1)S(1)} %get-tuple-element.18), channel_id=1, source_target_pairs={{16,0},{32,16},{48,32},{64,48},{80,64},{96,80},{112,96},{128,112},... | collective-permute-start | bytes 98312 | tf_op jit(solution)/shard_map/ppermute | solution.py:443
  11.2 26.2 %copy-start = (bf16[2048,128]{1,0:T(8,128)(2,1)S(1)}, bf16[2048,128]{1,0:T(8,128)(2,1)}, u32[]{:S(2)}) copy-start(bf16[2048,128]{1,0:T(8,128)(2,1)} %weight.1) | copy-start | bytes 1572868
  37.4 17.0 %copy-start.2 = (bf16[1,2048,320]{1,2,0:T(8,128)(2,1)S(1)}, bf16[1,2048,320]{1,2,0:T(8,128)(2,1)}, u32[]{:S(2)}) copy-start(bf16[1,2048,320]{1,2,0:T(8,128)(2,1)} %param.21) | copy-start | bytes 3932164
  38.8 33.4 %all-to-all-start.1 = ((bf16[16,64,128]{2,1,0:T(8,128)(2,1)}), bf16[16,64,128]{2,1,0:T(8,128)(2,1)S(1)}, u32[]{:S(2)}, u32[]{:S(2)}) async-start(bf16[16,64,128]{2,1,0:T(8,128)(2,1)} %get-tuple-element.21), calls=%async_computation.1 | async-start | bytes 524288 | tf_op jit(solution)/shard_map/all_to_all | solution.py:251
  54.3 3.1 %copy-start.3 = (bf16[1,2048,320]{1,2,0:T(8,128)(2,1)S(1)}, bf16[1,2048,320]{1,2,0:T(8,128)(2,1)}, u32[]{:S(2)}) copy-start(bf16[1,2048,320]{1,2,0:T(8,128)(2,1)} %param.22) | copy-start | bytes 3932164
  55.6 30.2 %collective-permute-start.5 = (bf16[160,2048]{1,0:T(8,128)(2,1)}, bf16[160,2048]{1,0:T(8,128)(2,1)}, u32[]{:S(2)}, u32[]{:S(2)}) collective-permute-start(bf16[160,2048]{1,0:T(8,128)(2,1)} %get-tuple-element.27), channel_id=1, source_target_pairs={{0,16},{1,5},{2,18},{3,7},{4,0},{5,21},{6,2},{7,23},{8,24},{9,13},... | collective-permute-start | bytes 1966088 | tf_op jit(solution)/shard_map/ppermute | solution.py:434
  58.7 29.2 %collective-permute-start.6 = (bf16[160,2048]{1,0:T(8,128)(2,1)}, bf16[160,2048]{1,0:T(8,128)(2,1)}, u32[]{:S(2)}, u32[]{:S(2)}) collective-permute-start(bf16[160,2048]{1,0:T(8,128)(2,1)} %get-tuple-element.25), channel_id=1, source_target_pairs={{0,16},{1,5},{2,18},{3,7},{4,0},{5,21},{6,2},{7,23},{8,24},{9,13},... | collective-permute-start | bytes 1966088 | tf_op jit(solution)/shard_map/ppermute | solution.py:434
  74.0 7.8 %copy-start.4 = (bf16[1,320,2048]{2,1,0:T(8,128)(2,1)S(1)}, bf16[1,320,2048]{2,1,0:T(8,128)(2,1)}, u32[]{:S(2)}) copy-start(bf16[1,320,2048]{2,1,0:T(8,128)(2,1)} %param.23) | copy-start | bytes 3932164
  74.0 56.0 %all-to-all-start.2 = ((bf16[16,512,128]{2,1,0:T(8,128)(2,1)}), bf16[16,512,128]{2,1,0:T(8,128)(2,1)S(1)}, u32[]{:S(2)}, u32[]{:S(2)}) async-start(bf16[16,512,128]{2,1,0:T(8,128)(2,1)} %spread.1), calls=%async_computation.2 | async-start | bytes 4194304 | tf_op jit(solution)/shard_map/all_to_all | solution.py:251
  77.9 30.7 %collective-permute-start.2 = (bf16[160,2048]{1,0:T(8,128)(2,1)}, bf16[160,2048]{1,0:T(8,128)(2,1)}, u32[]{:S(2)}, u32[]{:S(2)}) collective-permute-start(bf16[160,2048]{1,0:T(8,128)(2,1)} %get-tuple-element.28), channel_id=1, source_target_pairs={{0,16},{1,0},{2,18},{3,2},{4,5},{5,21},{6,7},{7,23},{8,24},{9,8},{... | collective-permute-start | bytes 1966088 | tf_op jit(solution)/shard_map/ppermute | solution.py:434
  79.8 50.2 %copy-start.1 = (f32[2048]{0:T(1024)S(1)}, f32[2048]{0:T(1024)}, u32[]{:S(2)}) copy-start(f32[2048]{0:T(1024)} %param.18) | copy-start | bytes 24580
  79.8 35.8 %collective-permute-start.3 = (bf16[160,2048]{1,0:T(8,128)(2,1)}, bf16[160,2048]{1,0:T(8,128)(2,1)}, u32[]{:S(2)}, u32[]{:S(2)}) collective-permute-start(bf16[160,2048]{1,0:T(8,128)(2,1)} %get-tuple-element.26), channel_id=1, source_target_pairs={{0,16},{1,0},{2,18},{3,2},{4,5},{5,21},{6,7},{7,23},{8,24},{9,8},{... | collective-permute-start | bytes 1966088 | tf_op jit(solution)/shard_map/ppermute | solution.py:434
  81.9 40.6 %collective-permute-start.4 = (bf16[160,2048]{1,0:T(8,128)(2,1)S(1)}, bf16[160,2048]{1,0:T(8,128)(2,1)S(1)}, u32[]{:S(2)}, u32[]{:S(2)}) collective-permute-start(bf16[160,2048]{1,0:T(8,128)(2,1)S(1)} %get-tuple-element.24), channel_id=1, source_target_pairs={{0,16},{1,0},{2,18},{3,2},{4,5},{5,21},{6,7},{7,23},{8,24},{9,8},{... | collective-permute-start | bytes 1966088 | tf_op jit(solution)/shard_map/ppermute | solution.py:434
  85.8 38.8 %collective-permute-start.7 = (bf16[160,2048]{1,0:T(8,128)(2,1)S(1)}, bf16[160,2048]{1,0:T(8,128)(2,1)S(1)}, u32[]{:S(2)}, u32[]{:S(2)}) collective-permute-start(bf16[160,2048]{1,0:T(8,128)(2,1)S(1)} %get-tuple-element.23), channel_id=1, source_target_pairs={{0,16},{1,5},{2,18},{3,7},{4,0},{5,21},{6,2},{7,23},{8,24},{9,13},... | collective-permute-start | bytes 1966088 | tf_op jit(solution)/shard_map/ppermute | solution.py:434
  88.0 38.8 %collective-permute-start.11 = (bf16[160,2048]{1,0:T(8,128)(2,1)}, bf16[160,2048]{1,0:T(8,128)(2,1)}, u32[]{:S(2)}, u32[]{:S(2)}) collective-permute-start(bf16[160,2048]{1,0:T(8,128)(2,1)} %collective-permute-done.5.gate_y), channel_id=1, source_target_pairs={{0,16},{2,18},{5,21},{7,23},{8,24},{10,26},{13,29},{15,31},{17,1},... | collective-permute-start | bytes 1966088 | tf_op jit(solution)/shard_map/ppermute | solution.py:435
  108.5 20.4 %collective-permute-start.12 = (bf16[160,2048]{1,0:T(8,128)(2,1)}, bf16[160,2048]{1,0:T(8,128)(2,1)}, u32[]{:S(2)}, u32[]{:S(2)}) collective-permute-start(bf16[160,2048]{1,0:T(8,128)(2,1)} %collective-permute-done.6.up_y), channel_id=1, source_target_pairs={{0,16},{2,18},{5,21},{7,23},{8,24},{10,26},{13,29},{15,31},{17,1},... | collective-permute-start | bytes 1966088 | tf_op jit(solution)/shard_map/ppermute | solution.py:435
  115.6 13.4 %collective-permute-start.8 = (bf16[160,2048]{1,0:T(8,128)(2,1)}, bf16[160,2048]{1,0:T(8,128)(2,1)}, u32[]{:S(2)}, u32[]{:S(2)}) collective-permute-start(bf16[160,2048]{1,0:T(8,128)(2,1)} %collective-permute-done.2.gate_x), channel_id=1, source_target_pairs={{0,16},{2,18},{5,21},{7,23},{8,24},{10,26},{13,29},{15,31},{17,1},... | collective-permute-start | bytes 1966088 | tf_op jit(solution)/shard_map/ppermute | solution.py:435
  122.5 7.5 %copy-start.5 = (bf16[160,2048]{1,0:T(8,128)(2,1)}, bf16[160,2048]{1,0:T(8,128)(2,1)S(1)}, u32[]{:S(2)}) copy-start(bf16[160,2048]{1,0:T(8,128)(2,1)S(1)} %collective-permute-done.4.down_x) | copy-start | bytes 1966084
  122.5 6.5 %collective-permute-start.9 = (bf16[160,2048]{1,0:T(8,128)(2,1)}, bf16[160,2048]{1,0:T(8,128)(2,1)}, u32[]{:S(2)}, u32[]{:S(2)}) collective-permute-start(bf16[160,2048]{1,0:T(8,128)(2,1)} %collective-permute-done.3.up_x), channel_id=1, source_target_pairs={{0,16},{2,18},{5,21},{7,23},{8,24},{10,26},{13,29},{15,31},{17,1},... | collective-permute-start | bytes 1966088 | tf_op jit(solution)/shard_map/ppermute | solution.py:435
  124.6 5.3 %copy-start.6 = (bf16[160,2048]{1,0:T(8,128)(2,1)}, bf16[160,2048]{1,0:T(8,128)(2,1)S(1)}, u32[]{:S(2)}) copy-start(bf16[160,2048]{1,0:T(8,128)(2,1)S(1)} %collective-permute-done.7.down_y) | copy-start | bytes 1966084
  124.7 4.3 %collective-permute-start.10 = (bf16[160,2048]{1,0:T(8,128)(2,1)S(1)}, bf16[160,2048]{1,0:T(8,128)(2,1)}, u32[]{:S(2)}, u32[]{:S(2)}) collective-permute-start(bf16[160,2048]{1,0:T(8,128)(2,1)S(1)} %collective-permute-done.4.down_x), channel_id=1, source_target_pairs={{0,16},{2,18},{5,21},{7,23},{8,24},{10,26},{13,29},{15,31},{17,1},... | collective-permute-start | bytes 1966088 | tf_op jit(solution)/shard_map/ppermute | solution.py:435
  126.8 3.1 %collective-permute-start.13 = (bf16[160,2048]{1,0:T(8,128)(2,1)S(1)}, bf16[160,2048]{1,0:T(8,128)(2,1)}, u32[]{:S(2)}, u32[]{:S(2)}) collective-permute-start(bf16[160,2048]{1,0:T(8,128)(2,1)S(1)} %collective-permute-done.7.down_y), channel_id=1, source_target_pairs={{0,16},{2,18},{5,21},{7,23},{8,24},{10,26},{13,29},{15,31},{17,1},... | collective-permute-start | bytes 1966088 | tf_op jit(solution)/shard_map/ppermute | solution.py:435
  174.1 13.4 %copy-start.8 = (f32[16,2]{0,1:T(2,128)S(1)}, f32[16,2]{0,1:T(2,128)}, u32[]{:S(2)}) copy-start(f32[16,2]{0,1:T(2,128)} %param.20) | copy-start | bytes 388
  175.5 30.5 %copy-start.7 = (bf16[16,2048]{1,0:T(8,128)(2,1)S(1)}, bf16[16,2048]{1,0:T(8,128)(2,1)}, u32[]{:S(2)}) copy-start(bf16[16,2048]{1,0:T(8,128)(2,1)} %residual.1) | copy-start | bytes 196612
  175.5 30.3 %all-to-all-start.4 = ((bf16[16,64,128]{2,1,0:T(8,128)(2,1)}), bf16[16,64,128]{2,1,0:T(8,128)(2,1)S(1)}, u32[]{:S(2)}, u32[]{:S(2)}) async-start(bf16[16,64,128]{2,1,0:T(8,128)(2,1)} %shares.1), calls=%async_computation.4 | async-start | bytes 524288 | tf_op jit(solution)/shard_map/all_to_all | solution.py:251

commit v5 on v4

--- a/solution.py
+++ b/solution.py
@@ -253,34 +253,72 @@
     )
 
 
+def pack_kernel(gate, up, down, *rest):
+    outs, sems = rest[:-1], rest[-1]
+    part = gate.shape[0] // len(outs)
+    copies = [
+        pltpu.make_async_copy(
+            source.at[pl.ds(k * part, part)], out.at[pl.ds(i * part, part)], sems.at[k * 3 + i]
+        )
+        for k, out in enumerate(outs)
+        for i, source in enumerate((gate, up, down))
+    ]
+    for copy in copies:
+        copy.start()
+    for copy in copies:
+        copy.wait()
+
+
+def pack(owned, ways):
+    half, width = owned[0].shape
+    return pl.pallas_call(
+        pack_kernel,
+        out_shape=tuple(pltpu.HBM((3 * half // ways, width), jnp.bfloat16) for _ in range(ways)),
+        in_specs=[ANYWHERE] * 3,
+        out_specs=(ANYWHERE,) * ways,
+        scratch_shapes=[pltpu.SemaphoreType.DMA((3 * ways,))],
+        cost_estimate=pl.CostEstimate(
+            flops=half * width, bytes_accessed=12 * half * width, transcendentals=0
+        ),
+        compiler_params=pltpu.CompilerParams(vmem_limit_bytes=2 * 2**20),
+        name="pack",
+    )(*in_hbm(owned))
+
+
 def expert_kernel(
-    serves, gathered, own, gain,
-    gate_own, up_own, down_own,
-    gate_x, up_x, down_x, gate_y, up_y, down_y,
-    gate_fx, up_fx, down_fx, gate_fy, up_fy, down_fy,
+    serves, gathered, own, gain, gate_own, up_own, down_own,
+    got_0, got_1, got_2, got_3, fwd_0, fwd_1, fwd_2, fwd_3,
     out, gate, up, down, normed, sems,
 ):
     half, width = gate_own.shape
-    part = half // 2
+    part = half // 4
     pairs, rows, piece = gathered.shape
     members = out.shape[0]
     each = rows // members
     tiles = width // 128
     targets = (gate, up, down)
 
-    def placed(sources, start, size, base):
+    def placed(packed, start, base):
         return [
-            pltpu.make_async_copy(source, target.at[pl.ds(start, size)], sems.at[base + i])
-            for i, (source, target) in enumerate(zip(sources, targets))
+            pltpu.make_async_copy(
+                packed.at[pl.ds(i * part, part)], target.at[pl.ds(start, part)], sems.at[base + i]
+            )
+            for i, target in enumerate(targets)
         ]
 
-    received_x = placed((gate_x, up_x, down_x), 0, part, 0)
-    received_y = placed((gate_y, up_y, down_y), part, part, 3)
-    held = placed((gate_own, up_own, down_own), half, half, 6)
-    forwarded_x = placed((gate_fx, up_fx, down_fx), half, part, 6)
-    forwarded_y = placed((gate_fy, up_fy, down_fy), half + part, part, 6)
-    for copy in received_x + received_y:
-        copy.start()
+    received = [
+        placed(packed, k * part, 3 * k) for k, packed in enumerate((got_0, got_1, got_2, got_3))
+    ]
+    forwarded = [
+        placed(packed, half + k * part, 12) for k, packed in enumerate((fwd_0, fwd_1, fwd_2, fwd_3))
+    ]
+    held = [
+        pltpu.make_async_copy(source, target.at[pl.ds(half, half)], sems.at[12 + i])
+        for i, (source, target) in enumerate(zip((gate_own, up_own, down_own), targets))
+    ]
+    for i in range(3):
+        for copies in received:
+            copies[i].start()
 
     @pl.when(serves[0] == 1)
     def _():
@@ -289,8 +327,9 @@
 
     @pl.when(serves[0] != 1)
     def _():
-        for copy in forwarded_x + forwarded_y:
-            copy.start()
+        for i in range(3):
+            for copies in forwarded:
+                copies[i].start()
 
     total = jnp.zeros((rows, 1), jnp.float32)
     for k in range(pairs):
@@ -304,7 +343,7 @@
     for t in range(members):
         out[t, each * tiles :, :] = own[t * 16 : (t + 1) * 16, :]
     for i in range(2):
-        for copy in (received_x[i], received_y[i], held[i]):
+        for copy in (*(copies[i] for copies in received), held[i]):
             copy.wait()
     contract = (((1,), (1,)), ((), ()))
     hidden = []
@@ -317,7 +356,7 @@
         )
         hidden.append((g / (1.0 + jnp.exp(-g)) * u).astype(jnp.bfloat16))
     hidden = jnp.concatenate(hidden, axis=1)
-    for copy in (received_x[2], received_y[2], held[2]):
+    for copy in (*(copies[2] for copies in received), held[2]):
         copy.wait()
     for chunk in range(width // 256):
         share = jnp.dot(
@@ -340,10 +379,10 @@
         out_shape=jax.ShapeDtypeStruct(
             (members, rows // members * (width // 128) + 16, 128), jnp.bfloat16
         ),
-        in_specs=[SMEM, VMEM, VMEM, VMEM] + [ANYWHERE] * 15,
+        in_specs=[SMEM, VMEM, VMEM, VMEM] + [ANYWHERE] * 11,
         out_specs=VMEM,
         scratch_shapes=[pltpu.VMEM((2 * half, width), jnp.bfloat16) for _ in range(3)]
-        + [pltpu.VMEM((rows, width), jnp.bfloat16), pltpu.SemaphoreType.DMA((9,))],
+        + [pltpu.VMEM((rows, width), jnp.bfloat16), pltpu.SemaphoreType.DMA((15,))],
         cost_estimate=pl.CostEstimate(
             flops=12 * rows * half * width,
             bytes_accessed=12 * half * width + 4 * rows * width,
@@ -410,29 +449,29 @@
     length = queries.shape[0]
     same_core = [[plane * 2 + core for plane in range(planes)] for core in range(2)]
 
-    moves_x, moves_y, passes = [], [], []
+    steps = ((0, 1), (0, 3), (1, 0), (3, 0))
+    moves, passes = [[] for _ in steps], []
     for plane in range(planes):
         for core in range(2):
             for member in range(n_tp):
                 source = (plane * 2 + core) * n_tp + member
                 across = (plane * 2 + 1 - core) * n_tp + member
                 if served_side(member) == core:
-                    for moves in (moves_x, moves_y, passes):
-                        moves.append((source, across))
+                    for way in moves:
+                        way.append((source, across))
+                    passes.append((source, across))
                 else:
-                    moves_x.append((source, source ^ 1))
-                    moves_y.append((source, source ^ 4))
+                    for way, (dy, dx) in zip(moves, steps):
+                        other = (member // 4 + dy) % 4 * 4 + (member % 4 + dx) % 4
+                        way.append((source, source - member + other))
     core_index = lax.axis_index("sp") % 2
     serves = (core_index == served_side(lax.axis_index("tp"))).astype(jnp.int32).reshape(1)
     owned = (gate_weight[0].T, up_weight[0].T, down_weight[0])
-    part = owned[0].shape[0] // 2
     received, forwarded = [], []
-    for direction, moves in (("x", moves_x), ("y", moves_y)):
-        lo = 0 if direction == "x" else part
-        for weight in owned:
-            piece = weight[lo : lo + part]
-            received.append(lax.ppermute(piece, ("sp", "tp"), moves))
-            forwarded.append(lax.ppermute(received[-1], ("sp", "tp"), passes))
+    packed = pack(owned, len(steps))
+    for k, way in enumerate(moves):
+        received.append(lax.ppermute(packed[k], ("sp", "tp"), way))
+        forwarded.append(lax.ppermute(received[-1], ("sp", "tp"), passes))
 
     low, high, joined, asked, base, sinks, slot_rows = prepare(
         keys.T, values.T, queries, residual, sink_logit.reshape(1, -1), routes.T

time: 208 us -> 298 us (1.43)
  the two profiles are of different devices: /device:TPU:64 before, /device:TPU:32 now
where the time goes in v5:
time: 298 us; the launch traced here: 297 us
  Pallas kernels  137 us (46%)
  blocking collectives  58.3 us (20%)
  starting transfers between devices  57.8 us (19%)
  waiting for transfers between devices  42.1 us (14%)
    pallas_call x1, Pallas kernels, pack(): pl.pallas_call(pack_kernel, out_shape=tuple((pltpu.HBM((3 * half // ways,...  120 us
    all_to_all x2, blocking collectives, exchange(): lax.all_to_all(value, axis, split_axis=0, concat_axis=0, tiled=True, axis...  58.3 us
    all_to_all x3, starting transfers between devices, exchange(): lax.all_to_all(value, axis, split_axis=0, concat_axis=0, tiled=True, axis...  34.5 us
    all_to_all x3, waiting for transfers between devices, exchange(): lax.all_to_all(value, axis, split_axis=0, concat_axis=0, tiled=True, axis...  30.3 us
    ppermute x4, starting transfers between devices, local(): forwarded.append(lax.ppermute(received[-1], ('sp', 'tp'), passes))  9.08 us
    ppermute x4, waiting for transfers between devices, local(): received.append(lax.ppermute(packed[k], ('sp', 'tp'), way))  8.77 us
    ppermute x4, starting transfers between devices, local(): received.append(lax.ppermute(packed[k], ('sp', 'tp'), way))  8.65 us
    pallas_call x1, Pallas kernels, run_expert(): pl.pallas_call(expert_kernel, out_shape=jax.ShapeDtypeStruct((members, ro...  8.31 us
  transfers between devices with their start and end apart: 13, of which 7 were waited for; matrix products, arithmetic and copies ran while one was open for 0% of the time, Pallas kernels for 41%

profile of v5, /device:TPU:32, one launch (start us, length us, event | category | flops | bytes accessed | tf_op | source)
XLA Modules:
  0.0 296.9 jit_solution(10011174943584935465)
XLA Ops:
  0.0 0.0 copy-start
  0.0 1.4 prepare.1
  1.4 1.9 collective-permute-start
  3.3 3.6 %collective-permute-start.1 = (bf16[128,128]{1,0:T(8,128)(2,1)S(1)}, bf16[128,128]{1,0:T(8,128)(2,1)S(1)}, u32[]{:S(2)}, u32[]{:S(2)}) collective-permute-start(bf16[128,128]{1,0:T(8,128)(2,1)S(1)} %get-tuple-element.22), channel_id=1, source_target_pairs={{16,0},{32,16},{48,32},{64,48},{80,64},{96,80},{112,96},{128,112},... | collective-permute-start | bytes 98312 | tf_op jit(solution)/shard_map/ppermute | solution.py:482
  7.0 0.1 pad_add_fusion.place
  7.0 0.0 collective-permute-done.low
  7.0 1.5 collective-permute-done.1.high
  8.5 2.7 attend.1
  11.2 26.1 %all_to_all.25.arrived = bf16[16,288,128]{2,1,0:T(8,128)(2,1)S(1)} all-to-all(bf16[16,288,128]{2,1,0:T(8,128)(2,1)S(1)} %attend.1), channel_id=1, replica_groups=mesh['sp'=32,'tp'=16] {'tp'}, dimensions={0} | all-to-all | bytes 2359296 | tf_op jit(solution)/shard_map/all_to_all | solution.py:251
  37.3 0.0 copy-done
  37.3 1.5 project.1
  38.7 16.0 %all-to-all-start.1 = ((bf16[16,64,128]{2,1,0:T(8,128)(2,1)}), bf16[16,64,128]{2,1,0:T(8,128)(2,1)S(1)}, u32[]{:S(2)}, u32[]{:S(2)}) async-start(bf16[16,64,128]{2,1,0:T(8,128)(2,1)} %get-tuple-element.25), calls=%async_computation.1 | async-start | bytes 524288 | tf_op jit(solution)/shard_map/all_to_all | solution.py:251
  54.7 120.3 %pack.1 = (bf16[240,2048]{1,0:T(8,128)(2,1)}, bf16[240,2048]{1,0:T(8,128)(2,1)}, bf16[240,2048]{1,0:T(8,128)(2,1)}, bf16[240,2048]{1,0:T(8,128)(2,1)}) custom-call(bf16[320,2048]{1,0:T(8,128)(2,1)} %bitcast.35, bf16[320,2048]{1,0:T(8,128)(2,1)} %bitcast.37, bf16[320,2048]{1,0:T(8,128)(2,1)} %bitcast.39), custom_call_target="tpu_custom_call" | custom-call | flops 655360 | bytes 7864320 | tf_op jit(solution)/shard_map/pack/pallas_call | solution.py:274
  175.1 1.9 collective-permute-start.2
  177.0 1.9 collective-permute-start.3
  178.9 2.9 collective-permute-start.4
  181.8 1.9 collective-permute-start.5
  183.8 0.0 all-to-all-done.1.dispatched
  183.8 1.6 spread.1
  185.4 0.0 copy-start.1
  185.4 6.5 %all-to-all-start.2 = ((bf16[16,512,128]{2,1,0:T(8,128)(2,1)}), bf16[16,512,128]{2,1,0:T(8,128)(2,1)S(1)}, u32[]{:S(2)}, u32[]{:S(2)}) async-start(bf16[16,512,128]{2,1,0:T(8,128)(2,1)} %spread.1), calls=%async_computation.2 | async-start | bytes 4194304 | tf_op jit(solution)/shard_map/all_to_all | solution.py:251
  192.0 0.5 collective-permute-done.2.got_0
  192.5 0.0 copy-start.2
  192.5 2.3 collective-permute-start.6
  194.8 0.0 collective-permute-done.3.got_1
  194.8 2.2 collective-permute-start.7
  197.0 0.2 collective-permute-done.4.got_2
  197.2 2.3 collective-permute-start.8
  199.5 8.1 %collective-permute-done.5.got_3 = bf16[240,2048]{1,0:T(8,128)(2,1)} collective-permute-done((bf16[240,2048]{1,0:T(8,128)(2,1)}, bf16[240,2048]{1,0:T(8,128)(2,1)}, u32[]{:S(2)}, u32[]{:S(2)}) %collective-permute-start.5) | collective-permute-done | bytes 983072 | tf_op jit(solution)/shard_map/ppermute | solution.py:473
  207.5 2.3 collective-permute-start.9
  209.8 0.0 collective-permute-done.6.fwd_0
  209.8 0.0 collective-permute-done.7.fwd_1
  209.8 0.0 collective-permute-done.8.fwd_2
  209.8 1.5 collective-permute-done.9.fwd_3
  211.3 13.0 %all-to-all-done.2.gathered = bf16[16,512,128]{2,1,0:T(8,128)(2,1)S(1)} async-done(((bf16[16,512,128]{2,1,0:T(8,128)(2,1)}), bf16[16,512,128]{2,1,0:T(8,128)(2,1)S(1)}, u32[]{:S(2)}, u32[]{:S(2)}) %all-to-all-start.2) | async-done | bytes 2097184 | tf_op jit(solution)/shard_map/all_to_all | solution.py:251
  224.4 0.0 copy-done.2
  224.4 0.0 copy-done.1
  224.4 8.3 %expert.1 = bf16[16,528,128]{2,1,0:T(8,128)(2,1)S(1)} custom-call(s32[1]{0:T(128)} %bitcast.serves, bf16[16,512,128]{2,1,0:T(8,128)(2,1)S(1)} %all-to-all-done.2.gathered, bf16[256,128]{1,0:T(8,128)(2,1)S(1)} %get-tuple-element.26.own, f32[1,2048]{1,0:T(1,128)S(1)} %bitcast.34, bf16[320,2048]{1,0:T(8,128)(2,1)} %bitcast.36, bf16[320,2048]{1,0:T(8,128)(2,1)} %bitcast.38, ...), custom_call_target="tpu_custom_call" | custom-call | flops 4026531840 | bytes 12058624 | tf_op jit(solution)/shard_map/expert/pallas_call | solution.py:377
  232.7 32.3 %all_to_all.26.shares = bf16[16,528,128]{2,1,0:T(8,128)(2,1)S(1)} all-to-all(bf16[16,528,128]{2,1,0:T(8,128)(2,1)S(1)} %expert.1), channel_id=1, replica_groups=mesh['sp'=32,'tp'=16] {'tp'}, dimensions={0} | all-to-all | bytes 4325376 | tf_op jit(solution)/shard_map/all_to_all | solution.py:251
  265.0 0.0 copy-start.4
  265.0 0.0 copy-start.3
  265.0 1.3 shares.1
  266.3 12.0 %all-to-all-start.4 = ((bf16[16,64,128]{2,1,0:T(8,128)(2,1)}), bf16[16,64,128]{2,1,0:T(8,128)(2,1)S(1)}, u32[]{:S(2)}, u32[]{:S(2)}) async-start(bf16[16,64,128]{2,1,0:T(8,128)(2,1)} %shares.1), calls=%async_computation.4 | async-start | bytes 524288 | tf_op jit(solution)/shard_map/all_to_all | solution.py:251
  278.3 0.1 copy.16
  278.4 0.0 copy-done.4
  278.4 0.1 iota_compare_fusion
  278.5 17.3 %all-to-all-done.4 = bf16[16,64,128]{2,1,0:T(8,128)(2,1)S(1)} async-done(((bf16[16,64,128]{2,1,0:T(8,128)(2,1)}), bf16[16,64,128]{2,1,0:T(8,128)(2,1)S(1)}, u32[]{:S(2)}, u32[]{:S(2)}) %all-to-all-start.4) | async-done | bytes 262176 | tf_op jit(solution)/shard_map/all_to_all | solution.py:251
  295.8 0.1 reshape.22
  295.9 0.2 convolution_multiply_fusion.1
  296.1 0.0 copy-done.3
  296.1 0.8 fusion.2
  (2 shorter events, 0.0 us)
Async XLA Ops:
  0.0 37.3 %copy-start = (bf16[2048,128]{1,0:T(8,128)(2,1)S(1)}, bf16[2048,128]{1,0:T(8,128)(2,1)}, u32[]{:S(2)}) copy-start(bf16[2048,128]{1,0:T(8,128)(2,1)} %weight.1) | copy-start | bytes 1572868
  1.4 5.7 %collective-permute-start = (bf16[128,128]{1,0:T(8,128)(2,1)S(1)}, bf16[128,128]{1,0:T(8,128)(2,1)S(1)}, u32[]{:S(2)}, u32[]{:S(2)}) collective-permute-start(bf16[128,128]{1,0:T(8,128)(2,1)S(1)} %get-tuple-element.20), channel_id=1, source_target_pairs={{0,16},{16,32},{32,48},{48,64},{64,80},{80,96},{96,112},{112,128},... | collective-permute-start | bytes 98312 | tf_op jit(solution)/shard_map/ppermute | solution.py:481
  3.3 5.2 %collective-permute-start.1 = (bf16[128,128]{1,0:T(8,128)(2,1)S(1)}, bf16[128,128]{1,0:T(8,128)(2,1)S(1)}, u32[]{:S(2)}, u32[]{:S(2)}) collective-permute-start(bf16[128,128]{1,0:T(8,128)(2,1)S(1)} %get-tuple-element.22), channel_id=1, source_target_pairs={{16,0},{32,16},{48,32},{64,48},{80,64},{96,80},{112,96},{128,112},... | collective-permute-start | bytes 98312 | tf_op jit(solution)/shard_map/ppermute | solution.py:482
  38.7 145.0 %all-to-all-start.1 = ((bf16[16,64,128]{2,1,0:T(8,128)(2,1)}), bf16[16,64,128]{2,1,0:T(8,128)(2,1)S(1)}, u32[]{:S(2)}, u32[]{:S(2)}) async-start(bf16[16,64,128]{2,1,0:T(8,128)(2,1)} %get-tuple-element.25), calls=%async_computation.1 | async-start | bytes 524288 | tf_op jit(solution)/shard_map/all_to_all | solution.py:251
  175.1 17.4 %collective-permute-start.2 = (bf16[240,2048]{1,0:T(8,128)(2,1)}, bf16[240,2048]{1,0:T(8,128)(2,1)S(1)}, u32[]{:S(2)}, u32[]{:S(2)}) collective-permute-start(bf16[240,2048]{1,0:T(8,128)(2,1)} %get-tuple-element.27), channel_id=1, source_target_pairs={{0,16},{1,2},{2,18},{3,0},{4,5},{5,21},{6,7},{7,23},{8,24},{9,10},... | collective-permute-start | bytes 2949128 | tf_op jit(solution)/shard_map/ppermute | solution.py:473
  177.0 17.8 %collective-permute-start.3 = (bf16[240,2048]{1,0:T(8,128)(2,1)}, bf16[240,2048]{1,0:T(8,128)(2,1)}, u32[]{:S(2)}, u32[]{:S(2)}) collective-permute-start(bf16[240,2048]{1,0:T(8,128)(2,1)} %get-tuple-element.28), channel_id=1, source_target_pairs={{0,16},{1,0},{2,18},{3,2},{4,7},{5,21},{6,5},{7,23},{8,24},{9,8},{... | collective-permute-start | bytes 2949128 | tf_op jit(solution)/shard_map/ppermute | solution.py:473
  178.9 18.3 %collective-permute-start.4 = (bf16[240,2048]{1,0:T(8,128)(2,1)}, bf16[240,2048]{1,0:T(8,128)(2,1)}, u32[]{:S(2)}, u32[]{:S(2)}) collective-permute-start(bf16[240,2048]{1,0:T(8,128)(2,1)} %get-tuple-element.29), channel_id=1, source_target_pairs={{0,16},{1,5},{2,18},{3,7},{4,8},{5,21},{6,10},{7,23},{8,24},{9,13}... | collective-permute-start | bytes 2949128 | tf_op jit(solution)/shard_map/ppermute | solution.py:473
  181.8 25.7 %collective-permute-start.5 = (bf16[240,2048]{1,0:T(8,128)(2,1)}, bf16[240,2048]{1,0:T(8,128)(2,1)}, u32[]{:S(2)}, u32[]{:S(2)}) collective-permute-start(bf16[240,2048]{1,0:T(8,128)(2,1)} %get-tuple-element.30), channel_id=1, source_target_pairs={{0,16},{1,13},{2,18},{3,15},{4,0},{5,21},{6,2},{7,23},{8,24},{9,5}... | collective-permute-start | bytes 2949128 | tf_op jit(solution)/shard_map/ppermute | solution.py:473
  185.4 39.0 %copy-start.1 = (f32[2048]{0:T(1024)S(1)}, f32[2048]{0:T(1024)}, u32[]{:S(2)}) copy-start(f32[2048]{0:T(1024)} %param.18) | copy-start | bytes 24580
  185.4 38.9 %all-to-all-start.2 = ((bf16[16,512,128]{2,1,0:T(8,128)(2,1)}), bf16[16,512,128]{2,1,0:T(8,128)(2,1)S(1)}, u32[]{:S(2)}, u32[]{:S(2)}) async-start(bf16[16,512,128]{2,1,0:T(8,128)(2,1)} %spread.1), calls=%async_computation.2 | async-start | bytes 4194304 | tf_op jit(solution)/shard_map/all_to_all | solution.py:251
  192.5 31.9 %copy-start.2 = (bf16[240,2048]{1,0:T(8,128)(2,1)}, bf16[240,2048]{1,0:T(8,128)(2,1)S(1)}, u32[]{:S(2)}) copy-start(bf16[240,2048]{1,0:T(8,128)(2,1)S(1)} %collective-permute-done.2.got_0) | copy-start | bytes 2949124
  192.5 17.3 %collective-permute-start.6 = (bf16[240,2048]{1,0:T(8,128)(2,1)S(1)}, bf16[240,2048]{1,0:T(8,128)(2,1)}, u32[]{:S(2)}, u32[]{:S(2)}) collective-permute-start(bf16[240,2048]{1,0:T(8,128)(2,1)S(1)} %collective-permute-done.2.got_0), channel_id=1, source_target_pairs={{0,16},{2,18},{5,21},{7,23},{8,24},{10,26},{13,29},{15,31},{17,1},... | collective-permute-start | bytes 2949128 | tf_op jit(solution)/shard_map/ppermute | solution.py:474
  194.8 15.0 %collective-permute-start.7 = (bf16[240,2048]{1,0:T(8,128)(2,1)}, bf16[240,2048]{1,0:T(8,128)(2,1)}, u32[]{:S(2)}, u32[]{:S(2)}) collective-permute-start(bf16[240,2048]{1,0:T(8,128)(2,1)} %collective-permute-done.3.got_1), channel_id=1, source_target_pairs={{0,16},{2,18},{5,21},{7,23},{8,24},{10,26},{13,29},{15,31},{17,1},... | collective-permute-start | bytes 2949128 | tf_op jit(solution)/shard_map/ppermute | solution.py:474
  197.2 12.6 %collective-permute-start.8 = (bf16[240,2048]{1,0:T(8,128)(2,1)}, bf16[240,2048]{1,0:T(8,128)(2,1)}, u32[]{:S(2)}, u32[]{:S(2)}) collective-permute-start(bf16[240,2048]{1,0:T(8,128)(2,1)} %collective-permute-done.4.got_2), channel_id=1, source_target_pairs={{0,16},{2,18},{5,21},{7,23},{8,24},{10,26},{13,29},{15,31},{17,1},... | collective-permute-start | bytes 2949128 | tf_op jit(solution)/shard_map/ppermute | solution.py:474
  207.5 3.8 %collective-permute-start.9 = (bf16[240,2048]{1,0:T(8,128)(2,1)}, bf16[240,2048]{1,0:T(8,128)(2,1)}, u32[]{:S(2)}, u32[]{:S(2)}) collective-permute-start(bf16[240,2048]{1,0:T(8,128)(2,1)} %collective-permute-done.5.got_3), channel_id=1, source_target_pairs={{0,16},{2,18},{5,21},{7,23},{8,24},{10,26},{13,29},{15,31},{17,1},... | collective-permute-start | bytes 2949128 | tf_op jit(solution)/shard_map/ppermute | solution.py:474
  265.0 13.4 %copy-start.4 = (f32[16,2]{0,1:T(2,128)S(1)}, f32[16,2]{0,1:T(2,128)}, u32[]{:S(2)}) copy-start(f32[16,2]{0,1:T(2,128)} %param.20) | copy-start | bytes 388
  265.0 31.1 %copy-start.3 = (bf16[16,2048]{1,0:T(8,128)(2,1)S(1)}, bf16[16,2048]{1,0:T(8,128)(2,1)}, u32[]{:S(2)}) copy-start(bf16[16,2048]{1,0:T(8,128)(2,1)} %residual.1) | copy-start | bytes 196612
  266.3 29.5 %all-to-all-start.4 = ((bf16[16,64,128]{2,1,0:T(8,128)(2,1)}), bf16[16,64,128]{2,1,0:T(8,128)(2,1)S(1)}, u32[]{:S(2)}, u32[]{:S(2)}) async-start(bf16[16,64,128]{2,1,0:T(8,128)(2,1)} %shares.1), calls=%async_computation.4 | async-start | bytes 524288 | tf_op jit(solution)/shard_map/all_to_all | solution.py:251

commit v6 on v5

--- a/solution.py
+++ b/solution.py
@@ -273,14 +273,16 @@
     half, width = owned[0].shape
     return pl.pallas_call(
         pack_kernel,
-        out_shape=tuple(pltpu.HBM((3 * half // ways, width), jnp.bfloat16) for _ in range(ways)),
+        out_shape=tuple(
+            jax.ShapeDtypeStruct((3 * half // ways, width), jnp.bfloat16) for _ in range(ways)
+        ),
         in_specs=[ANYWHERE] * 3,
-        out_specs=(ANYWHERE,) * ways,
+        out_specs=(VMEM,) * ways,
         scratch_shapes=[pltpu.SemaphoreType.DMA((3 * ways,))],
         cost_estimate=pl.CostEstimate(
             flops=half * width, bytes_accessed=12 * half * width, transcendentals=0
         ),
-        compiler_params=pltpu.CompilerParams(vmem_limit_bytes=2 * 2**20),
+        compiler_params=pltpu.CompilerParams(vmem_limit_bytes=8 * 2**20),
         name="pack",
     )(*in_hbm(owned))
 

time: 298 us -> 182 us (0.61)
  Pallas kernels: 137 us -> 20.5 us
  waiting for transfers between devices: 42.1 us -> 46.8 us
  starting transfers between devices: 57.8 us -> 54 us
    pallas_call x1, Pallas kernels: 120 us -> 3.77 us  [pack(): pl.pallas_call(pack_kernel, out_shape=tuple((jax.ShapeDtypeStruct((3 * ha...]
    all_to_all x3, waiting for transfers between devices: 30.3 us -> 39.7 us  [exchange(): lax.all_to_all(value, axis, split_axis=0, concat_axis=0, tiled=True, axis...]
    ppermute x4, waiting for transfers between devices: 8.77 us -> 3.37 us  [local(): received.append(lax.ppermute(packed[k], ('sp', 'tp'), way))]
  transfers between devices with their start and end apart: 13 -> 13, of which waited for: 7 -> 6; matrix products, arithmetic and copies ran while one was open for 0% -> 0% of each run, Pallas kernels for 41% -> 3%
where the time goes in v6:
time: 182 us; the launch traced here: 181 us
  blocking collectives  58 us (32%)
  starting transfers between devices  54 us (30%)
  waiting for transfers between devices  46.8 us (26%)
  Pallas kernels  20.5 us (11%)
    all_to_all x2, blocking collectives, exchange(): lax.all_to_all(value, axis, split_axis=0, concat_axis=0, tiled=True, axis...  58 us
    all_to_all x3, waiting for transfers between devices, exchange(): lax.all_to_all(value, axis, split_axis=0, concat_axis=0, tiled=True, axis...  39.7 us
    all_to_all x3, starting transfers between devices, exchange(): lax.all_to_all(value, axis, split_axis=0, concat_axis=0, tiled=True, axis...  31.6 us
    ppermute x4, starting transfers between devices, local(): received.append(lax.ppermute(packed[k], ('sp', 'tp'), way))  8.66 us
    pallas_call x1, Pallas kernels, run_expert(): pl.pallas_call(expert_kernel, out_shape=jax.ShapeDtypeStruct((members, ro...  8.31 us
    ppermute x4, starting transfers between devices, local(): forwarded.append(lax.ppermute(received[-1], ('sp', 'tp'), passes))  8.18 us
    pallas_call x1, Pallas kernels, pack(): pl.pallas_call(pack_kernel, out_shape=tuple((jax.ShapeDtypeStruct((3 * ha...  3.77 us
    ppermute x1, starting transfers between devices, local(): high = lax.ppermute(high, 'sp', backward)  3.64 us
  transfers between devices with their start and end apart: 13, of which 6 were waited for; matrix products, arithmetic and copies ran while one was open for 0% of the time, Pallas kernels for 3%

profile of v6, /device:TPU:32, one launch (start us, length us, event | category | flops | bytes accessed | tf_op | source)
XLA Modules:
  0.0 180.9 jit_solution(11713998883721846233)
XLA Ops:
  0.0 0.0 copy-start
  0.0 1.4 prepare.1
  1.4 1.9 %collective-permute-start = (bf16[128,128]{1,0:T(8,128)(2,1)S(1)}, bf16[128,128]{1,0:T(8,128)(2,1)S(1)}, u32[]{:S(2)}, u32[]{:S(2)}) collective-permute-start(bf16[128,128]{1,0:T(8,128)(2,1)S(1)} %get-tuple-element.20), channel_id=1, source_target_pairs={{0,16},{16,32},{32,48},{48,64},{64,80},{80,96},{96,112},{112,128},... | collective-permute-start | bytes 98312 | tf_op jit(solution)/shard_map/ppermute | solution.py:483
  3.3 3.6 %collective-permute-start.1 = (bf16[128,128]{1,0:T(8,128)(2,1)S(1)}, bf16[128,128]{1,0:T(8,128)(2,1)S(1)}, u32[]{:S(2)}, u32[]{:S(2)}) collective-permute-start(bf16[128,128]{1,0:T(8,128)(2,1)S(1)} %get-tuple-element.22), channel_id=1, source_target_pairs={{16,0},{32,16},{48,32},{64,48},{80,64},{96,80},{112,96},{128,112},... | collective-permute-start | bytes 98312 | tf_op jit(solution)/shard_map/ppermute | solution.py:484
  7.0 0.1 pad_add_fusion.place
  7.0 0.0 collective-permute-done.low
  7.0 1.5 collective-permute-done.1.high
  8.5 2.7 %attend.1 = bf16[16,288,128]{2,1,0:T(8,128)(2,1)S(1)} custom-call(s32[2]{0:T(128)S(1)} %pad_add_fusion.place, f32[1,2]{1,0:T(1,128)S(1)} %get-tuple-element.18.sink, bf16[256,128]{1,0:T(8,128)(2,1)S(1)} %get-tuple-element.19.queries, bf16[128,128]{1,0:T(8,128)(2,1)S(1)} %collective-permute-done.low, bf16[128,256]{1,0:T(8,128)(2,1)S(1)} %get-tuple-element.21.own, ...), custom_call_target="tpu_custom_call" | custom-call | flops 50331648 | bytes 2097152 | tf_op jit(solution)/shard_map/attend/pallas_call | solution.py:136
  11.2 26.1 %all_to_all.25.arrived = bf16[16,288,128]{2,1,0:T(8,128)(2,1)S(1)} all-to-all(bf16[16,288,128]{2,1,0:T(8,128)(2,1)S(1)} %attend.1), channel_id=1, replica_groups=mesh['sp'=32,'tp'=16] {'tp'}, dimensions={0} | all-to-all | bytes 2359296 | tf_op jit(solution)/shard_map/all_to_all | solution.py:251
  37.3 0.0 copy-done
  37.3 1.4 project.1
  38.7 16.0 %all-to-all-start.1 = ((bf16[16,64,128]{2,1,0:T(8,128)(2,1)}), bf16[16,64,128]{2,1,0:T(8,128)(2,1)S(1)}, u32[]{:S(2)}, u32[]{:S(2)}) async-start(bf16[16,64,128]{2,1,0:T(8,128)(2,1)} %get-tuple-element.25), calls=%async_computation.1 | async-start | bytes 524288 | tf_op jit(solution)/shard_map/all_to_all | solution.py:251
  54.7 3.8 %pack.1 = (bf16[240,2048]{1,0:T(8,128)(2,1)}, bf16[240,2048]{1,0:T(8,128)(2,1)}, bf16[240,2048]{1,0:T(8,128)(2,1)}, bf16[240,2048]{1,0:T(8,128)(2,1)S(1)}) custom-call(bf16[320,2048]{1,0:T(8,128)(2,1)} %bitcast.35, bf16[320,2048]{1,0:T(8,128)(2,1)} %bitcast.37, bf16[320,2048]{1,0:T(8,128)(2,1)} %bitcast.39), custom_call_target="tpu_custom_call" | custom-call | flops 655360 | bytes 7864320 | tf_op jit(solution)/shard_map/pack/pallas_call | solution.py:274
  58.5 1.9 %collective-permute-start.2 = (bf16[240,2048]{1,0:T(8,128)(2,1)}, bf16[240,2048]{1,0:T(8,128)(2,1)}, u32[]{:S(2)}, u32[]{:S(2)}) collective-permute-start(bf16[240,2048]{1,0:T(8,128)(2,1)} %get-tuple-element.27), channel_id=1, source_target_pairs={{0,16},{1,2},{2,18},{3,0},{4,5},{5,21},{6,7},{7,23},{8,24},{9,10},... | collective-permute-start | bytes 2949128 | tf_op jit(solution)/shard_map/ppermute | solution.py:475
  60.4 1.9 %collective-permute-start.3 = (bf16[240,2048]{1,0:T(8,128)(2,1)}, bf16[240,2048]{1,0:T(8,128)(2,1)}, u32[]{:S(2)}, u32[]{:S(2)}) collective-permute-start(bf16[240,2048]{1,0:T(8,128)(2,1)} %get-tuple-element.28), channel_id=1, source_target_pairs={{0,16},{1,0},{2,18},{3,2},{4,7},{5,21},{6,5},{7,23},{8,24},{9,8},{... | collective-permute-start | bytes 2949128 | tf_op jit(solution)/shard_map/ppermute | solution.py:475
  62.4 2.9 %collective-permute-start.4 = (bf16[240,2048]{1,0:T(8,128)(2,1)}, bf16[240,2048]{1,0:T(8,128)(2,1)}, u32[]{:S(2)}, u32[]{:S(2)}) collective-permute-start(bf16[240,2048]{1,0:T(8,128)(2,1)} %get-tuple-element.29), channel_id=1, source_target_pairs={{0,16},{1,5},{2,18},{3,7},{4,8},{5,21},{6,10},{7,23},{8,24},{9,13}... | collective-permute-start | bytes 2949128 | tf_op jit(solution)/shard_map/ppermute | solution.py:475
  65.3 1.9 %collective-permute-start.5 = (bf16[240,2048]{1,0:T(8,128)(2,1)S(1)}, bf16[240,2048]{1,0:T(8,128)(2,1)}, u32[]{:S(2)}, u32[]{:S(2)}) collective-permute-start(bf16[240,2048]{1,0:T(8,128)(2,1)S(1)} %get-tuple-element.30), channel_id=1, source_target_pairs={{0,16},{1,13},{2,18},{3,15},{4,0},{5,21},{6,2},{7,23},{8,24},{9,5}... | collective-permute-start | bytes 2949128 | tf_op jit(solution)/shard_map/ppermute | solution.py:475
  67.2 5.1 %all-to-all-done.1.dispatched = bf16[16,64,128]{2,1,0:T(8,128)(2,1)S(1)} async-done(((bf16[16,64,128]{2,1,0:T(8,128)(2,1)}), bf16[16,64,128]{2,1,0:T(8,128)(2,1)S(1)}, u32[]{:S(2)}, u32[]{:S(2)}) %all-to-all-start.1) | async-done | bytes 262176 | tf_op jit(solution)/shard_map/all_to_all | solution.py:251
  72.2 1.6 spread.1
  73.9 0.0 copy-start.1
  73.9 3.7 %all-to-all-start.2 = ((bf16[16,512,128]{2,1,0:T(8,128)(2,1)}), bf16[16,512,128]{2,1,0:T(8,128)(2,1)S(1)}, u32[]{:S(2)}, u32[]{:S(2)}) async-start(bf16[16,512,128]{2,1,0:T(8,128)(2,1)} %spread.1), calls=%async_computation.2 | async-start | bytes 4194304 | tf_op jit(solution)/shard_map/all_to_all | solution.py:251
  77.6 0.0 collective-permute-done.2.got_0
  77.7 2.3 %collective-permute-start.6 = (bf16[240,2048]{1,0:T(8,128)(2,1)}, bf16[240,2048]{1,0:T(8,128)(2,1)}, u32[]{:S(2)}, u32[]{:S(2)}) collective-permute-start(bf16[240,2048]{1,0:T(8,128)(2,1)} %collective-permute-done.2.got_0), channel_id=1, source_target_pairs={{0,16},{2,18},{5,21},{7,23},{8,24},{10,26},{13,29},{15,31},{17,1},... | collective-permute-start | bytes 2949128 | tf_op jit(solution)/shard_map/ppermute | solution.py:476
  79.9 0.0 collective-permute-done.3.got_1
  79.9 2.3 %collective-permute-start.7 = (bf16[240,2048]{1,0:T(8,128)(2,1)}, bf16[240,2048]{1,0:T(8,128)(2,1)}, u32[]{:S(2)}, u32[]{:S(2)}) collective-permute-start(bf16[240,2048]{1,0:T(8,128)(2,1)} %collective-permute-done.3.got_1), channel_id=1, source_target_pairs={{0,16},{2,18},{5,21},{7,23},{8,24},{10,26},{13,29},{15,31},{17,1},... | collective-permute-start | bytes 2949128 | tf_op jit(solution)/shard_map/ppermute | solution.py:476
  82.2 0.0 collective-permute-done.4.got_2
  82.2 2.3 %collective-permute-start.8 = (bf16[240,2048]{1,0:T(8,128)(2,1)}, bf16[240,2048]{1,0:T(8,128)(2,1)}, u32[]{:S(2)}, u32[]{:S(2)}) collective-permute-start(bf16[240,2048]{1,0:T(8,128)(2,1)} %collective-permute-done.4.got_2), channel_id=1, source_target_pairs={{0,16},{2,18},{5,21},{7,23},{8,24},{10,26},{13,29},{15,31},{17,1},... | collective-permute-start | bytes 2949128 | tf_op jit(solution)/shard_map/ppermute | solution.py:476
  84.5 3.4 %collective-permute-done.5.got_3 = bf16[240,2048]{1,0:T(8,128)(2,1)} collective-permute-done((bf16[240,2048]{1,0:T(8,128)(2,1)S(1)}, bf16[240,2048]{1,0:T(8,128)(2,1)}, u32[]{:S(2)}, u32[]{:S(2)}) %collective-permute-start.5) | collective-permute-done | bytes 983072 | tf_op jit(solution)/shard_map/ppermute | solution.py:475
  87.9 1.3 collective-permute-start.9
  89.3 0.0 collective-permute-done.6.fwd_0
  89.3 0.0 collective-permute-done.7.fwd_1
  89.3 0.0 collective-permute-done.8.fwd_2
  89.3 2.3 %collective-permute-done.9.fwd_3 = bf16[240,2048]{1,0:T(8,128)(2,1)S(1)} collective-permute-done((bf16[240,2048]{1,0:T(8,128)(2,1)}, bf16[240,2048]{1,0:T(8,128)(2,1)S(1)}, u32[]{:S(2)}, u32[]{:S(2)}) %collective-permute-start.9) | collective-permute-done | bytes 983072 | tf_op jit(solution)/shard_map/ppermute | solution.py:476
  91.5 0.0 copy-start.2
  91.5 17.2 %all-to-all-done.2.gathered = bf16[16,512,128]{2,1,0:T(8,128)(2,1)S(1)} async-done(((bf16[16,512,128]{2,1,0:T(8,128)(2,1)}), bf16[16,512,128]{2,1,0:T(8,128)(2,1)S(1)}, u32[]{:S(2)}, u32[]{:S(2)}) %all-to-all-start.2) | async-done | bytes 2097184 | tf_op jit(solution)/shard_map/all_to_all | solution.py:251
  108.7 0.0 copy-done.2
  108.7 0.0 copy-done.1
  108.7 8.3 %expert.1 = bf16[16,528,128]{2,1,0:T(8,128)(2,1)S(1)} custom-call(s32[1]{0:T(128)} %bitcast.serves, bf16[16,512,128]{2,1,0:T(8,128)(2,1)S(1)} %all-to-all-done.2.gathered, bf16[256,128]{1,0:T(8,128)(2,1)S(1)} %get-tuple-element.26.own, f32[1,2048]{1,0:T(1,128)S(1)} %bitcast.34, bf16[320,2048]{1,0:T(8,128)(2,1)} %bitcast.36, bf16[320,2048]{1,0:T(8,128)(2,1)} %bitcast.38, ...), custom_call_target="tpu_custom_call" | custom-call | flops 4026531840 | bytes 12058624 | tf_op jit(solution)/shard_map/expert/pallas_call | solution.py:379
  117.0 32.0 %all_to_all.26.shares = bf16[16,528,128]{2,1,0:T(8,128)(2,1)S(1)} all-to-all(bf16[16,528,128]{2,1,0:T(8,128)(2,1)S(1)} %expert.1), channel_id=1, replica_groups=mesh['sp'=32,'tp'=16] {'tp'}, dimensions={0} | all-to-all | bytes 4325376 | tf_op jit(solution)/shard_map/all_to_all | solution.py:251
  149.0 0.0 copy-start.4
  149.0 0.0 copy-start.3
  149.0 1.3 shares.1
  150.3 11.9 %all-to-all-start.4 = ((bf16[16,64,128]{2,1,0:T(8,128)(2,1)}), bf16[16,64,128]{2,1,0:T(8,128)(2,1)S(1)}, u32[]{:S(2)}, u32[]{:S(2)}) async-start(bf16[16,64,128]{2,1,0:T(8,128)(2,1)} %shares.1), calls=%async_computation.4 | async-start | bytes 524288 | tf_op jit(solution)/shard_map/all_to_all | solution.py:251
  162.2 0.1 copy.16
  162.3 0.0 copy-done.4
  162.3 0.1 iota_compare_fusion
  162.4 17.5 %all-to-all-done.4 = bf16[16,64,128]{2,1,0:T(8,128)(2,1)S(1)} async-done(((bf16[16,64,128]{2,1,0:T(8,128)(2,1)}), bf16[16,64,128]{2,1,0:T(8,128)(2,1)S(1)}, u32[]{:S(2)}, u32[]{:S(2)}) %all-to-all-start.4) | async-done | bytes 262176 | tf_op jit(solution)/shard_map/all_to_all | solution.py:251
  179.9 0.1 reshape.22
  180.0 0.2 convolution_multiply_fusion.1
  180.1 0.0 copy-done.3
  180.1 0.8 fusion.2
  (2 shorter events, 0.0 us)
Async XLA Ops:
  0.0 37.3 %copy-start = (bf16[2048,128]{1,0:T(8,128)(2,1)S(1)}, bf16[2048,128]{1,0:T(8,128)(2,1)}, u32[]{:S(2)}) copy-start(bf16[2048,128]{1,0:T(8,128)(2,1)} %weight.1) | copy-start | bytes 1572868
  1.4 5.7 %collective-permute-start = (bf16[128,128]{1,0:T(8,128)(2,1)S(1)}, bf16[128,128]{1,0:T(8,128)(2,1)S(1)}, u32[]{:S(2)}, u32[]{:S(2)}) collective-permute-start(bf16[128,128]{1,0:T(8,128)(2,1)S(1)} %get-tuple-element.20), channel_id=1, source_target_pairs={{0,16},{16,32},{32,48},{48,64},{64,80},{80,96},{96,112},{112,128},... | collective-permute-start | bytes 98312 | tf_op jit(solution)/shard_map/ppermute | solution.py:483
  3.3 5.2 %collective-permute-start.1 = (bf16[128,128]{1,0:T(8,128)(2,1)S(1)}, bf16[128,128]{1,0:T(8,128)(2,1)S(1)}, u32[]{:S(2)}, u32[]{:S(2)}) collective-permute-start(bf16[128,128]{1,0:T(8,128)(2,1)S(1)} %get-tuple-element.22), channel_id=1, source_target_pairs={{16,0},{32,16},{48,32},{64,48},{80,64},{96,80},{112,96},{128,112},... | collective-permute-start | bytes 98312 | tf_op jit(solution)/shard_map/ppermute | solution.py:484
  38.7 33.5 %all-to-all-start.1 = ((bf16[16,64,128]{2,1,0:T(8,128)(2,1)}), bf16[16,64,128]{2,1,0:T(8,128)(2,1)S(1)}, u32[]{:S(2)}, u32[]{:S(2)}) async-start(bf16[16,64,128]{2,1,0:T(8,128)(2,1)} %get-tuple-element.25), calls=%async_computation.1 | async-start | bytes 524288 | tf_op jit(solution)/shard_map/all_to_all | solution.py:251
  58.5 19.2 %collective-permute-start.2 = (bf16[240,2048]{1,0:T(8,128)(2,1)}, bf16[240,2048]{1,0:T(8,128)(2,1)}, u32[]{:S(2)}, u32[]{:S(2)}) collective-permute-start(bf16[240,2048]{1,0:T(8,128)(2,1)} %get-tuple-element.27), channel_id=1, source_target_pairs={{0,16},{1,2},{2,18},{3,0},{4,5},{5,21},{6,7},{7,23},{8,24},{9,10},... | collective-permute-start | bytes 2949128 | tf_op jit(solution)/shard_map/ppermute | solution.py:475
  60.4 19.5 %collective-permute-start.3 = (bf16[240,2048]{1,0:T(8,128)(2,1)}, bf16[240,2048]{1,0:T(8,128)(2,1)}, u32[]{:S(2)}, u32[]{:S(2)}) collective-permute-start(bf16[240,2048]{1,0:T(8,128)(2,1)} %get-tuple-element.28), channel_id=1, source_target_pairs={{0,16},{1,0},{2,18},{3,2},{4,7},{5,21},{6,5},{7,23},{8,24},{9,8},{... | collective-permute-start | bytes 2949128 | tf_op jit(solution)/shard_map/ppermute | solution.py:475
  62.4 19.9 %collective-permute-start.4 = (bf16[240,2048]{1,0:T(8,128)(2,1)}, bf16[240,2048]{1,0:T(8,128)(2,1)}, u32[]{:S(2)}, u32[]{:S(2)}) collective-permute-start(bf16[240,2048]{1,0:T(8,128)(2,1)} %get-tuple-element.29), channel_id=1, source_target_pairs={{0,16},{1,5},{2,18},{3,7},{4,8},{5,21},{6,10},{7,23},{8,24},{9,13}... | collective-permute-start | bytes 2949128 | tf_op jit(solution)/shard_map/ppermute | solution.py:475
  65.3 22.6 %collective-permute-start.5 = (bf16[240,2048]{1,0:T(8,128)(2,1)S(1)}, bf16[240,2048]{1,0:T(8,128)(2,1)}, u32[]{:S(2)}, u32[]{:S(2)}) collective-permute-start(bf16[240,2048]{1,0:T(8,128)(2,1)S(1)} %get-tuple-element.30), channel_id=1, source_target_pairs={{0,16},{1,13},{2,18},{3,15},{4,0},{5,21},{6,2},{7,23},{8,24},{9,5}... | collective-permute-start | bytes 2949128 | tf_op jit(solution)/shard_map/ppermute | solution.py:475
  73.9 34.8 %copy-start.1 = (f32[2048]{0:T(1024)S(1)}, f32[2048]{0:T(1024)}, u32[]{:S(2)}) copy-start(f32[2048]{0:T(1024)} %param.18) | copy-start | bytes 24580
  73.9 34.8 %all-to-all-start.2 = ((bf16[16,512,128]{2,1,0:T(8,128)(2,1)}), bf16[16,512,128]{2,1,0:T(8,128)(2,1)S(1)}, u32[]{:S(2)}, u32[]{:S(2)}) async-start(bf16[16,512,128]{2,1,0:T(8,128)(2,1)} %spread.1), calls=%async_computation.2 | async-start | bytes 4194304 | tf_op jit(solution)/shard_map/all_to_all | solution.py:251
  77.7 11.6 %collective-permute-start.6 = (bf16[240,2048]{1,0:T(8,128)(2,1)}, bf16[240,2048]{1,0:T(8,128)(2,1)}, u32[]{:S(2)}, u32[]{:S(2)}) collective-permute-start(bf16[240,2048]{1,0:T(8,128)(2,1)} %collective-permute-done.2.got_0), channel_id=1, source_target_pairs={{0,16},{2,18},{5,21},{7,23},{8,24},{10,26},{13,29},{15,31},{17,1},... | collective-permute-start | bytes 2949128 | tf_op jit(solution)/shard_map/ppermute | solution.py:476
  79.9 9.3 %collective-permute-start.7 = (bf16[240,2048]{1,0:T(8,128)(2,1)}, bf16[240,2048]{1,0:T(8,128)(2,1)}, u32[]{:S(2)}, u32[]{:S(2)}) collective-permute-start(bf16[240,2048]{1,0:T(8,128)(2,1)} %collective-permute-done.3.got_1), channel_id=1, source_target_pairs={{0,16},{2,18},{5,21},{7,23},{8,24},{10,26},{13,29},{15,31},{17,1},... | collective-permute-start | bytes 2949128 | tf_op jit(solution)/shard_map/ppermute | solution.py:476
  82.2 7.0 %collective-permute-start.8 = (bf16[240,2048]{1,0:T(8,128)(2,1)}, bf16[240,2048]{1,0:T(8,128)(2,1)}, u32[]{:S(2)}, u32[]{:S(2)}) collective-permute-start(bf16[240,2048]{1,0:T(8,128)(2,1)} %collective-permute-done.4.got_2), channel_id=1, source_target_pairs={{0,16},{2,18},{5,21},{7,23},{8,24},{10,26},{13,29},{15,31},{17,1},... | collective-permute-start | bytes 2949128 | tf_op jit(solution)/shard_map/ppermute | solution.py:476
  87.9 3.7 %collective-permute-start.9 = (bf16[240,2048]{1,0:T(8,128)(2,1)}, bf16[240,2048]{1,0:T(8,128)(2,1)S(1)}, u32[]{:S(2)}, u32[]{:S(2)}) collective-permute-start(bf16[240,2048]{1,0:T(8,128)(2,1)} %collective-permute-done.5.got_3), channel_id=1, source_target_pairs={{0,16},{2,18},{5,21},{7,23},{8,24},{10,26},{13,29},{15,31},{17,1},... | collective-permute-start | bytes 2949128 | tf_op jit(solution)/shard_map/ppermute | solution.py:476
  91.5 17.2 %copy-start.2 = (bf16[240,2048]{1,0:T(8,128)(2,1)}, bf16[240,2048]{1,0:T(8,128)(2,1)S(1)}, u32[]{:S(2)}) copy-start(bf16[240,2048]{1,0:T(8,128)(2,1)S(1)} %collective-permute-done.9.fwd_3) | copy-start | bytes 2949124
  149.0 13.3 %copy-start.4 = (f32[16,2]{0,1:T(2,128)S(1)}, f32[16,2]{0,1:T(2,128)}, u32[]{:S(2)}) copy-start(f32[16,2]{0,1:T(2,128)} %param.20) | copy-start | bytes 388
  149.0 31.1 %copy-start.3 = (bf16[16,2048]{1,0:T(8,128)(2,1)S(1)}, bf16[16,2048]{1,0:T(8,128)(2,1)}, u32[]{:S(2)}) copy-start(bf16[16,2048]{1,0:T(8,128)(2,1)} %residual.1) | copy-start | bytes 196612
  150.3 29.5 %all-to-all-start.4 = ((bf16[16,64,128]{2,1,0:T(8,128)(2,1)}), bf16[16,64,128]{2,1,0:T(8,128)(2,1)S(1)}, u32[]{:S(2)}, u32[]{:S(2)}) async-start(bf16[16,64,128]{2,1,0:T(8,128)(2,1)} %shares.1), calls=%async_computation.4 | async-start | bytes 524288 | tf_op jit(solution)/shard_map/all_to_all | solution.py:251

commit v7 on v6

--- a/solution.py
+++ b/solution.py
@@ -24,6 +24,10 @@
 
 def served_side(member):
     return (member + member // 4) % 2
+
+
+def served_rank(member):
+    return member // 4 % 2
 
 
 def prep_kernel(
@@ -211,13 +215,18 @@
     for plane in range(planes):
         rows[plane * lines : (plane + 1) * lines, :] = dispatched[plane].astype(jnp.float32)
     copies = [
-        pltpu.make_async_copy(block.at[served_side(t)], out.at[t], sems.at[t])
+        pltpu.make_async_copy(
+            block.at[served_side(t) * 2 + served_rank(t)], out.at[t], sems.at[t]
+        )
         for t in range(members)
     ]
     for side in range(2):
         for at in range(lines // 2):
             group = rows[pl.ds(side * (lines // 2) + at, planes, stride=lines), :]
-            block[side, at * planes : (at + 1) * planes, :] = group.astype(jnp.bfloat16)
+            token, rank = at // 2, at % 2
+            block[side * 2 + rank, token * planes : (token + 1) * planes, :] = group.astype(
+                jnp.bfloat16
+            )
         for t in range(members):
             if served_side(t) == side:
                 copies[t].start()
@@ -229,12 +238,12 @@
     planes, lines, lanes = dispatched.shape
     return pl.pallas_call(
         spread_kernel,
-        out_shape=pltpu.HBM((members, planes * lines // 2, lanes), jnp.bfloat16),
+        out_shape=pltpu.HBM((members, planes * lines // 4, lanes), jnp.bfloat16),
         in_specs=[VMEM],
         out_specs=ANYWHERE,
         scratch_shapes=[
             pltpu.VMEM((planes * lines, lanes), jnp.float32),
-            pltpu.VMEM((2, planes * lines // 2, lanes), jnp.bfloat16),
+            pltpu.VMEM((4, planes * lines // 4, lanes), jnp.bfloat16),
             pltpu.SemaphoreType.DMA((members,)),
         ],
         cost_estimate=pl.CostEstimate(
@@ -293,7 +302,7 @@
     out, gate, up, down, normed, sems,
 ):
     half, width = gate_own.shape
-    part = half // 4
+    part = half // 2
     pairs, rows, piece = gathered.shape
     members = out.shape[0]
     each = rows // members
@@ -311,16 +320,15 @@
     received = [
         placed(packed, k * part, 3 * k) for k, packed in enumerate((got_0, got_1, got_2, got_3))
     ]
-    forwarded = [
-        placed(packed, half + k * part, 12) for k, packed in enumerate((fwd_0, fwd_1, fwd_2, fwd_3))
-    ]
+    received += [placed(fwd_0, 4 * part, 12), placed(fwd_1, 5 * part, 15)]
+    forwarded = [placed(fwd_2, 6 * part, 18), placed(fwd_3, 7 * part, 18)]
     held = [
-        pltpu.make_async_copy(source, target.at[pl.ds(half, half)], sems.at[12 + i])
+        pltpu.make_async_copy(source, target.at[pl.ds(3 * half, half)], sems.at[18 + i])
         for i, (source, target) in enumerate(zip((gate_own, up_own, down_own), targets))
     ]
-    for i in range(3):
-        for copies in received:
-            copies[i].start()
+    for copies in received:
+        for copy in copies[:2]:
+            copy.start()
 
     @pl.when(serves[0] == 1)
     def _():
@@ -332,6 +340,9 @@
         for i in range(3):
             for copies in forwarded:
                 copies[i].start()
+
+    for copies in received:
+        copies[2].start()
 
     total = jnp.zeros((rows, 1), jnp.float32)
     for k in range(pairs):
@@ -344,12 +355,19 @@
         normed[:, k * piece : (k + 1) * piece] = scaled.astype(jnp.bfloat16)
     for t in range(members):
         out[t, each * tiles :, :] = own[t * 16 : (t + 1) * 16, :]
-    for i in range(2):
-        for copy in (*(copies[i] for copies in received), held[i]):
-            copy.wait()
     contract = (((1,), (1,)), ((), ()))
     hidden = []
-    for start, size in ((0, 256), (256, 256), (512, 128)):
+    arrived = 0
+    for start in range(0, 4 * half, 256):
+        size = 256
+        while arrived < 6 and arrived * part < start + size:
+            for copy in received[arrived][:2]:
+                copy.wait()
+            arrived += 1
+        if arrived == 6 and start + size > 6 * part:
+            for copy in held[:2]:
+                copy.wait()
+            arrived += 1
         g = lax.dot_general(
             normed[...], gate[pl.ds(start, size), :], contract, preferred_element_type=jnp.float32
         )
@@ -383,11 +401,11 @@
         ),
         in_specs=[SMEM, VMEM, VMEM, VMEM] + [ANYWHERE] * 11,
         out_specs=VMEM,
-        scratch_shapes=[pltpu.VMEM((2 * half, width), jnp.bfloat16) for _ in range(3)]
-        + [pltpu.VMEM((rows, width), jnp.bfloat16), pltpu.SemaphoreType.DMA((15,))],
+        scratch_shapes=[pltpu.VMEM((4 * half, width), jnp.bfloat16) for _ in range(3)]
+        + [pltpu.VMEM((rows, width), jnp.bfloat16), pltpu.SemaphoreType.DMA((21,))],
         cost_estimate=pl.CostEstimate(
-            flops=12 * rows * half * width,
-            bytes_accessed=12 * half * width + 4 * rows * width,
+            flops=24 * rows * half * width,
+            bytes_accessed=24 * half * width + 4 * rows * width,
             transcendentals=2 * rows * half,
         ),
         compiler_params=pltpu.CompilerParams(vmem_limit_bytes=28 * 2**20),
@@ -398,25 +416,23 @@
 def sum_kernel(shares, out, acc):
     members, rows, lanes = shares.shape
     planes = out.shape[0]
-    tiles = (rows - 16) // (2 * planes)
+    tiles = (rows - 16) // planes
     for side in range(2):
-        for block in range(2):
-            lo, size = block * (rows - 16) // 2, (rows - 16) // 2
-            total = jnp.zeros((size, lanes), jnp.float32)
+        for rank in range(2):
+            total = jnp.zeros((rows - 16, lanes), jnp.float32)
             for t in range(members):
-                if served_side(t) == side:
-                    total = total + shares[t, pl.ds(lo, size), :].astype(jnp.float32)
-            acc[pl.ds(lo, size), :] = total
-        for rank in range(2):
+                if served_side(t) == side and served_rank(t) == rank:
+                    total = total + shares[t, pl.ds(0, rows - 16), :].astype(jnp.float32)
+            acc[...] = total
             for plane in range(planes):
-                rows_of = acc[pl.ds(rank * planes + plane, tiles, stride=2 * planes), :]
+                rows_of = acc[pl.ds(plane, tiles, stride=planes), :]
                 at = (side * 2 + rank) * tiles
                 out[plane, at : at + tiles, :] = rows_of.astype(jnp.bfloat16)
 
 
 def sum_shares(shares, planes):
     members, rows, lanes = shares.shape
-    tiles = (rows - 16) // (2 * planes)
+    tiles = (rows - 16) // planes
     return pl.pallas_call(
         sum_kernel,
         out_shape=jax.ShapeDtypeStruct((planes, 4 * tiles, lanes), jnp.bfloat16),
@@ -452,28 +468,34 @@
     same_core = [[plane * 2 + core for plane in range(planes)] for core in range(2)]
 
     steps = ((0, 1), (0, 3), (1, 0), (3, 0))
-    moves, passes = [[] for _ in steps], []
+    diagonal = ((1, 1), (3, 3))
+    moves, passes = [[] for _ in steps], [[] for _ in steps]
     for plane in range(planes):
         for core in range(2):
             for member in range(n_tp):
-                source = (plane * 2 + core) * n_tp + member
-                across = (plane * 2 + 1 - core) * n_tp + member
-                if served_side(member) == core:
-                    for way in moves:
-                        way.append((source, across))
-                    passes.append((source, across))
-                else:
-                    for way, (dy, dx) in zip(moves, steps):
-                        other = (member // 4 + dy) % 4 * 4 + (member % 4 + dx) % 4
-                        way.append((source, source - member + other))
+                base = (plane * 2 + core) * n_tp
+                across = (plane * 2 + 1 - core) * n_tp
+                y, x = member // 4, member % 4
+                right = served_side(member) == core
+                for k, (dy, dx) in enumerate(steps):
+                    if right and k < 2:
+                        dy, dx = diagonal[k]
+                        target = across + (y + dy) % 4 * 4 + (x + dx) % 4
+                    elif right:
+                        target = across + member
+                    else:
+                        target = base + (y + dy) % 4 * 4 + (x + dx) % 4
+                    moves[k].append((base + member, target))
+                    if right or k < 2:
+                        passes[k].append((base + member, across + member))
     core_index = lax.axis_index("sp") % 2
     serves = (core_index == served_side(lax.axis_index("tp"))).astype(jnp.int32).reshape(1)
     owned = (gate_weight[0].T, up_weight[0].T, down_weight[0])
     received, forwarded = [], []
-    packed = pack(owned, len(steps))
+    packed = pack(owned, 2)
     for k, way in enumerate(moves):
-        received.append(lax.ppermute(packed[k], ("sp", "tp"), way))
-        forwarded.append(lax.ppermute(received[-1], ("sp", "tp"), passes))
+        received.append(lax.ppermute(packed[k % 2], ("sp", "tp"), way))
+        forwarded.append(lax.ppermute(received[-1], ("sp", "tp"), passes[k]))
 
     low, high, joined, asked, base, sinks, slot_rows = prepare(
         keys.T, values.T, queries, residual, sink_logit.reshape(1, -1), routes.T
@@ -494,7 +516,7 @@
     pieces = run_expert(serves, gathered, own, norm_gain, owned, (*received, *forwarded))
 
     shares = exchange(pieces, "tp")
-    own_rows = shares[:, 2 * n_tp * planes :].transpose(1, 0, 2).reshape(tok_rows, width)
+    own_rows = shares[:, n_tp * planes :].transpose(1, 0, 2).reshape(tok_rows, width)
     returning = sum_shares(shares, planes)
 
     returned = exchange(returning, "sp", same_core)

time: 182 us -> 186 us (1.022)
  starting transfers between devices: 54 us -> 56.9 us
  Pallas kernels: 20.5 us -> 18.6 us
    ppermute x8, starting transfers between devices: 16.8 us -> 22.7 us  [the longest x4 12.5 us: local(): received.append(lax.ppermute(packed[k % 2], ('sp', 'tp'), way))]
    ppermute x8, waiting for transfers between devices: 5.63 us -> 0.02 us  [the longest x4 0.01 us: local(): forwarded.append(lax.ppermute(received[-1], ('sp', 'tp'), passes[k]))]
    ppermute x1, waiting for transfers between devices: 0.01 us -> 4.9 us  [local(): low = lax.ppermute(low, 'sp', forward)]
    all_to_all x3, starting transfers between devices: 31.6 us -> 29.1 us  [exchange(): lax.all_to_all(value, axis, split_axis=0, concat_axis=0, tiled=True, axis...]
    all_to_all x3, waiting for transfers between devices: 39.7 us -> 42.2 us  [exchange(): lax.all_to_all(value, axis, split_axis=0, concat_axis=0, tiled=True, axis...]
  transfers between devices with their start and end apart: 13 -> 13, of which waited for: 6 -> 5; matrix products, arithmetic and copies ran while one was open for 0% -> 0% of each run, Pallas kernels for 3% -> 4%
where the time goes in v7:
time: 186 us; the launch traced here: 185 us
  blocking collectives  59.5 us (32%)
  starting transfers between devices  56.9 us (31%)
  waiting for transfers between devices  48.6 us (26%)
  Pallas kernels  18.6 us (10%)
    all_to_all x2, blocking collectives, exchange(): lax.all_to_all(value, axis, split_axis=0, concat_axis=0, tiled=True, axis...  59.5 us
    all_to_all x3, waiting for transfers between devices, exchange(): lax.all_to_all(value, axis, split_axis=0, concat_axis=0, tiled=True, axis...  42.2 us
    all_to_all x3, starting transfers between devices, exchange(): lax.all_to_all(value, axis, split_axis=0, concat_axis=0, tiled=True, axis...  29.1 us
    ppermute x4, starting transfers between devices, local(): received.append(lax.ppermute(packed[k % 2], ('sp', 'tp'), way))  12.5 us
    ppermute x4, starting transfers between devices, local(): forwarded.append(lax.ppermute(received[-1], ('sp', 'tp'), passes[k]))  10.2 us
    pallas_call x1, Pallas kernels, run_expert(): pl.pallas_call(expert_kernel, out_shape=jax.ShapeDtypeStruct((members, ro...  7.39 us
    ppermute x1, waiting for transfers between devices, local(): low = lax.ppermute(low, 'sp', forward)  4.9 us
  transfers between devices with their start and end apart: 13, of which 5 were waited for; matrix products, arithmetic and copies ran while one was open for 0% of the time, Pallas kernels for 4%

profile of v7, /device:TPU:32, one launch (start us, length us, event | category | flops | bytes accessed | tf_op | source)
XLA Modules:
  0.0 185.2 jit_solution(12894610868415536691)
XLA Ops:
  0.0 3.5 %pack.1 = (bf16[480,2048]{1,0:T(8,128)(2,1)}, bf16[480,2048]{1,0:T(8,128)(2,1)S(1)}) custom-call(bf16[320,2048]{1,0:T(8,128)(2,1)} %bitcast.35, bf16[320,2048]{1,0:T(8,128)(2,1)} %bitcast.37, bf16[320,2048]{1,0:T(8,128)(2,1)} %bitcast.39), custom_call_target="tpu_custom_call" | custom-call | flops 655360 | bytes 7864320 | tf_op jit(solution)/shard_map/pack/pallas_call | solution.py:283
  3.5 3.9 %collective-permute-start.2 = (bf16[480,2048]{1,0:T(8,128)(2,1)}, bf16[480,2048]{1,0:T(8,128)(2,1)}, u32[]{:S(2)}, u32[]{:S(2)}) collective-permute-start(bf16[480,2048]{1,0:T(8,128)(2,1)} %get-tuple-element.25), channel_id=1, source_target_pairs={{0,21},{1,2},{2,23},{3,0},{4,5},{5,26},{6,7},{7,24},{8,29},{9,10},... | collective-permute-start | bytes 5898248 | tf_op jit(solution)/shard_map/ppermute | solution.py:497
  7.3 4.8 %collective-permute-start.3 = (bf16[480,2048]{1,0:T(8,128)(2,1)S(1)}, bf16[480,2048]{1,0:T(8,128)(2,1)}, u32[]{:S(2)}, u32[]{:S(2)}) collective-permute-start(bf16[480,2048]{1,0:T(8,128)(2,1)S(1)} %get-tuple-element.26), channel_id=1, source_target_pairs={{0,31},{1,0},{2,29},{3,2},{4,7},{5,16},{6,5},{7,18},{8,23},{9,8},{... | collective-permute-start | bytes 5898248 | tf_op jit(solution)/shard_map/ppermute | solution.py:497
  12.2 1.9 %collective-permute-start.4 = (bf16[480,2048]{1,0:T(8,128)(2,1)}, bf16[480,2048]{1,0:T(8,128)(2,1)}, u32[]{:S(2)}, u32[]{:S(2)}) collective-permute-start(bf16[480,2048]{1,0:T(8,128)(2,1)} %get-tuple-element.25), channel_id=1, source_target_pairs={{0,16},{1,5},{2,18},{3,7},{4,8},{5,21},{6,10},{7,23},{8,24},{9,13}... | collective-permute-start | bytes 5898248 | tf_op jit(solution)/shard_map/ppermute | solution.py:497
  14.1 1.9 %collective-permute-start.5 = (bf16[480,2048]{1,0:T(8,128)(2,1)S(1)}, bf16[480,2048]{1,0:T(8,128)(2,1)}, u32[]{:S(2)}, u32[]{:S(2)}) collective-permute-start(bf16[480,2048]{1,0:T(8,128)(2,1)S(1)} %get-tuple-element.26), channel_id=1, source_target_pairs={{0,16},{1,13},{2,18},{3,15},{4,0},{5,21},{6,2},{7,23},{8,24},{9,5}... | collective-permute-start | bytes 5898248 | tf_op jit(solution)/shard_map/ppermute | solution.py:497
  16.0 0.0 copy-start
  16.0 1.4 prepare.1
  17.4 3.3 %collective-permute-start = (bf16[128,128]{1,0:T(8,128)(2,1)S(1)}, bf16[128,128]{1,0:T(8,128)(2,1)S(1)}, u32[]{:S(2)}, u32[]{:S(2)}) collective-permute-start(bf16[128,128]{1,0:T(8,128)(2,1)S(1)} %get-tuple-element.18), channel_id=1, source_target_pairs={{0,16},{16,32},{32,48},{48,64},{64,80},{80,96},{96,112},{112,128},... | collective-permute-start | bytes 98312 | tf_op jit(solution)/shard_map/ppermute | solution.py:505
  20.7 4.9 %collective-permute-done.low = bf16[128,128]{1,0:T(8,128)(2,1)S(1)} collective-permute-done((bf16[128,128]{1,0:T(8,128)(2,1)S(1)}, bf16[128,128]{1,0:T(8,128)(2,1)S(1)}, u32[]{:S(2)}, u32[]{:S(2)}) %collective-permute-start) | collective-permute-done | bytes 32800 | tf_op jit(solution)/shard_map/ppermute | solution.py:505
  25.6 1.9 %collective-permute-start.1 = (bf16[128,128]{1,0:T(8,128)(2,1)S(1)}, bf16[128,128]{1,0:T(8,128)(2,1)S(1)}, u32[]{:S(2)}, u32[]{:S(2)}) collective-permute-start(bf16[128,128]{1,0:T(8,128)(2,1)S(1)} %get-tuple-element.20), channel_id=1, source_target_pairs={{16,0},{32,16},{48,32},{64,48},{80,64},{96,80},{112,96},{128,112},... | collective-permute-start | bytes 98312 | tf_op jit(solution)/shard_map/ppermute | solution.py:506
  27.6 0.1 pad_add_fusion.place
  27.6 1.5 collective-permute-done.1.high
  29.1 2.7 %attend.1 = bf16[16,288,128]{2,1,0:T(8,128)(2,1)S(1)} custom-call(s32[2]{0:T(128)S(1)} %pad_add_fusion.place, f32[1,2]{1,0:T(1,128)S(1)} %get-tuple-element.16.sink, bf16[256,128]{1,0:T(8,128)(2,1)S(1)} %get-tuple-element.17.queries, bf16[128,128]{1,0:T(8,128)(2,1)S(1)} %collective-permute-done.low, bf16[128,256]{1,0:T(8,128)(2,1)S(1)} %get-tuple-element.19.own, ...), custom_call_target="tpu_custom_call" | custom-call | flops 50331648 | bytes 2097152 | tf_op jit(solution)/shard_map/attend/pallas_call | solution.py:140
  31.8 39.3 %all_to_all.25.arrived = bf16[16,288,128]{2,1,0:T(8,128)(2,1)S(1)} all-to-all(bf16[16,288,128]{2,1,0:T(8,128)(2,1)S(1)} %attend.1), channel_id=1, replica_groups=mesh['sp'=32,'tp'=16] {'tp'}, dimensions={0} | all-to-all | bytes 2359296 | tf_op jit(solution)/shard_map/all_to_all | solution.py:260
  71.1 0.0 copy-done
  71.1 1.4 project.1
  72.5 0.0 copy-start.1
  72.5 15.4 %all-to-all-start.1 = ((bf16[16,64,128]{2,1,0:T(8,128)(2,1)}), bf16[16,64,128]{2,1,0:T(8,128)(2,1)S(1)}, u32[]{:S(2)}, u32[]{:S(2)}) async-start(bf16[16,64,128]{2,1,0:T(8,128)(2,1)} %get-tuple-element.23), calls=%async_computation.1 | async-start | bytes 524288 | tf_op jit(solution)/shard_map/all_to_all | solution.py:260
  87.8 0.0 collective-permute-done.2.got_0
  87.8 1.9 %collective-permute-start.6 = (bf16[480,2048]{1,0:T(8,128)(2,1)}, bf16[480,2048]{1,0:T(8,128)(2,1)}, u32[]{:S(2)}, u32[]{:S(2)}) collective-permute-start(bf16[480,2048]{1,0:T(8,128)(2,1)} %collective-permute-done.2.got_0), channel_id=1, source_target_pairs={{0,16},{1,17},{2,18},{3,19},{4,20},{5,21},{6,22},{7,23},{8,24},{9,... | collective-permute-start | bytes 5898248 | tf_op jit(solution)/shard_map/ppermute | solution.py:498
  89.8 0.0 collective-permute-done.3.got_1
  89.8 2.4 %collective-permute-start.7 = (bf16[480,2048]{1,0:T(8,128)(2,1)}, bf16[480,2048]{1,0:T(8,128)(2,1)}, u32[]{:S(2)}, u32[]{:S(2)}) collective-permute-start(bf16[480,2048]{1,0:T(8,128)(2,1)} %collective-permute-done.3.got_1), channel_id=1, source_target_pairs={{0,16},{1,17},{2,18},{3,19},{4,20},{5,21},{6,22},{7,23},{8,24},{9,... | collective-permute-start | bytes 5898248 | tf_op jit(solution)/shard_map/ppermute | solution.py:498
  92.2 0.0 collective-permute-done.4.got_2
  92.2 3.3 %collective-permute-start.8 = (bf16[480,2048]{1,0:T(8,128)(2,1)}, bf16[480,2048]{1,0:T(8,128)(2,1)}, u32[]{:S(2)}, u32[]{:S(2)}) collective-permute-start(bf16[480,2048]{1,0:T(8,128)(2,1)} %collective-permute-done.4.got_2), channel_id=1, source_target_pairs={{0,16},{2,18},{5,21},{7,23},{8,24},{10,26},{13,29},{15,31},{17,1},... | collective-permute-start | bytes 5898248 | tf_op jit(solution)/shard_map/ppermute | solution.py:498
  95.5 0.0 collective-permute-done.5.got_3
  95.5 2.6 %collective-permute-start.9 = (bf16[480,2048]{1,0:T(8,128)(2,1)}, bf16[480,2048]{1,0:T(8,128)(2,1)}, u32[]{:S(2)}, u32[]{:S(2)}) collective-permute-start(bf16[480,2048]{1,0:T(8,128)(2,1)} %collective-permute-done.5.got_3), channel_id=1, source_target_pairs={{0,16},{2,18},{5,21},{7,23},{8,24},{10,26},{13,29},{15,31},{17,1},... | collective-permute-start | bytes 5898248 | tf_op jit(solution)/shard_map/ppermute | solution.py:498
  98.1 7.1 %all-to-all-done.1.dispatched = bf16[16,64,128]{2,1,0:T(8,128)(2,1)S(1)} async-done(((bf16[16,64,128]{2,1,0:T(8,128)(2,1)}), bf16[16,64,128]{2,1,0:T(8,128)(2,1)S(1)}, u32[]{:S(2)}, u32[]{:S(2)}) %all-to-all-start.1) | async-done | bytes 262176 | tf_op jit(solution)/shard_map/all_to_all | solution.py:260
  105.2 1.3 spread.1
  106.5 6.5 %all-to-all-start.2 = ((bf16[16,256,128]{2,1,0:T(8,128)(2,1)}), bf16[16,256,128]{2,1,0:T(8,128)(2,1)S(1)}, u32[]{:S(2)}, u32[]{:S(2)}) async-start(bf16[16,256,128]{2,1,0:T(8,128)(2,1)} %spread.1), calls=%async_computation.2 | async-start | bytes 2097152 | tf_op jit(solution)/shard_map/all_to_all | solution.py:260
  113.0 17.6 %all-to-all-done.2.gathered = bf16[16,256,128]{2,1,0:T(8,128)(2,1)S(1)} async-done(((bf16[16,256,128]{2,1,0:T(8,128)(2,1)}), bf16[16,256,128]{2,1,0:T(8,128)(2,1)S(1)}, u32[]{:S(2)}, u32[]{:S(2)}) %all-to-all-start.2) | async-done | bytes 1048608 | tf_op jit(solution)/shard_map/all_to_all | solution.py:260
  130.6 0.0 collective-permute-done.6.fwd_0
  130.6 0.0 collective-permute-done.7.fwd_1
  130.6 0.0 collective-permute-done.8.fwd_2
  130.6 0.0 collective-permute-done.9.fwd_3
  130.6 0.0 copy-done.1
  130.6 7.4 %expert.1 = bf16[16,272,128]{2,1,0:T(8,128)(2,1)S(1)} custom-call(s32[1]{0:T(128)} %bitcast.serves, bf16[16,256,128]{2,1,0:T(8,128)(2,1)S(1)} %all-to-all-done.2.gathered, bf16[256,128]{1,0:T(8,128)(2,1)S(1)} %get-tuple-element.24.own, f32[1,2048]{1,0:T(1,128)S(1)} %bitcast.34, bf16[320,2048]{1,0:T(8,128)(2,1)} %bitcast.36, bf16[320,2048]{1,0:T(8,128)(2,1)} %bitcast.38, ...), custom_call_target="tpu_custom_call" | custom-call | flops 4026531840 | bytes 17825792 | tf_op jit(solution)/shard_map/expert/pallas_call | solution.py:397
  138.0 0.0 copy-start.3
  138.0 20.2 %all_to_all.26.shares = bf16[16,272,128]{2,1,0:T(8,128)(2,1)S(1)} all-to-all(bf16[16,272,128]{2,1,0:T(8,128)(2,1)S(1)} %expert.1), channel_id=1, replica_groups=mesh['sp'=32,'tp'=16] {'tp'}, dimensions={0} | all-to-all | bytes 2228224 | tf_op jit(solution)/shard_map/all_to_all | solution.py:260
  158.2 0.0 copy-start.2
  158.2 1.0 shares.1
  159.2 7.2 %all-to-all-start.4 = ((bf16[16,64,128]{2,1,0:T(8,128)(2,1)}), bf16[16,64,128]{2,1,0:T(8,128)(2,1)S(1)}, u32[]{:S(2)}, u32[]{:S(2)}) async-start(bf16[16,64,128]{2,1,0:T(8,128)(2,1)} %shares.1), calls=%async_computation.4 | async-start | bytes 524288 | tf_op jit(solution)/shard_map/all_to_all | solution.py:260
  166.5 0.1 copy.16
  166.6 0.0 copy-done.3
  166.6 0.1 iota_compare_fusion
  166.7 17.4 %all-to-all-done.4 = bf16[16,64,128]{2,1,0:T(8,128)(2,1)S(1)} async-done(((bf16[16,64,128]{2,1,0:T(8,128)(2,1)}), bf16[16,64,128]{2,1,0:T(8,128)(2,1)S(1)}, u32[]{:S(2)}, u32[]{:S(2)}) %all-to-all-start.4) | async-done | bytes 262176 | tf_op jit(solution)/shard_map/all_to_all | solution.py:260
  184.1 0.1 reshape.22
  184.2 0.2 convolution_multiply_fusion.1
  184.4 0.0 copy-done.2
  184.4 0.8 fusion.2
  (2 shorter events, 0.0 us)
Async XLA Ops:
  3.5 84.4 %collective-permute-start.2 = (bf16[480,2048]{1,0:T(8,128)(2,1)}, bf16[480,2048]{1,0:T(8,128)(2,1)}, u32[]{:S(2)}, u32[]{:S(2)}) collective-permute-start(bf16[480,2048]{1,0:T(8,128)(2,1)} %get-tuple-element.25), channel_id=1, source_target_pairs={{0,21},{1,2},{2,23},{3,0},{4,5},{5,26},{6,7},{7,24},{8,29},{9,10},... | collective-permute-start | bytes 5898248 | tf_op jit(solution)/shard_map/ppermute | solution.py:497
  7.3 82.4 %collective-permute-start.3 = (bf16[480,2048]{1,0:T(8,128)(2,1)S(1)}, bf16[480,2048]{1,0:T(8,128)(2,1)}, u32[]{:S(2)}, u32[]{:S(2)}) collective-permute-start(bf16[480,2048]{1,0:T(8,128)(2,1)S(1)} %get-tuple-element.26), channel_id=1, source_target_pairs={{0,31},{1,0},{2,29},{3,2},{4,7},{5,16},{6,5},{7,18},{8,23},{9,8},{... | collective-permute-start | bytes 5898248 | tf_op jit(solution)/shard_map/ppermute | solution.py:497
  12.2 80.1 %collective-permute-start.4 = (bf16[480,2048]{1,0:T(8,128)(2,1)}, bf16[480,2048]{1,0:T(8,128)(2,1)}, u32[]{:S(2)}, u32[]{:S(2)}) collective-permute-start(bf16[480,2048]{1,0:T(8,128)(2,1)} %get-tuple-element.25), channel_id=1, source_target_pairs={{0,16},{1,5},{2,18},{3,7},{4,8},{5,21},{6,10},{7,23},{8,24},{9,13}... | collective-permute-start | bytes 5898248 | tf_op jit(solution)/shard_map/ppermute | solution.py:497
  14.1 81.4 %collective-permute-start.5 = (bf16[480,2048]{1,0:T(8,128)(2,1)S(1)}, bf16[480,2048]{1,0:T(8,128)(2,1)}, u32[]{:S(2)}, u32[]{:S(2)}) collective-permute-start(bf16[480,2048]{1,0:T(8,128)(2,1)S(1)} %get-tuple-element.26), channel_id=1, source_target_pairs={{0,16},{1,13},{2,18},{3,15},{4,0},{5,21},{6,2},{7,23},{8,24},{9,5}... | collective-permute-start | bytes 5898248 | tf_op jit(solution)/shard_map/ppermute | solution.py:497
  16.0 55.1 %copy-start = (bf16[2048,128]{1,0:T(8,128)(2,1)S(1)}, bf16[2048,128]{1,0:T(8,128)(2,1)}, u32[]{:S(2)}) copy-start(bf16[2048,128]{1,0:T(8,128)(2,1)} %weight.1) | copy-start | bytes 1572868
  17.4 8.2 %collective-permute-start = (bf16[128,128]{1,0:T(8,128)(2,1)S(1)}, bf16[128,128]{1,0:T(8,128)(2,1)S(1)}, u32[]{:S(2)}, u32[]{:S(2)}) collective-permute-start(bf16[128,128]{1,0:T(8,128)(2,1)S(1)} %get-tuple-element.18), channel_id=1, source_target_pairs={{0,16},{16,32},{32,48},{48,64},{64,80},{80,96},{96,112},{112,128},... | collective-permute-start | bytes 98312 | tf_op jit(solution)/shard_map/ppermute | solution.py:505
  25.6 3.5 %collective-permute-start.1 = (bf16[128,128]{1,0:T(8,128)(2,1)S(1)}, bf16[128,128]{1,0:T(8,128)(2,1)S(1)}, u32[]{:S(2)}, u32[]{:S(2)}) collective-permute-start(bf16[128,128]{1,0:T(8,128)(2,1)S(1)} %get-tuple-element.20), channel_id=1, source_target_pairs={{16,0},{32,16},{48,32},{64,48},{80,64},{96,80},{112,96},{128,112},... | collective-permute-start | bytes 98312 | tf_op jit(solution)/shard_map/ppermute | solution.py:506
  72.5 58.1 %copy-start.1 = (f32[2048]{0:T(1024)S(1)}, f32[2048]{0:T(1024)}, u32[]{:S(2)}) copy-start(f32[2048]{0:T(1024)} %param.18) | copy-start | bytes 24580
  72.5 32.7 %all-to-all-start.1 = ((bf16[16,64,128]{2,1,0:T(8,128)(2,1)}), bf16[16,64,128]{2,1,0:T(8,128)(2,1)S(1)}, u32[]{:S(2)}, u32[]{:S(2)}) async-start(bf16[16,64,128]{2,1,0:T(8,128)(2,1)} %get-tuple-element.23), calls=%async_computation.1 | async-start | bytes 524288 | tf_op jit(solution)/shard_map/all_to_all | solution.py:260
  87.8 42.7 %collective-permute-start.6 = (bf16[480,2048]{1,0:T(8,128)(2,1)}, bf16[480,2048]{1,0:T(8,128)(2,1)}, u32[]{:S(2)}, u32[]{:S(2)}) collective-permute-start(bf16[480,2048]{1,0:T(8,128)(2,1)} %collective-permute-done.2.got_0), channel_id=1, source_target_pairs={{0,16},{1,17},{2,18},{3,19},{4,20},{5,21},{6,22},{7,23},{8,24},{9,... | collective-permute-start | bytes 5898248 | tf_op jit(solution)/shard_map/ppermute | solution.py:498
  89.8 40.8 %collective-permute-start.7 = (bf16[480,2048]{1,0:T(8,128)(2,1)}, bf16[480,2048]{1,0:T(8,128)(2,1)}, u32[]{:S(2)}, u32[]{:S(2)}) collective-permute-start(bf16[480,2048]{1,0:T(8,128)(2,1)} %collective-permute-done.3.got_1), channel_id=1, source_target_pairs={{0,16},{1,17},{2,18},{3,19},{4,20},{5,21},{6,22},{7,23},{8,24},{9,... | collective-permute-start | bytes 5898248 | tf_op jit(solution)/shard_map/ppermute | solution.py:498
  92.2 38.4 %collective-permute-start.8 = (bf16[480,2048]{1,0:T(8,128)(2,1)}, bf16[480,2048]{1,0:T(8,128)(2,1)}, u32[]{:S(2)}, u32[]{:S(2)}) collective-permute-start(bf16[480,2048]{1,0:T(8,128)(2,1)} %collective-permute-done.4.got_2), channel_id=1, source_target_pairs={{0,16},{2,18},{5,21},{7,23},{8,24},{10,26},{13,29},{15,31},{17,1},... | collective-permute-start | bytes 5898248 | tf_op jit(solution)/shard_map/ppermute | solution.py:498
  95.5 35.1 %collective-permute-start.9 = (bf16[480,2048]{1,0:T(8,128)(2,1)}, bf16[480,2048]{1,0:T(8,128)(2,1)}, u32[]{:S(2)}, u32[]{:S(2)}) collective-permute-start(bf16[480,2048]{1,0:T(8,128)(2,1)} %collective-permute-done.5.got_3), channel_id=1, source_target_pairs={{0,16},{2,18},{5,21},{7,23},{8,24},{10,26},{13,29},{15,31},{17,1},... | collective-permute-start | bytes 5898248 | tf_op jit(solution)/shard_map/ppermute | solution.py:498
  106.5 24.1 %all-to-all-start.2 = ((bf16[16,256,128]{2,1,0:T(8,128)(2,1)}), bf16[16,256,128]{2,1,0:T(8,128)(2,1)S(1)}, u32[]{:S(2)}, u32[]{:S(2)}) async-start(bf16[16,256,128]{2,1,0:T(8,128)(2,1)} %spread.1), calls=%async_computation.2 | async-start | bytes 2097152 | tf_op jit(solution)/shard_map/all_to_all | solution.py:260
  138.0 28.6 %copy-start.3 = (f32[16,2]{0,1:T(2,128)S(1)}, f32[16,2]{0,1:T(2,128)}, u32[]{:S(2)}) copy-start(f32[16,2]{0,1:T(2,128)} %param.20) | copy-start | bytes 388
  158.2 26.1 %copy-start.2 = (bf16[16,2048]{1,0:T(8,128)(2,1)S(1)}, bf16[16,2048]{1,0:T(8,128)(2,1)}, u32[]{:S(2)}) copy-start(bf16[16,2048]{1,0:T(8,128)(2,1)} %residual.1) | copy-start | bytes 196612
  159.2 24.9 %all-to-all-start.4 = ((bf16[16,64,128]{2,1,0:T(8,128)(2,1)}), bf16[16,64,128]{2,1,0:T(8,128)(2,1)S(1)}, u32[]{:S(2)}, u32[]{:S(2)}) async-start(bf16[16,64,128]{2,1,0:T(8,128)(2,1)} %shares.1), calls=%async_computation.4 | async-start | bytes 524288 | tf_op jit(solution)/shard_map/all_to_all | solution.py:260

commit v8 on v7

--- a/solution.py
+++ b/solution.py
@@ -262,32 +262,41 @@
     )
 
 
-def pack_kernel(gate, up, down, *rest):
-    outs, sems = rest[:-1], rest[-1]
-    part = gate.shape[0] // len(outs)
-    copies = [
-        pltpu.make_async_copy(
-            source.at[pl.ds(k * part, part)], out.at[pl.ds(i * part, part)], sems.at[k * 3 + i]
-        )
-        for k, out in enumerate(outs)
-        for i, source in enumerate((gate, up, down))
+def pack_kernel(gate, up, down, first, second, held, sems):
+    half = gate.shape[0]
+    part = half // 2
+    sources, outs = (gate, up, down), (first, second)
+    loads = [
+        pltpu.make_async_copy(source, held.at[i], sems.at[i]) for i, source in enumerate(sources)
     ]
-    for copy in copies:
+    for copy in loads:
         copy.start()
-    for copy in copies:
+    stores = []
+    for i, copy in enumerate(loads):
         copy.wait()
-
-
-def pack(owned, ways):
+        for k, out in enumerate(outs):
+            stores.append(
+                pltpu.make_async_copy(
+                    held.at[i, pl.ds(k * part, part)],
+                    out.at[pl.ds(i * part, part)],
+                    sems.at[3 + 2 * i + k],
+                )
+            )
+            stores[-1].start()
+    for copy in stores:
+        copy.wait()
+
+
+def pack(owned):
     half, width = owned[0].shape
     return pl.pallas_call(
         pack_kernel,
-        out_shape=tuple(
-            jax.ShapeDtypeStruct((3 * half // ways, width), jnp.bfloat16) for _ in range(ways)
-        ),
+        out_shape=tuple(pltpu.HBM((3 * half // 2, width), jnp.bfloat16) for _ in range(2)),
         in_specs=[ANYWHERE] * 3,
-        out_specs=(VMEM,) * ways,
-        scratch_shapes=[pltpu.SemaphoreType.DMA((3 * ways,))],
+        out_specs=(ANYWHERE,) * 2,
+        scratch_shapes=[
+            pltpu.VMEM((3, half, width), jnp.bfloat16), pltpu.SemaphoreType.DMA((9,)),
+        ],
         cost_estimate=pl.CostEstimate(
             flops=half * width, bytes_accessed=12 * half * width, transcendentals=0
         ),
@@ -492,7 +501,7 @@
     serves = (core_index == served_side(lax.axis_index("tp"))).astype(jnp.int32).reshape(1)
     owned = (gate_weight[0].T, up_weight[0].T, down_weight[0])
     received, forwarded = [], []
-    packed = pack(owned, 2)
+    packed = pack(owned)
     for k, way in enumerate(moves):
         received.append(lax.ppermute(packed[k % 2], ("sp", "tp"), way))
         forwarded.append(lax.ppermute(received[-1], ("sp", "tp"), passes[k]))

time: 186 us -> 186 us (level)
  no operation moved by 1% of the time
where the time goes in v8:
time: 186 us; the launch traced here: 185 us
  blocking collectives  59.7 us (32%)
  starting transfers between devices  56.9 us (31%)
  waiting for transfers between devices  48.6 us (26%)
  Pallas kernels  18.5 us (10%)
    all_to_all x2, blocking collectives, exchange(): lax.all_to_all(value, axis, split_axis=0, concat_axis=0, tiled=True, axis...  59.7 us
    all_to_all x3, waiting for transfers between devices, exchange(): lax.all_to_all(value, axis, split_axis=0, concat_axis=0, tiled=True, axis...  42.2 us
    all_to_all x3, starting transfers between devices, exchange(): lax.all_to_all(value, axis, split_axis=0, concat_axis=0, tiled=True, axis...  29 us
    ppermute x4, starting transfers between devices, local(): received.append(lax.ppermute(packed[k % 2], ('sp', 'tp'), way))  12.5 us
    ppermute x4, starting transfers between devices, local(): forwarded.append(lax.ppermute(received[-1], ('sp', 'tp'), passes[k]))  10.2 us
    pallas_call x1, Pallas kernels, run_expert(): pl.pallas_call(expert_kernel, out_shape=jax.ShapeDtypeStruct((members, ro...  7.39 us
    ppermute x1, waiting for transfers between devices, local(): low = lax.ppermute(low, 'sp', forward)  4.9 us
  transfers between devices with their start and end apart: 13, of which 5 were waited for; matrix products, arithmetic and copies ran while one was open for 0% of the time, Pallas kernels for 4%

profile of v8, /device:TPU:32, one launch (start us, length us, event | category | flops | bytes accessed | tf_op | source)
XLA Modules:
  0.0 185.3 jit_solution(13815074605456453127)
XLA Ops:
  0.0 3.3 %pack.1 = (bf16[480,2048]{1,0:T(8,128)(2,1)}, bf16[480,2048]{1,0:T(8,128)(2,1)}) custom-call(bf16[320,2048]{1,0:T(8,128)(2,1)} %bitcast.35, bf16[320,2048]{1,0:T(8,128)(2,1)} %bitcast.37, bf16[320,2048]{1,0:T(8,128)(2,1)} %bitcast.39), custom_call_target="tpu_custom_call" | custom-call | flops 655360 | bytes 7864320 | tf_op jit(solution)/shard_map/pack/pallas_call | solution.py:292
  3.3 3.9 %collective-permute-start.2 = (bf16[480,2048]{1,0:T(8,128)(2,1)}, bf16[480,2048]{1,0:T(8,128)(2,1)S(1)}, u32[]{:S(2)}, u32[]{:S(2)}) collective-permute-start(bf16[480,2048]{1,0:T(8,128)(2,1)} %get-tuple-element.25), channel_id=1, source_target_pairs={{0,21},{1,2},{2,23},{3,0},{4,5},{5,26},{6,7},{7,24},{8,29},{9,10},... | collective-permute-start | bytes 5898248 | tf_op jit(solution)/shard_map/ppermute | solution.py:506
  7.2 4.8 %collective-permute-start.3 = (bf16[480,2048]{1,0:T(8,128)(2,1)}, bf16[480,2048]{1,0:T(8,128)(2,1)}, u32[]{:S(2)}, u32[]{:S(2)}) collective-permute-start(bf16[480,2048]{1,0:T(8,128)(2,1)} %get-tuple-element.26), channel_id=1, source_target_pairs={{0,31},{1,0},{2,29},{3,2},{4,7},{5,16},{6,5},{7,18},{8,23},{9,8},{... | collective-permute-start | bytes 5898248 | tf_op jit(solution)/shard_map/ppermute | solution.py:506
  12.0 1.9 %collective-permute-start.4 = (bf16[480,2048]{1,0:T(8,128)(2,1)}, bf16[480,2048]{1,0:T(8,128)(2,1)}, u32[]{:S(2)}, u32[]{:S(2)}) collective-permute-start(bf16[480,2048]{1,0:T(8,128)(2,1)} %get-tuple-element.25), channel_id=1, source_target_pairs={{0,16},{1,5},{2,18},{3,7},{4,8},{5,21},{6,10},{7,23},{8,24},{9,13}... | collective-permute-start | bytes 5898248 | tf_op jit(solution)/shard_map/ppermute | solution.py:506
  13.9 1.9 %collective-permute-start.5 = (bf16[480,2048]{1,0:T(8,128)(2,1)}, bf16[480,2048]{1,0:T(8,128)(2,1)}, u32[]{:S(2)}, u32[]{:S(2)}) collective-permute-start(bf16[480,2048]{1,0:T(8,128)(2,1)} %get-tuple-element.26), channel_id=1, source_target_pairs={{0,16},{1,13},{2,18},{3,15},{4,0},{5,21},{6,2},{7,23},{8,24},{9,5}... | collective-permute-start | bytes 5898248 | tf_op jit(solution)/shard_map/ppermute | solution.py:506
  15.8 0.0 copy-start
  15.9 1.4 prepare.1
  17.2 3.3 %collective-permute-start = (bf16[128,128]{1,0:T(8,128)(2,1)S(1)}, bf16[128,128]{1,0:T(8,128)(2,1)S(1)}, u32[]{:S(2)}, u32[]{:S(2)}) collective-permute-start(bf16[128,128]{1,0:T(8,128)(2,1)S(1)} %get-tuple-element.18), channel_id=1, source_target_pairs={{0,16},{16,32},{32,48},{48,64},{64,80},{80,96},{96,112},{112,128},... | collective-permute-start | bytes 98312 | tf_op jit(solution)/shard_map/ppermute | solution.py:514
  20.6 4.9 %collective-permute-done.low = bf16[128,128]{1,0:T(8,128)(2,1)S(1)} collective-permute-done((bf16[128,128]{1,0:T(8,128)(2,1)S(1)}, bf16[128,128]{1,0:T(8,128)(2,1)S(1)}, u32[]{:S(2)}, u32[]{:S(2)}) %collective-permute-start) | collective-permute-done | bytes 32800 | tf_op jit(solution)/shard_map/ppermute | solution.py:514
  25.5 1.9 %collective-permute-start.1 = (bf16[128,128]{1,0:T(8,128)(2,1)S(1)}, bf16[128,128]{1,0:T(8,128)(2,1)S(1)}, u32[]{:S(2)}, u32[]{:S(2)}) collective-permute-start(bf16[128,128]{1,0:T(8,128)(2,1)S(1)} %get-tuple-element.20), channel_id=1, source_target_pairs={{16,0},{32,16},{48,32},{64,48},{80,64},{96,80},{112,96},{128,112},... | collective-permute-start | bytes 98312 | tf_op jit(solution)/shard_map/ppermute | solution.py:515
  27.4 0.1 pad_add_fusion.place
  27.5 1.5 collective-permute-done.1.high
  29.0 2.7 %attend.1 = bf16[16,288,128]{2,1,0:T(8,128)(2,1)S(1)} custom-call(s32[2]{0:T(128)S(1)} %pad_add_fusion.place, f32[1,2]{1,0:T(1,128)S(1)} %get-tuple-element.16.sink, bf16[256,128]{1,0:T(8,128)(2,1)S(1)} %get-tuple-element.17.queries, bf16[128,128]{1,0:T(8,128)(2,1)S(1)} %collective-permute-done.low, bf16[128,256]{1,0:T(8,128)(2,1)S(1)} %get-tuple-element.19.own, ...), custom_call_target="tpu_custom_call" | custom-call | flops 50331648 | bytes 2097152 | tf_op jit(solution)/shard_map/attend/pallas_call | solution.py:140
  31.7 39.5 %all_to_all.25.arrived = bf16[16,288,128]{2,1,0:T(8,128)(2,1)S(1)} all-to-all(bf16[16,288,128]{2,1,0:T(8,128)(2,1)S(1)} %attend.1), channel_id=1, replica_groups=mesh['sp'=32,'tp'=16] {'tp'}, dimensions={0} | all-to-all | bytes 2359296 | tf_op jit(solution)/shard_map/all_to_all | solution.py:260
  71.1 0.0 copy-done
  71.1 1.4 project.1
  72.5 0.0 copy-start.1
  72.5 15.3 %all-to-all-start.1 = ((bf16[16,64,128]{2,1,0:T(8,128)(2,1)}), bf16[16,64,128]{2,1,0:T(8,128)(2,1)S(1)}, u32[]{:S(2)}, u32[]{:S(2)}) async-start(bf16[16,64,128]{2,1,0:T(8,128)(2,1)} %get-tuple-element.23), calls=%async_computation.1 | async-start | bytes 524288 | tf_op jit(solution)/shard_map/all_to_all | solution.py:260
  87.9 0.0 collective-permute-done.2.got_0
  87.9 0.0 copy-start.2
  87.9 1.9 %collective-permute-start.6 = (bf16[480,2048]{1,0:T(8,128)(2,1)S(1)}, bf16[480,2048]{1,0:T(8,128)(2,1)}, u32[]{:S(2)}, u32[]{:S(2)}) collective-permute-start(bf16[480,2048]{1,0:T(8,128)(2,1)S(1)} %collective-permute-done.2.got_0), channel_id=1, source_target_pairs={{0,16},{1,17},{2,18},{3,19},{4,20},{5,21},{6,22},{7,23},{8,24},{9,... | collective-permute-start | bytes 5898248 | tf_op jit(solution)/shard_map/ppermute | solution.py:507
  89.8 0.0 collective-permute-done.3.got_1
  89.8 2.4 %collective-permute-start.7 = (bf16[480,2048]{1,0:T(8,128)(2,1)}, bf16[480,2048]{1,0:T(8,128)(2,1)}, u32[]{:S(2)}, u32[]{:S(2)}) collective-permute-start(bf16[480,2048]{1,0:T(8,128)(2,1)} %collective-permute-done.3.got_1), channel_id=1, source_target_pairs={{0,16},{1,17},{2,18},{3,19},{4,20},{5,21},{6,22},{7,23},{8,24},{9,... | collective-permute-start | bytes 5898248 | tf_op jit(solution)/shard_map/ppermute | solution.py:507
  92.3 0.0 collective-permute-done.4.got_2
  92.3 3.3 %collective-permute-start.8 = (bf16[480,2048]{1,0:T(8,128)(2,1)}, bf16[480,2048]{1,0:T(8,128)(2,1)}, u32[]{:S(2)}, u32[]{:S(2)}) collective-permute-start(bf16[480,2048]{1,0:T(8,128)(2,1)} %collective-permute-done.4.got_2), channel_id=1, source_target_pairs={{0,16},{2,18},{5,21},{7,23},{8,24},{10,26},{13,29},{15,31},{17,1},... | collective-permute-start | bytes 5898248 | tf_op jit(solution)/shard_map/ppermute | solution.py:507
  95.5 0.0 collective-permute-done.5.got_3
  95.5 2.6 %collective-permute-start.9 = (bf16[480,2048]{1,0:T(8,128)(2,1)}, bf16[480,2048]{1,0:T(8,128)(2,1)}, u32[]{:S(2)}, u32[]{:S(2)}) collective-permute-start(bf16[480,2048]{1,0:T(8,128)(2,1)} %collective-permute-done.5.got_3), channel_id=1, source_target_pairs={{0,16},{2,18},{5,21},{7,23},{8,24},{10,26},{13,29},{15,31},{17,1},... | collective-permute-start | bytes 5898248 | tf_op jit(solution)/shard_map/ppermute | solution.py:507
  98.1 7.1 %all-to-all-done.1.dispatched = bf16[16,64,128]{2,1,0:T(8,128)(2,1)S(1)} async-done(((bf16[16,64,128]{2,1,0:T(8,128)(2,1)}), bf16[16,64,128]{2,1,0:T(8,128)(2,1)S(1)}, u32[]{:S(2)}, u32[]{:S(2)}) %all-to-all-start.1) | async-done | bytes 262176 | tf_op jit(solution)/shard_map/all_to_all | solution.py:260
  105.2 1.3 spread.1
  106.5 6.5 %all-to-all-start.2 = ((bf16[16,256,128]{2,1,0:T(8,128)(2,1)}), bf16[16,256,128]{2,1,0:T(8,128)(2,1)S(1)}, u32[]{:S(2)}, u32[]{:S(2)}) async-start(bf16[16,256,128]{2,1,0:T(8,128)(2,1)} %spread.1), calls=%async_computation.2 | async-start | bytes 2097152 | tf_op jit(solution)/shard_map/all_to_all | solution.py:260
  113.0 17.6 %all-to-all-done.2.gathered = bf16[16,256,128]{2,1,0:T(8,128)(2,1)S(1)} async-done(((bf16[16,256,128]{2,1,0:T(8,128)(2,1)}), bf16[16,256,128]{2,1,0:T(8,128)(2,1)S(1)}, u32[]{:S(2)}, u32[]{:S(2)}) %all-to-all-start.2) | async-done | bytes 1048608 | tf_op jit(solution)/shard_map/all_to_all | solution.py:260
  130.7 0.0 collective-permute-done.6.fwd_0
  130.7 0.0 collective-permute-done.7.fwd_1
  130.7 0.0 collective-permute-done.8.fwd_2
  130.7 0.0 collective-permute-done.9.fwd_3
  130.7 0.0 copy-done.2
  130.7 0.0 copy-done.1
  130.7 7.4 %expert.1 = bf16[16,272,128]{2,1,0:T(8,128)(2,1)S(1)} custom-call(s32[1]{0:T(128)} %bitcast.serves, bf16[16,256,128]{2,1,0:T(8,128)(2,1)S(1)} %all-to-all-done.2.gathered, bf16[256,128]{1,0:T(8,128)(2,1)S(1)} %get-tuple-element.24.own, f32[1,2048]{1,0:T(1,128)S(1)} %bitcast.34, bf16[320,2048]{1,0:T(8,128)(2,1)} %bitcast.36, bf16[320,2048]{1,0:T(8,128)(2,1)} %bitcast.38, ...), custom_call_target="tpu_custom_call" | custom-call | flops 4026531840 | bytes 17825792 | tf_op jit(solution)/shard_map/expert/pallas_call | solution.py:406
  138.1 0.0 copy-start.4
  138.2 20.3 %all_to_all.26.shares = bf16[16,272,128]{2,1,0:T(8,128)(2,1)S(1)} all-to-all(bf16[16,272,128]{2,1,0:T(8,128)(2,1)S(1)} %expert.1), channel_id=1, replica_groups=mesh['sp'=32,'tp'=16] {'tp'}, dimensions={0} | all-to-all | bytes 2228224 | tf_op jit(solution)/shard_map/all_to_all | solution.py:260
  158.4 0.0 copy-start.3
  158.4 1.0 shares.1
  159.4 7.1 %all-to-all-start.4 = ((bf16[16,64,128]{2,1,0:T(8,128)(2,1)}), bf16[16,64,128]{2,1,0:T(8,128)(2,1)S(1)}, u32[]{:S(2)}, u32[]{:S(2)}) async-start(bf16[16,64,128]{2,1,0:T(8,128)(2,1)} %shares.1), calls=%async_computation.4 | async-start | bytes 524288 | tf_op jit(solution)/shard_map/all_to_all | solution.py:260
  166.6 0.1 copy.16
  166.7 0.0 copy-done.4
  166.7 0.1 iota_compare_fusion
  166.7 17.4 %all-to-all-done.4 = bf16[16,64,128]{2,1,0:T(8,128)(2,1)S(1)} async-done(((bf16[16,64,128]{2,1,0:T(8,128)(2,1)}), bf16[16,64,128]{2,1,0:T(8,128)(2,1)S(1)}, u32[]{:S(2)}, u32[]{:S(2)}) %all-to-all-start.4) | async-done | bytes 262176 | tf_op jit(solution)/shard_map/all_to_all | solution.py:260
  184.2 0.1 reshape.22
  184.3 0.2 convolution_multiply_fusion.1
  184.5 0.0 copy-done.3
  184.5 0.8 fusion.2
  (2 shorter events, 0.0 us)
Async XLA Ops:
  3.3 84.6 %collective-permute-start.2 = (bf16[480,2048]{1,0:T(8,128)(2,1)}, bf16[480,2048]{1,0:T(8,128)(2,1)S(1)}, u32[]{:S(2)}, u32[]{:S(2)}) collective-permute-start(bf16[480,2048]{1,0:T(8,128)(2,1)} %get-tuple-element.25), channel_id=1, source_target_pairs={{0,21},{1,2},{2,23},{3,0},{4,5},{5,26},{6,7},{7,24},{8,29},{9,10},... | collective-permute-start | bytes 5898248 | tf_op jit(solution)/shard_map/ppermute | solution.py:506
  7.2 82.7 %collective-permute-start.3 = (bf16[480,2048]{1,0:T(8,128)(2,1)}, bf16[480,2048]{1,0:T(8,128)(2,1)}, u32[]{:S(2)}, u32[]{:S(2)}) collective-permute-start(bf16[480,2048]{1,0:T(8,128)(2,1)} %get-tuple-element.26), channel_id=1, source_target_pairs={{0,31},{1,0},{2,29},{3,2},{4,7},{5,16},{6,5},{7,18},{8,23},{9,8},{... | collective-permute-start | bytes 5898248 | tf_op jit(solution)/shard_map/ppermute | solution.py:506
  12.0 80.3 %collective-permute-start.4 = (bf16[480,2048]{1,0:T(8,128)(2,1)}, bf16[480,2048]{1,0:T(8,128)(2,1)}, u32[]{:S(2)}, u32[]{:S(2)}) collective-permute-start(bf16[480,2048]{1,0:T(8,128)(2,1)} %get-tuple-element.25), channel_id=1, source_target_pairs={{0,16},{1,5},{2,18},{3,7},{4,8},{5,21},{6,10},{7,23},{8,24},{9,13}... | collective-permute-start | bytes 5898248 | tf_op jit(solution)/shard_map/ppermute | solution.py:506
  13.9 81.6 %collective-permute-start.5 = (bf16[480,2048]{1,0:T(8,128)(2,1)}, bf16[480,2048]{1,0:T(8,128)(2,1)}, u32[]{:S(2)}, u32[]{:S(2)}) collective-permute-start(bf16[480,2048]{1,0:T(8,128)(2,1)} %get-tuple-element.26), channel_id=1, source_target_pairs={{0,16},{1,13},{2,18},{3,15},{4,0},{5,21},{6,2},{7,23},{8,24},{9,5}... | collective-permute-start | bytes 5898248 | tf_op jit(solution)/shard_map/ppermute | solution.py:506
  15.8 55.3 %copy-start = (bf16[2048,128]{1,0:T(8,128)(2,1)S(1)}, bf16[2048,128]{1,0:T(8,128)(2,1)}, u32[]{:S(2)}) copy-start(bf16[2048,128]{1,0:T(8,128)(2,1)} %weight.1) | copy-start | bytes 1572868
  17.2 8.2 %collective-permute-start = (bf16[128,128]{1,0:T(8,128)(2,1)S(1)}, bf16[128,128]{1,0:T(8,128)(2,1)S(1)}, u32[]{:S(2)}, u32[]{:S(2)}) collective-permute-start(bf16[128,128]{1,0:T(8,128)(2,1)S(1)} %get-tuple-element.18), channel_id=1, source_target_pairs={{0,16},{16,32},{32,48},{48,64},{64,80},{80,96},{96,112},{112,128},... | collective-permute-start | bytes 98312 | tf_op jit(solution)/shard_map/ppermute | solution.py:514
  25.5 3.5 %collective-permute-start.1 = (bf16[128,128]{1,0:T(8,128)(2,1)S(1)}, bf16[128,128]{1,0:T(8,128)(2,1)S(1)}, u32[]{:S(2)}, u32[]{:S(2)}) collective-permute-start(bf16[128,128]{1,0:T(8,128)(2,1)S(1)} %get-tuple-element.20), channel_id=1, source_target_pairs={{16,0},{32,16},{48,32},{64,48},{80,64},{96,80},{112,96},{128,112},... | collective-permute-start | bytes 98312 | tf_op jit(solution)/shard_map/ppermute | solution.py:515
  72.5 58.2 %copy-start.1 = (f32[2048]{0:T(1024)S(1)}, f32[2048]{0:T(1024)}, u32[]{:S(2)}) copy-start(f32[2048]{0:T(1024)} %param.18) | copy-start | bytes 24580
  72.5 32.7 %all-to-all-start.1 = ((bf16[16,64,128]{2,1,0:T(8,128)(2,1)}), bf16[16,64,128]{2,1,0:T(8,128)(2,1)S(1)}, u32[]{:S(2)}, u32[]{:S(2)}) async-start(bf16[16,64,128]{2,1,0:T(8,128)(2,1)} %get-tuple-element.23), calls=%async_computation.1 | async-start | bytes 524288 | tf_op jit(solution)/shard_map/all_to_all | solution.py:260
  87.9 42.8 %copy-start.2 = (bf16[480,2048]{1,0:T(8,128)(2,1)}, bf16[480,2048]{1,0:T(8,128)(2,1)S(1)}, u32[]{:S(2)}) copy-start(bf16[480,2048]{1,0:T(8,128)(2,1)S(1)} %collective-permute-done.2.got_0) | copy-start | bytes 5898244
  87.9 42.8 %collective-permute-start.6 = (bf16[480,2048]{1,0:T(8,128)(2,1)S(1)}, bf16[480,2048]{1,0:T(8,128)(2,1)}, u32[]{:S(2)}, u32[]{:S(2)}) collective-permute-start(bf16[480,2048]{1,0:T(8,128)(2,1)S(1)} %collective-permute-done.2.got_0), channel_id=1, source_target_pairs={{0,16},{1,17},{2,18},{3,19},{4,20},{5,21},{6,22},{7,23},{8,24},{9,... | collective-permute-start | bytes 5898248 | tf_op jit(solution)/shard_map/ppermute | solution.py:507
  89.8 40.9 %collective-permute-start.7 = (bf16[480,2048]{1,0:T(8,128)(2,1)}, bf16[480,2048]{1,0:T(8,128)(2,1)}, u32[]{:S(2)}, u32[]{:S(2)}) collective-permute-start(bf16[480,2048]{1,0:T(8,128)(2,1)} %collective-permute-done.3.got_1), channel_id=1, source_target_pairs={{0,16},{1,17},{2,18},{3,19},{4,20},{5,21},{6,22},{7,23},{8,24},{9,... | collective-permute-start | bytes 5898248 | tf_op jit(solution)/shard_map/ppermute | solution.py:507
  92.3 38.4 %collective-permute-start.8 = (bf16[480,2048]{1,0:T(8,128)(2,1)}, bf16[480,2048]{1,0:T(8,128)(2,1)}, u32[]{:S(2)}, u32[]{:S(2)}) collective-permute-start(bf16[480,2048]{1,0:T(8,128)(2,1)} %collective-permute-done.4.got_2), channel_id=1, source_target_pairs={{0,16},{2,18},{5,21},{7,23},{8,24},{10,26},{13,29},{15,31},{17,1},... | collective-permute-start | bytes 5898248 | tf_op jit(solution)/shard_map/ppermute | solution.py:507
  95.5 35.2 %collective-permute-start.9 = (bf16[480,2048]{1,0:T(8,128)(2,1)}, bf16[480,2048]{1,0:T(8,128)(2,1)}, u32[]{:S(2)}, u32[]{:S(2)}) collective-permute-start(bf16[480,2048]{1,0:T(8,128)(2,1)} %collective-permute-done.5.got_3), channel_id=1, source_target_pairs={{0,16},{2,18},{5,21},{7,23},{8,24},{10,26},{13,29},{15,31},{17,1},... | collective-permute-start | bytes 5898248 | tf_op jit(solution)/shard_map/ppermute | solution.py:507
  106.5 24.2 %all-to-all-start.2 = ((bf16[16,256,128]{2,1,0:T(8,128)(2,1)}), bf16[16,256,128]{2,1,0:T(8,128)(2,1)S(1)}, u32[]{:S(2)}, u32[]{:S(2)}) async-start(bf16[16,256,128]{2,1,0:T(8,128)(2,1)} %spread.1), calls=%async_computation.2 | async-start | bytes 2097152 | tf_op jit(solution)/shard_map/all_to_all | solution.py:260
  138.1 28.5 %copy-start.4 = (f32[16,2]{0,1:T(2,128)S(1)}, f32[16,2]{0,1:T(2,128)}, u32[]{:S(2)}) copy-start(f32[16,2]{0,1:T(2,128)} %param.20) | copy-start | bytes 388
  158.4 26.0 %copy-start.3 = (bf16[16,2048]{1,0:T(8,128)(2,1)S(1)}, bf16[16,2048]{1,0:T(8,128)(2,1)}, u32[]{:S(2)}) copy-start(bf16[16,2048]{1,0:T(8,128)(2,1)} %residual.1) | copy-start | bytes 196612
  159.4 24.7 %all-to-all-start.4 = ((bf16[16,64,128]{2,1,0:T(8,128)(2,1)}), bf16[16,64,128]{2,1,0:T(8,128)(2,1)S(1)}, u32[]{:S(2)}, u32[]{:S(2)}) async-start(bf16[16,64,128]{2,1,0:T(8,128)(2,1)} %shares.1), calls=%async_computation.4 | async-start | bytes 524288 | tf_op jit(solution)/shard_map/all_to_all | solution.py:260

commit v9 on v8

--- a/solution.py
+++ b/solution.py
@@ -97,11 +97,26 @@
     )(*in_hbm((keys, values, queries, residual, sink, routes)))
 
 
-def attend_kernel(place, sink, queries, low, own, high, residual, slots, out):
+def attend_kernel(place, sink, queries, low, own, high, residual, slots, out, held, rest, sems):
     members = out.shape[0]
     length, both = queries.shape
     tok_rows = residual.shape[0]
     total = place[1] * length
+    copies = []
+
+    def send(source, t, start, size):
+        copies.append(
+            pltpu.make_async_copy(
+                source, out.at[t, pl.ds(start, size)], sems.at[len(copies)]
+            )
+        )
+        copies[-1].start()
+
+    for t in range(members):
+        rest[t, :tok_rows, :] = residual[:, t * 128 : (t + 1) * 128]
+        rest[t, tok_rows:, :] = slots[...]
+    for t in range(members):
+        send(rest.at[t], t, length, 2 * tok_rows)
     band = jnp.concatenate([low[...], own[...], high[...]], axis=1)
     row = lax.broadcasted_iota(jnp.int32, (WINDOW, 3 * WINDOW), 0)
     col = lax.broadcasted_iota(jnp.int32, (WINDOW, 3 * WINDOW), 1)
@@ -127,11 +142,11 @@
                 )
             )
         attended = jnp.concatenate(heads, axis=1).astype(jnp.bfloat16)
+        held[block * WINDOW : (block + 1) * WINDOW, :] = attended
         for t in range(members):
-            out[t, block * WINDOW : (block + 1) * WINDOW, :] = attended
-    for t in range(members):
-        out[t, length : length + tok_rows, :] = residual[:, t * 128 : (t + 1) * 128]
-        out[t, length + tok_rows :, :] = slots[...]
+            send(held.at[pl.ds(block * WINDOW, WINDOW)], t, block * WINDOW, WINDOW)
+    for copy in copies:
+        copy.wait()
 
 
 def run_attention(place, sink, queries, low, own, high, residual, slots, members):
@@ -139,9 +154,14 @@
     tok_rows = residual.shape[0]
     return pl.pallas_call(
         attend_kernel,
-        out_shape=jax.ShapeDtypeStruct((members, length + 2 * tok_rows, 128), jnp.bfloat16),
+        out_shape=pltpu.HBM((members, length + 2 * tok_rows, 128), jnp.bfloat16),
         in_specs=[SMEM] + [VMEM] * 7,
-        out_specs=VMEM,
+        out_specs=ANYWHERE,
+        scratch_shapes=[
+            pltpu.VMEM((length, 128), jnp.bfloat16),
+            pltpu.VMEM((members, 2 * tok_rows, 128), jnp.bfloat16),
+            pltpu.SemaphoreType.DMA((members * (1 + length // WINDOW),)),
+        ],
         cost_estimate=pl.CostEstimate(
             flops=4 * length * both * 3 * WINDOW,
             bytes_accessed=4 * members * length * 128,

time: 186 us -> 186 us (level)
  no operation moved by 1% of the time
where the time goes in v9:
time: 186 us; the launch traced here: 185 us
  blocking collectives  58.4 us (31%)
  starting transfers between devices  56.8 us (31%)
  waiting for transfers between devices  48.6 us (26%)
  Pallas kernels  19.8 us (11%)
    all_to_all x2, blocking collectives, exchange(): lax.all_to_all(value, axis, split_axis=0, concat_axis=0, tiled=True, axis...  58.4 us
    all_to_all x3, waiting for transfers between devices, exchange(): lax.all_to_all(value, axis, split_axis=0, concat_axis=0, tiled=True, axis...  42.2 us
    all_to_all x3, starting transfers between devices, exchange(): lax.all_to_all(value, axis, split_axis=0, concat_axis=0, tiled=True, axis...  28.9 us
    ppermute x4, starting transfers between devices, local(): received.append(lax.ppermute(packed[k % 2], ('sp', 'tp'), way))  12.5 us
    ppermute x4, starting transfers between devices, local(): forwarded.append(lax.ppermute(received[-1], ('sp', 'tp'), passes[k]))  10.2 us
    pallas_call x1, Pallas kernels, run_expert(): pl.pallas_call(expert_kernel, out_shape=jax.ShapeDtypeStruct((members, ro...  7.39 us
    ppermute x1, waiting for transfers between devices, local(): low = lax.ppermute(low, 'sp', forward)  4.9 us
    pallas_call x1, Pallas kernels, run_attention(): pl.pallas_call(attend_kernel, out_shape=pltpu.HBM((members, length + 2 *...  3.97 us
  transfers between devices with their start and end apart: 13, of which 5 were waited for; matrix products, arithmetic and copies ran while one was open for 0% of the time, Pallas kernels for 4%

profile of v9, /device:TPU:32, one launch (start us, length us, event | category | flops | bytes accessed | tf_op | source)
XLA Modules:
  0.0 185.3 jit_solution(9966185527597939673)
XLA Ops:
  0.0 3.3 %pack.1 = (bf16[480,2048]{1,0:T(8,128)(2,1)}, bf16[480,2048]{1,0:T(8,128)(2,1)}) custom-call(bf16[320,2048]{1,0:T(8,128)(2,1)} %bitcast.35, bf16[320,2048]{1,0:T(8,128)(2,1)} %bitcast.37, bf16[320,2048]{1,0:T(8,128)(2,1)} %bitcast.39), custom_call_target="tpu_custom_call" | custom-call | flops 655360 | bytes 7864320 | tf_op jit(solution)/shard_map/pack/pallas_call | solution.py:312
  3.3 3.9 %collective-permute-start.2 = (bf16[480,2048]{1,0:T(8,128)(2,1)}, bf16[480,2048]{1,0:T(8,128)(2,1)S(1)}, u32[]{:S(2)}, u32[]{:S(2)}) collective-permute-start(bf16[480,2048]{1,0:T(8,128)(2,1)} %get-tuple-element.25), channel_id=1, source_target_pairs={{0,21},{1,2},{2,23},{3,0},{4,5},{5,26},{6,7},{7,24},{8,29},{9,10},... | collective-permute-start | bytes 5898248 | tf_op jit(solution)/shard_map/ppermute | solution.py:526
  7.2 4.8 %collective-permute-start.3 = (bf16[480,2048]{1,0:T(8,128)(2,1)}, bf16[480,2048]{1,0:T(8,128)(2,1)}, u32[]{:S(2)}, u32[]{:S(2)}) collective-permute-start(bf16[480,2048]{1,0:T(8,128)(2,1)} %get-tuple-element.26), channel_id=1, source_target_pairs={{0,31},{1,0},{2,29},{3,2},{4,7},{5,16},{6,5},{7,18},{8,23},{9,8},{... | collective-permute-start | bytes 5898248 | tf_op jit(solution)/shard_map/ppermute | solution.py:526
  12.0 1.9 %collective-permute-start.4 = (bf16[480,2048]{1,0:T(8,128)(2,1)}, bf16[480,2048]{1,0:T(8,128)(2,1)}, u32[]{:S(2)}, u32[]{:S(2)}) collective-permute-start(bf16[480,2048]{1,0:T(8,128)(2,1)} %get-tuple-element.25), channel_id=1, source_target_pairs={{0,16},{1,5},{2,18},{3,7},{4,8},{5,21},{6,10},{7,23},{8,24},{9,13}... | collective-permute-start | bytes 5898248 | tf_op jit(solution)/shard_map/ppermute | solution.py:526
  13.9 1.9 %collective-permute-start.5 = (bf16[480,2048]{1,0:T(8,128)(2,1)}, bf16[480,2048]{1,0:T(8,128)(2,1)}, u32[]{:S(2)}, u32[]{:S(2)}) collective-permute-start(bf16[480,2048]{1,0:T(8,128)(2,1)} %get-tuple-element.26), channel_id=1, source_target_pairs={{0,16},{1,13},{2,18},{3,15},{4,0},{5,21},{6,2},{7,23},{8,24},{9,5}... | collective-permute-start | bytes 5898248 | tf_op jit(solution)/shard_map/ppermute | solution.py:526
  15.9 0.0 copy-start
  15.9 1.4 prepare.1
  17.3 3.3 %collective-permute-start = (bf16[128,128]{1,0:T(8,128)(2,1)S(1)}, bf16[128,128]{1,0:T(8,128)(2,1)S(1)}, u32[]{:S(2)}, u32[]{:S(2)}) collective-permute-start(bf16[128,128]{1,0:T(8,128)(2,1)S(1)} %get-tuple-element.18), channel_id=1, source_target_pairs={{0,16},{16,32},{32,48},{48,64},{64,80},{80,96},{96,112},{112,128},... | collective-permute-start | bytes 98312 | tf_op jit(solution)/shard_map/ppermute | solution.py:534
  20.6 4.9 %collective-permute-done.low = bf16[128,128]{1,0:T(8,128)(2,1)S(1)} collective-permute-done((bf16[128,128]{1,0:T(8,128)(2,1)S(1)}, bf16[128,128]{1,0:T(8,128)(2,1)S(1)}, u32[]{:S(2)}, u32[]{:S(2)}) %collective-permute-start) | collective-permute-done | bytes 32800 | tf_op jit(solution)/shard_map/ppermute | solution.py:534
  25.5 1.9 %collective-permute-start.1 = (bf16[128,128]{1,0:T(8,128)(2,1)S(1)}, bf16[128,128]{1,0:T(8,128)(2,1)S(1)}, u32[]{:S(2)}, u32[]{:S(2)}) collective-permute-start(bf16[128,128]{1,0:T(8,128)(2,1)S(1)} %get-tuple-element.20), channel_id=1, source_target_pairs={{16,0},{32,16},{48,32},{64,48},{80,64},{96,80},{112,96},{128,112},... | collective-permute-start | bytes 98312 | tf_op jit(solution)/shard_map/ppermute | solution.py:535
  27.4 0.1 pad_add_fusion.place
  27.5 1.5 collective-permute-done.1.high
  29.0 4.0 %attend.1 = bf16[16,288,128]{2,1,0:T(8,128)(2,1)} custom-call(s32[2]{0:T(128)S(1)} %pad_add_fusion.place, f32[1,2]{1,0:T(1,128)S(1)} %get-tuple-element.16.sink, bf16[256,128]{1,0:T(8,128)(2,1)S(1)} %get-tuple-element.17.queries, bf16[128,128]{1,0:T(8,128)(2,1)S(1)} %collective-permute-done.low, bf16[128,256]{1,0:T(8,128)(2,1)S(1)} %get-tuple-element.19.own, ...), custom_call_target="tpu_custom_call" | custom-call | flops 50331648 | bytes 2097152 | tf_op jit(solution)/shard_map/attend/pallas_call | solution.py:155
  33.0 38.2 %all_to_all.25.arrived = bf16[16,288,128]{2,1,0:T(8,128)(2,1)S(1)} all-to-all(bf16[16,288,128]{2,1,0:T(8,128)(2,1)} %attend.1), channel_id=1, replica_groups=mesh['sp'=32,'tp'=16] {'tp'}, dimensions={0} | all-to-all | bytes 2359296 | tf_op jit(solution)/shard_map/all_to_all | solution.py:280
  71.1 0.0 copy-done
  71.1 1.4 project.1
  72.6 0.0 copy-start.1
  72.6 15.3 %all-to-all-start.1 = ((bf16[16,64,128]{2,1,0:T(8,128)(2,1)}), bf16[16,64,128]{2,1,0:T(8,128)(2,1)S(1)}, u32[]{:S(2)}, u32[]{:S(2)}) async-start(bf16[16,64,128]{2,1,0:T(8,128)(2,1)} %get-tuple-element.23), calls=%async_computation.1 | async-start | bytes 524288 | tf_op jit(solution)/shard_map/all_to_all | solution.py:280
  87.9 0.0 collective-permute-done.2.got_0
  87.9 0.0 copy-start.2
  87.9 1.9 %collective-permute-start.6 = (bf16[480,2048]{1,0:T(8,128)(2,1)S(1)}, bf16[480,2048]{1,0:T(8,128)(2,1)}, u32[]{:S(2)}, u32[]{:S(2)}) collective-permute-start(bf16[480,2048]{1,0:T(8,128)(2,1)S(1)} %collective-permute-done.2.got_0), channel_id=1, source_target_pairs={{0,16},{1,17},{2,18},{3,19},{4,20},{5,21},{6,22},{7,23},{8,24},{9,... | collective-permute-start | bytes 5898248 | tf_op jit(solution)/shard_map/ppermute | solution.py:527
  89.8 0.0 collective-permute-done.3.got_1
  89.9 2.4 %collective-permute-start.7 = (bf16[480,2048]{1,0:T(8,128)(2,1)}, bf16[480,2048]{1,0:T(8,128)(2,1)}, u32[]{:S(2)}, u32[]{:S(2)}) collective-permute-start(bf16[480,2048]{1,0:T(8,128)(2,1)} %collective-permute-done.3.got_1), channel_id=1, source_target_pairs={{0,16},{1,17},{2,18},{3,19},{4,20},{5,21},{6,22},{7,23},{8,24},{9,... | collective-permute-start | bytes 5898248 | tf_op jit(solution)/shard_map/ppermute | solution.py:527
  92.3 0.0 collective-permute-done.4.got_2
  92.3 3.2 %collective-permute-start.8 = (bf16[480,2048]{1,0:T(8,128)(2,1)}, bf16[480,2048]{1,0:T(8,128)(2,1)}, u32[]{:S(2)}, u32[]{:S(2)}) collective-permute-start(bf16[480,2048]{1,0:T(8,128)(2,1)} %collective-permute-done.4.got_2), channel_id=1, source_target_pairs={{0,16},{2,18},{5,21},{7,23},{8,24},{10,26},{13,29},{15,31},{17,1},... | collective-permute-start | bytes 5898248 | tf_op jit(solution)/shard_map/ppermute | solution.py:527
  95.5 0.0 collective-permute-done.5.got_3
  95.5 2.6 %collective-permute-start.9 = (bf16[480,2048]{1,0:T(8,128)(2,1)}, bf16[480,2048]{1,0:T(8,128)(2,1)}, u32[]{:S(2)}, u32[]{:S(2)}) collective-permute-start(bf16[480,2048]{1,0:T(8,128)(2,1)} %collective-permute-done.5.got_3), channel_id=1, source_target_pairs={{0,16},{2,18},{5,21},{7,23},{8,24},{10,26},{13,29},{15,31},{17,1},... | collective-permute-start | bytes 5898248 | tf_op jit(solution)/shard_map/ppermute | solution.py:527
  98.1 7.1 %all-to-all-done.1.dispatched = bf16[16,64,128]{2,1,0:T(8,128)(2,1)S(1)} async-done(((bf16[16,64,128]{2,1,0:T(8,128)(2,1)}), bf16[16,64,128]{2,1,0:T(8,128)(2,1)S(1)}, u32[]{:S(2)}, u32[]{:S(2)}) %all-to-all-start.1) | async-done | bytes 262176 | tf_op jit(solution)/shard_map/all_to_all | solution.py:280
  105.2 1.3 spread.1
  106.6 6.4 %all-to-all-start.2 = ((bf16[16,256,128]{2,1,0:T(8,128)(2,1)}), bf16[16,256,128]{2,1,0:T(8,128)(2,1)S(1)}, u32[]{:S(2)}, u32[]{:S(2)}) async-start(bf16[16,256,128]{2,1,0:T(8,128)(2,1)} %spread.1), calls=%async_computation.2 | async-start | bytes 2097152 | tf_op jit(solution)/shard_map/all_to_all | solution.py:280
  113.1 17.6 %all-to-all-done.2.gathered = bf16[16,256,128]{2,1,0:T(8,128)(2,1)S(1)} async-done(((bf16[16,256,128]{2,1,0:T(8,128)(2,1)}), bf16[16,256,128]{2,1,0:T(8,128)(2,1)S(1)}, u32[]{:S(2)}, u32[]{:S(2)}) %all-to-all-start.2) | async-done | bytes 1048608 | tf_op jit(solution)/shard_map/all_to_all | solution.py:280
  130.7 0.0 collective-permute-done.6.fwd_0
  130.7 0.0 collective-permute-done.7.fwd_1
  130.7 0.0 collective-permute-done.8.fwd_2
  130.7 0.0 collective-permute-done.9.fwd_3
  130.7 0.0 copy-done.2
  130.7 0.0 copy-done.1
  130.7 7.4 %expert.1 = bf16[16,272,128]{2,1,0:T(8,128)(2,1)S(1)} custom-call(s32[1]{0:T(128)} %bitcast.serves, bf16[16,256,128]{2,1,0:T(8,128)(2,1)S(1)} %all-to-all-done.2.gathered, bf16[256,128]{1,0:T(8,128)(2,1)S(1)} %get-tuple-element.24.own, f32[1,2048]{1,0:T(1,128)S(1)} %bitcast.34, bf16[320,2048]{1,0:T(8,128)(2,1)} %bitcast.36, bf16[320,2048]{1,0:T(8,128)(2,1)} %bitcast.38, ...), custom_call_target="tpu_custom_call" | custom-call | flops 4026531840 | bytes 17825792 | tf_op jit(solution)/shard_map/expert/pallas_call | solution.py:426
  138.1 0.0 copy-start.4
  138.1 20.3 %all_to_all.26.shares = bf16[16,272,128]{2,1,0:T(8,128)(2,1)S(1)} all-to-all(bf16[16,272,128]{2,1,0:T(8,128)(2,1)S(1)} %expert.1), channel_id=1, replica_groups=mesh['sp'=32,'tp'=16] {'tp'}, dimensions={0} | all-to-all | bytes 2228224 | tf_op jit(solution)/shard_map/all_to_all | solution.py:280
  158.4 0.0 copy-start.3
  158.4 1.0 shares.1
  159.4 7.2 %all-to-all-start.4 = ((bf16[16,64,128]{2,1,0:T(8,128)(2,1)}), bf16[16,64,128]{2,1,0:T(8,128)(2,1)S(1)}, u32[]{:S(2)}, u32[]{:S(2)}) async-start(bf16[16,64,128]{2,1,0:T(8,128)(2,1)} %shares.1), calls=%async_computation.4 | async-start | bytes 524288 | tf_op jit(solution)/shard_map/all_to_all | solution.py:280
  166.6 0.1 copy.16
  166.7 0.0 copy-done.4
  166.7 0.1 iota_compare_fusion
  166.8 17.4 %all-to-all-done.4 = bf16[16,64,128]{2,1,0:T(8,128)(2,1)S(1)} async-done(((bf16[16,64,128]{2,1,0:T(8,128)(2,1)}), bf16[16,64,128]{2,1,0:T(8,128)(2,1)S(1)}, u32[]{:S(2)}, u32[]{:S(2)}) %all-to-all-start.4) | async-done | bytes 262176 | tf_op jit(solution)/shard_map/all_to_all | solution.py:280
  184.2 0.1 reshape.22
  184.3 0.2 convolution_multiply_fusion.1
  184.5 0.0 copy-done.3
  184.5 0.8 fusion.2
  (2 shorter events, 0.0 us)
Async XLA Ops:
  3.3 84.6 %collective-permute-start.2 = (bf16[480,2048]{1,0:T(8,128)(2,1)}, bf16[480,2048]{1,0:T(8,128)(2,1)S(1)}, u32[]{:S(2)}, u32[]{:S(2)}) collective-permute-start(bf16[480,2048]{1,0:T(8,128)(2,1)} %get-tuple-element.25), channel_id=1, source_target_pairs={{0,21},{1,2},{2,23},{3,0},{4,5},{5,26},{6,7},{7,24},{8,29},{9,10},... | collective-permute-start | bytes 5898248 | tf_op jit(solution)/shard_map/ppermute | solution.py:526
  7.2 82.7 %collective-permute-start.3 = (bf16[480,2048]{1,0:T(8,128)(2,1)}, bf16[480,2048]{1,0:T(8,128)(2,1)}, u32[]{:S(2)}, u32[]{:S(2)}) collective-permute-start(bf16[480,2048]{1,0:T(8,128)(2,1)} %get-tuple-element.26), channel_id=1, source_target_pairs={{0,31},{1,0},{2,29},{3,2},{4,7},{5,16},{6,5},{7,18},{8,23},{9,8},{... | collective-permute-start | bytes 5898248 | tf_op jit(solution)/shard_map/ppermute | solution.py:526
  12.0 80.3 %collective-permute-start.4 = (bf16[480,2048]{1,0:T(8,128)(2,1)}, bf16[480,2048]{1,0:T(8,128)(2,1)}, u32[]{:S(2)}, u32[]{:S(2)}) collective-permute-start(bf16[480,2048]{1,0:T(8,128)(2,1)} %get-tuple-element.25), channel_id=1, source_target_pairs={{0,16},{1,5},{2,18},{3,7},{4,8},{5,21},{6,10},{7,23},{8,24},{9,13}... | collective-permute-start | bytes 5898248 | tf_op jit(solution)/shard_map/ppermute | solution.py:526
  13.9 81.6 %collective-permute-start.5 = (bf16[480,2048]{1,0:T(8,128)(2,1)}, bf16[480,2048]{1,0:T(8,128)(2,1)}, u32[]{:S(2)}, u32[]{:S(2)}) collective-permute-start(bf16[480,2048]{1,0:T(8,128)(2,1)} %get-tuple-element.26), channel_id=1, source_target_pairs={{0,16},{1,13},{2,18},{3,15},{4,0},{5,21},{6,2},{7,23},{8,24},{9,5}... | collective-permute-start | bytes 5898248 | tf_op jit(solution)/shard_map/ppermute | solution.py:526
  15.9 55.3 %copy-start = (bf16[2048,128]{1,0:T(8,128)(2,1)S(1)}, bf16[2048,128]{1,0:T(8,128)(2,1)}, u32[]{:S(2)}) copy-start(bf16[2048,128]{1,0:T(8,128)(2,1)} %weight.1) | copy-start | bytes 1572868
  17.3 8.2 %collective-permute-start = (bf16[128,128]{1,0:T(8,128)(2,1)S(1)}, bf16[128,128]{1,0:T(8,128)(2,1)S(1)}, u32[]{:S(2)}, u32[]{:S(2)}) collective-permute-start(bf16[128,128]{1,0:T(8,128)(2,1)S(1)} %get-tuple-element.18), channel_id=1, source_target_pairs={{0,16},{16,32},{32,48},{48,64},{64,80},{80,96},{96,112},{112,128},... | collective-permute-start | bytes 98312 | tf_op jit(solution)/shard_map/ppermute | solution.py:534
  25.5 3.5 %collective-permute-start.1 = (bf16[128,128]{1,0:T(8,128)(2,1)S(1)}, bf16[128,128]{1,0:T(8,128)(2,1)S(1)}, u32[]{:S(2)}, u32[]{:S(2)}) collective-permute-start(bf16[128,128]{1,0:T(8,128)(2,1)S(1)} %get-tuple-element.20), channel_id=1, source_target_pairs={{16,0},{32,16},{48,32},{64,48},{80,64},{96,80},{112,96},{128,112},... | collective-permute-start | bytes 98312 | tf_op jit(solution)/shard_map/ppermute | solution.py:535
  72.6 58.2 %copy-start.1 = (f32[2048]{0:T(1024)S(1)}, f32[2048]{0:T(1024)}, u32[]{:S(2)}) copy-start(f32[2048]{0:T(1024)} %param.18) | copy-start | bytes 24580
  72.6 32.7 %all-to-all-start.1 = ((bf16[16,64,128]{2,1,0:T(8,128)(2,1)}), bf16[16,64,128]{2,1,0:T(8,128)(2,1)S(1)}, u32[]{:S(2)}, u32[]{:S(2)}) async-start(bf16[16,64,128]{2,1,0:T(8,128)(2,1)} %get-tuple-element.23), calls=%async_computation.1 | async-start | bytes 524288 | tf_op jit(solution)/shard_map/all_to_all | solution.py:280
  87.9 42.8 %copy-start.2 = (bf16[480,2048]{1,0:T(8,128)(2,1)}, bf16[480,2048]{1,0:T(8,128)(2,1)S(1)}, u32[]{:S(2)}) copy-start(bf16[480,2048]{1,0:T(8,128)(2,1)S(1)} %collective-permute-done.2.got_0) | copy-start | bytes 5898244
  87.9 42.8 %collective-permute-start.6 = (bf16[480,2048]{1,0:T(8,128)(2,1)S(1)}, bf16[480,2048]{1,0:T(8,128)(2,1)}, u32[]{:S(2)}, u32[]{:S(2)}) collective-permute-start(bf16[480,2048]{1,0:T(8,128)(2,1)S(1)} %collective-permute-done.2.got_0), channel_id=1, source_target_pairs={{0,16},{1,17},{2,18},{3,19},{4,20},{5,21},{6,22},{7,23},{8,24},{9,... | collective-permute-start | bytes 5898248 | tf_op jit(solution)/shard_map/ppermute | solution.py:527
  89.9 40.8 %collective-permute-start.7 = (bf16[480,2048]{1,0:T(8,128)(2,1)}, bf16[480,2048]{1,0:T(8,128)(2,1)}, u32[]{:S(2)}, u32[]{:S(2)}) collective-permute-start(bf16[480,2048]{1,0:T(8,128)(2,1)} %collective-permute-done.3.got_1), channel_id=1, source_target_pairs={{0,16},{1,17},{2,18},{3,19},{4,20},{5,21},{6,22},{7,23},{8,24},{9,... | collective-permute-start | bytes 5898248 | tf_op jit(solution)/shard_map/ppermute | solution.py:527
  92.3 38.4 %collective-permute-start.8 = (bf16[480,2048]{1,0:T(8,128)(2,1)}, bf16[480,2048]{1,0:T(8,128)(2,1)}, u32[]{:S(2)}, u32[]{:S(2)}) collective-permute-start(bf16[480,2048]{1,0:T(8,128)(2,1)} %collective-permute-done.4.got_2), channel_id=1, source_target_pairs={{0,16},{2,18},{5,21},{7,23},{8,24},{10,26},{13,29},{15,31},{17,1},... | collective-permute-start | bytes 5898248 | tf_op jit(solution)/shard_map/ppermute | solution.py:527
  95.5 35.2 %collective-permute-start.9 = (bf16[480,2048]{1,0:T(8,128)(2,1)}, bf16[480,2048]{1,0:T(8,128)(2,1)}, u32[]{:S(2)}, u32[]{:S(2)}) collective-permute-start(bf16[480,2048]{1,0:T(8,128)(2,1)} %collective-permute-done.5.got_3), channel_id=1, source_target_pairs={{0,16},{2,18},{5,21},{7,23},{8,24},{10,26},{13,29},{15,31},{17,1},... | collective-permute-start | bytes 5898248 | tf_op jit(solution)/shard_map/ppermute | solution.py:527
  106.6 24.1 %all-to-all-start.2 = ((bf16[16,256,128]{2,1,0:T(8,128)(2,1)}), bf16[16,256,128]{2,1,0:T(8,128)(2,1)S(1)}, u32[]{:S(2)}, u32[]{:S(2)}) async-start(bf16[16,256,128]{2,1,0:T(8,128)(2,1)} %spread.1), calls=%async_computation.2 | async-start | bytes 2097152 | tf_op jit(solution)/shard_map/all_to_all | solution.py:280
  138.1 28.5 %copy-start.4 = (f32[16,2]{0,1:T(2,128)S(1)}, f32[16,2]{0,1:T(2,128)}, u32[]{:S(2)}) copy-start(f32[16,2]{0,1:T(2,128)} %param.20) | copy-start | bytes 388
  158.4 26.1 %copy-start.3 = (bf16[16,2048]{1,0:T(8,128)(2,1)S(1)}, bf16[16,2048]{1,0:T(8,128)(2,1)}, u32[]{:S(2)}) copy-start(bf16[16,2048]{1,0:T(8,128)(2,1)} %residual.1) | copy-start | bytes 196612
  159.4 24.8 %all-to-all-start.4 = ((bf16[16,64,128]{2,1,0:T(8,128)(2,1)}), bf16[16,64,128]{2,1,0:T(8,128)(2,1)S(1)}, u32[]{:S(2)}, u32[]{:S(2)}) async-start(bf16[16,64,128]{2,1,0:T(8,128)(2,1)} %shares.1), calls=%async_computation.4 | async-start | bytes 524288 | tf_op jit(solution)/shard_map/all_to_all | solution.py:280

commit v10 on v8

--- a/solution.py
+++ b/solution.py
@@ -487,15 +487,15 @@
                 y, x = member // 4, member % 4
                 right = served_side(member) == core
                 for k, (dy, dx) in enumerate(steps):
-                    if right and k < 2:
-                        dy, dx = diagonal[k]
+                    if right and k >= 2:
+                        dy, dx = diagonal[k - 2]
                         target = across + (y + dy) % 4 * 4 + (x + dx) % 4
                     elif right:
                         target = across + member
                     else:
                         target = base + (y + dy) % 4 * 4 + (x + dx) % 4
                     moves[k].append((base + member, target))
-                    if right or k < 2:
+                    if right or k >= 2:
                         passes[k].append((base + member, across + member))
     core_index = lax.axis_index("sp") % 2
     serves = (core_index == served_side(lax.axis_index("tp"))).astype(jnp.int32).reshape(1)
@@ -522,7 +522,7 @@
     dispatched = exchange(sending, "sp", same_core)
     to_servers = spread(dispatched, n_tp)
     gathered = exchange(to_servers, "tp")
-    pieces = run_expert(serves, gathered, own, norm_gain, owned, (*received, *forwarded))
+    pieces = run_expert(serves, gathered, own, norm_gain, owned, (*received, *forwarded[2:], *forwarded[:2]))
 
     shares = exchange(pieces, "tp")
     own_rows = shares[:, n_tp * planes :].transpose(1, 0, 2).reshape(tok_rows, width)

time: 186 us -> 183 us (0.984)
  blocking collectives: 59.7 us -> 57.8 us
    all_to_all x2, blocking collectives: 59.7 us -> 57.8 us  [exchange(): lax.all_to_all(value, axis, split_axis=0, concat_axis=0, tiled=True, axis...]
where the time goes in v10:
time: 183 us
  blocking collectives  57.8 us (32%)
  starting transfers between devices  56.7 us (31%)
  waiting for transfers between devices  48.2 us (26%)
  Pallas kernels  18.5 us (10%)
    all_to_all x2, blocking collectives, exchange(): lax.all_to_all(value, axis, split_axis=0, concat_axis=0, tiled=True, axis...  57.8 us
    all_to_all x3, waiting for transfers between devices, exchange(): lax.all_to_all(value, axis, split_axis=0, concat_axis=0, tiled=True, axis...  41.6 us
    all_to_all x3, starting transfers between devices, exchange(): lax.all_to_all(value, axis, split_axis=0, concat_axis=0, tiled=True, axis...  28.9 us
    ppermute x4, starting transfers between devices, local(): received.append(lax.ppermute(packed[k % 2], ('sp', 'tp'), way))  12.3 us
    ppermute x4, starting transfers between devices, local(): forwarded.append(lax.ppermute(received[-1], ('sp', 'tp'), passes[k]))  10.2 us
    pallas_call x1, Pallas kernels, run_expert(): pl.pallas_call(expert_kernel, out_shape=jax.ShapeDtypeStruct((members, ro...  7.39 us
    ppermute x1, waiting for transfers between devices, local(): low = lax.ppermute(low, 'sp', forward)  5.08 us
  transfers between devices with their start and end apart: 13, of which 5 were waited for; matrix products, arithmetic and copies ran while one was open for 0% of the time, Pallas kernels for 4%

profile of v10, /device:TPU:32, one launch (start us, length us, event | category | flops | bytes accessed | tf_op | source)
XLA Modules:
  0.0 182.7 jit_solution(18300895894375109730)
XLA Ops:
  0.0 3.3 %pack.1 = (bf16[480,2048]{1,0:T(8,128)(2,1)}, bf16[480,2048]{1,0:T(8,128)(2,1)}) custom-call(bf16[320,2048]{1,0:T(8,128)(2,1)} %bitcast.35, bf16[320,2048]{1,0:T(8,128)(2,1)} %bitcast.37, bf16[320,2048]{1,0:T(8,128)(2,1)} %bitcast.39), custom_call_target="tpu_custom_call" | custom-call | flops 655360 | bytes 7864320 | tf_op jit(solution)/shard_map/pack/pallas_call | solution.py:292
  3.3 3.9 %collective-permute-start.4 = (bf16[480,2048]{1,0:T(8,128)(2,1)}, bf16[480,2048]{1,0:T(8,128)(2,1)S(1)}, u32[]{:S(2)}, u32[]{:S(2)}) collective-permute-start(bf16[480,2048]{1,0:T(8,128)(2,1)} %get-tuple-element.25), channel_id=1, source_target_pairs={{0,21},{1,5},{2,23},{3,7},{4,8},{5,26},{6,10},{7,24},{8,29},{9,13}... | collective-permute-start | bytes 5898248 | tf_op jit(solution)/shard_map/ppermute | solution.py:506
  7.2 4.6 %collective-permute-start.5 = (bf16[480,2048]{1,0:T(8,128)(2,1)}, bf16[480,2048]{1,0:T(8,128)(2,1)}, u32[]{:S(2)}, u32[]{:S(2)}) collective-permute-start(bf16[480,2048]{1,0:T(8,128)(2,1)} %get-tuple-element.26), channel_id=1, source_target_pairs={{0,31},{1,13},{2,29},{3,15},{4,0},{5,16},{6,2},{7,18},{8,23},{9,5}... | collective-permute-start | bytes 5898248 | tf_op jit(solution)/shard_map/ppermute | solution.py:506
  11.8 1.9 %collective-permute-start.2 = (bf16[480,2048]{1,0:T(8,128)(2,1)}, bf16[480,2048]{1,0:T(8,128)(2,1)}, u32[]{:S(2)}, u32[]{:S(2)}) collective-permute-start(bf16[480,2048]{1,0:T(8,128)(2,1)} %get-tuple-element.25), channel_id=1, source_target_pairs={{0,16},{1,2},{2,18},{3,0},{4,5},{5,21},{6,7},{7,23},{8,24},{9,10},... | collective-permute-start | bytes 5898248 | tf_op jit(solution)/shard_map/ppermute | solution.py:506
  13.7 1.9 %collective-permute-start.3 = (bf16[480,2048]{1,0:T(8,128)(2,1)}, bf16[480,2048]{1,0:T(8,128)(2,1)}, u32[]{:S(2)}, u32[]{:S(2)}) collective-permute-start(bf16[480,2048]{1,0:T(8,128)(2,1)} %get-tuple-element.26), channel_id=1, source_target_pairs={{0,16},{1,0},{2,18},{3,2},{4,7},{5,21},{6,5},{7,23},{8,24},{9,8},{... | collective-permute-start | bytes 5898248 | tf_op jit(solution)/shard_map/ppermute | solution.py:506
  15.7 0.0 copy-start
  15.7 1.4 prepare.1
  17.1 3.3 %collective-permute-start = (bf16[128,128]{1,0:T(8,128)(2,1)S(1)}, bf16[128,128]{1,0:T(8,128)(2,1)S(1)}, u32[]{:S(2)}, u32[]{:S(2)}) collective-permute-start(bf16[128,128]{1,0:T(8,128)(2,1)S(1)} %get-tuple-element.18), channel_id=1, source_target_pairs={{0,16},{16,32},{32,48},{48,64},{64,80},{80,96},{96,112},{112,128},... | collective-permute-start | bytes 98312 | tf_op jit(solution)/shard_map/ppermute | solution.py:514
  20.4 5.1 %collective-permute-done.low = bf16[128,128]{1,0:T(8,128)(2,1)S(1)} collective-permute-done((bf16[128,128]{1,0:T(8,128)(2,1)S(1)}, bf16[128,128]{1,0:T(8,128)(2,1)S(1)}, u32[]{:S(2)}, u32[]{:S(2)}) %collective-permute-start) | collective-permute-done | bytes 32800 | tf_op jit(solution)/shard_map/ppermute | solution.py:514
  25.5 1.9 %collective-permute-start.1 = (bf16[128,128]{1,0:T(8,128)(2,1)S(1)}, bf16[128,128]{1,0:T(8,128)(2,1)S(1)}, u32[]{:S(2)}, u32[]{:S(2)}) collective-permute-start(bf16[128,128]{1,0:T(8,128)(2,1)S(1)} %get-tuple-element.20), channel_id=1, source_target_pairs={{16,0},{32,16},{48,32},{64,48},{80,64},{96,80},{112,96},{128,112},... | collective-permute-start | bytes 98312 | tf_op jit(solution)/shard_map/ppermute | solution.py:515
  27.4 0.1 pad_add_fusion.place
  27.5 1.5 collective-permute-done.1.high
  29.0 2.7 %attend.1 = bf16[16,288,128]{2,1,0:T(8,128)(2,1)S(1)} custom-call(s32[2]{0:T(128)S(1)} %pad_add_fusion.place, f32[1,2]{1,0:T(1,128)S(1)} %get-tuple-element.16.sink, bf16[256,128]{1,0:T(8,128)(2,1)S(1)} %get-tuple-element.17.queries, bf16[128,128]{1,0:T(8,128)(2,1)S(1)} %collective-permute-done.low, bf16[128,256]{1,0:T(8,128)(2,1)S(1)} %get-tuple-element.19.own, ...), custom_call_target="tpu_custom_call" | custom-call | flops 50331648 | bytes 2097152 | tf_op jit(solution)/shard_map/attend/pallas_call | solution.py:140
  31.7 37.6 %all_to_all.25.arrived = bf16[16,288,128]{2,1,0:T(8,128)(2,1)S(1)} all-to-all(bf16[16,288,128]{2,1,0:T(8,128)(2,1)S(1)} %attend.1), channel_id=1, replica_groups=mesh['sp'=32,'tp'=16] {'tp'}, dimensions={0} | all-to-all | bytes 2359296 | tf_op jit(solution)/shard_map/all_to_all | solution.py:260
  69.3 0.0 copy-done
  69.3 1.4 project.1
  70.7 0.0 copy-start.1
  70.7 15.4 %all-to-all-start.1 = ((bf16[16,64,128]{2,1,0:T(8,128)(2,1)}), bf16[16,64,128]{2,1,0:T(8,128)(2,1)S(1)}, u32[]{:S(2)}, u32[]{:S(2)}) async-start(bf16[16,64,128]{2,1,0:T(8,128)(2,1)} %get-tuple-element.23), calls=%async_computation.1 | async-start | bytes 524288 | tf_op jit(solution)/shard_map/all_to_all | solution.py:260
  86.1 0.0 collective-permute-done.4.got_2
  86.1 0.0 copy-start.2
  86.1 1.9 %collective-permute-start.6 = (bf16[480,2048]{1,0:T(8,128)(2,1)S(1)}, bf16[480,2048]{1,0:T(8,128)(2,1)}, u32[]{:S(2)}, u32[]{:S(2)}) collective-permute-start(bf16[480,2048]{1,0:T(8,128)(2,1)S(1)} %collective-permute-done.4.got_2), channel_id=1, source_target_pairs={{0,16},{1,17},{2,18},{3,19},{4,20},{5,21},{6,22},{7,23},{8,24},{9,... | collective-permute-start | bytes 5898248 | tf_op jit(solution)/shard_map/ppermute | solution.py:507
  88.0 0.0 collective-permute-done.5.got_3
  88.0 2.4 %collective-permute-start.7 = (bf16[480,2048]{1,0:T(8,128)(2,1)}, bf16[480,2048]{1,0:T(8,128)(2,1)}, u32[]{:S(2)}, u32[]{:S(2)}) collective-permute-start(bf16[480,2048]{1,0:T(8,128)(2,1)} %collective-permute-done.5.got_3), channel_id=1, source_target_pairs={{0,16},{1,17},{2,18},{3,19},{4,20},{5,21},{6,22},{7,23},{8,24},{9,... | collective-permute-start | bytes 5898248 | tf_op jit(solution)/shard_map/ppermute | solution.py:507
  90.4 0.0 collective-permute-done.2.got_0
  90.4 3.3 %collective-permute-start.8 = (bf16[480,2048]{1,0:T(8,128)(2,1)}, bf16[480,2048]{1,0:T(8,128)(2,1)}, u32[]{:S(2)}, u32[]{:S(2)}) collective-permute-start(bf16[480,2048]{1,0:T(8,128)(2,1)} %collective-permute-done.2.got_0), channel_id=1, source_target_pairs={{0,16},{2,18},{5,21},{7,23},{8,24},{10,26},{13,29},{15,31},{17,1},... | collective-permute-start | bytes 5898248 | tf_op jit(solution)/shard_map/ppermute | solution.py:507
  93.7 0.0 collective-permute-done.3.got_1
  93.7 2.6 %collective-permute-start.9 = (bf16[480,2048]{1,0:T(8,128)(2,1)}, bf16[480,2048]{1,0:T(8,128)(2,1)}, u32[]{:S(2)}, u32[]{:S(2)}) collective-permute-start(bf16[480,2048]{1,0:T(8,128)(2,1)} %collective-permute-done.3.got_1), channel_id=1, source_target_pairs={{0,16},{2,18},{5,21},{7,23},{8,24},{10,26},{13,29},{15,31},{17,1},... | collective-permute-start | bytes 5898248 | tf_op jit(solution)/shard_map/ppermute | solution.py:507
  96.3 7.3 %all-to-all-done.1.dispatched = bf16[16,64,128]{2,1,0:T(8,128)(2,1)S(1)} async-done(((bf16[16,64,128]{2,1,0:T(8,128)(2,1)}), bf16[16,64,128]{2,1,0:T(8,128)(2,1)S(1)}, u32[]{:S(2)}, u32[]{:S(2)}) %all-to-all-start.1) | async-done | bytes 262176 | tf_op jit(solution)/shard_map/all_to_all | solution.py:260
  103.6 1.3 spread.1
  104.9 6.5 %all-to-all-start.2 = ((bf16[16,256,128]{2,1,0:T(8,128)(2,1)}), bf16[16,256,128]{2,1,0:T(8,128)(2,1)S(1)}, u32[]{:S(2)}, u32[]{:S(2)}) async-start(bf16[16,256,128]{2,1,0:T(8,128)(2,1)} %spread.1), calls=%async_computation.2 | async-start | bytes 2097152 | tf_op jit(solution)/shard_map/all_to_all | solution.py:260
  111.5 16.8 %all-to-all-done.2.gathered = bf16[16,256,128]{2,1,0:T(8,128)(2,1)S(1)} async-done(((bf16[16,256,128]{2,1,0:T(8,128)(2,1)}), bf16[16,256,128]{2,1,0:T(8,128)(2,1)S(1)}, u32[]{:S(2)}, u32[]{:S(2)}) %all-to-all-start.2) | async-done | bytes 1048608 | tf_op jit(solution)/shard_map/all_to_all | solution.py:260
  128.3 0.0 collective-permute-done.6.fwd_0
  128.3 0.0 collective-permute-done.7.fwd_1
  128.3 0.0 collective-permute-done.8.fwd_2
  128.3 0.0 collective-permute-done.9.fwd_3
  128.3 0.0 copy-done.2
  128.3 0.0 copy-done.1
  128.3 7.4 %expert.1 = bf16[16,272,128]{2,1,0:T(8,128)(2,1)S(1)} custom-call(s32[1]{0:T(128)} %bitcast.serves, bf16[16,256,128]{2,1,0:T(8,128)(2,1)S(1)} %all-to-all-done.2.gathered, bf16[256,128]{1,0:T(8,128)(2,1)S(1)} %get-tuple-element.24.own, f32[1,2048]{1,0:T(1,128)S(1)} %bitcast.34, bf16[320,2048]{1,0:T(8,128)(2,1)} %bitcast.36, bf16[320,2048]{1,0:T(8,128)(2,1)} %bitcast.38, ...), custom_call_target="tpu_custom_call" | custom-call | flops 4026531840 | bytes 17825792 | tf_op jit(solution)/shard_map/expert/pallas_call | solution.py:406
  135.7 0.0 copy-start.4
  135.7 20.2 %all_to_all.26.shares = bf16[16,272,128]{2,1,0:T(8,128)(2,1)S(1)} all-to-all(bf16[16,272,128]{2,1,0:T(8,128)(2,1)S(1)} %expert.1), channel_id=1, replica_groups=mesh['sp'=32,'tp'=16] {'tp'}, dimensions={0} | all-to-all | bytes 2228224 | tf_op jit(solution)/shard_map/all_to_all | solution.py:260
  155.9 0.0 copy-start.3
  155.9 1.0 shares.1
  156.9 7.1 %all-to-all-start.4 = ((bf16[16,64,128]{2,1,0:T(8,128)(2,1)}), bf16[16,64,128]{2,1,0:T(8,128)(2,1)S(1)}, u32[]{:S(2)}, u32[]{:S(2)}) async-start(bf16[16,64,128]{2,1,0:T(8,128)(2,1)} %shares.1), calls=%async_computation.4 | async-start | bytes 524288 | tf_op jit(solution)/shard_map/all_to_all | solution.py:260
  164.0 0.1 copy.16
  164.1 0.0 copy-done.4
  164.1 0.1 iota_compare_fusion
  164.2 17.5 %all-to-all-done.4 = bf16[16,64,128]{2,1,0:T(8,128)(2,1)S(1)} async-done(((bf16[16,64,128]{2,1,0:T(8,128)(2,1)}), bf16[16,64,128]{2,1,0:T(8,128)(2,1)S(1)}, u32[]{:S(2)}, u32[]{:S(2)}) %all-to-all-start.4) | async-done | bytes 262176 | tf_op jit(solution)/shard_map/all_to_all | solution.py:260
  181.7 0.1 reshape.22
  181.8 0.2 convolution_multiply_fusion.1
  181.9 0.0 copy-done.3
  181.9 0.8 fusion.2
  (2 shorter events, 0.0 us)
Async XLA Ops:
  3.3 82.7 %collective-permute-start.4 = (bf16[480,2048]{1,0:T(8,128)(2,1)}, bf16[480,2048]{1,0:T(8,128)(2,1)S(1)}, u32[]{:S(2)}, u32[]{:S(2)}) collective-permute-start(bf16[480,2048]{1,0:T(8,128)(2,1)} %get-tuple-element.25), channel_id=1, source_target_pairs={{0,21},{1,5},{2,23},{3,7},{4,8},{5,26},{6,10},{7,24},{8,29},{9,13}... | collective-permute-start | bytes 5898248 | tf_op jit(solution)/shard_map/ppermute | solution.py:506
  7.2 80.8 %collective-permute-start.5 = (bf16[480,2048]{1,0:T(8,128)(2,1)}, bf16[480,2048]{1,0:T(8,128)(2,1)}, u32[]{:S(2)}, u32[]{:S(2)}) collective-permute-start(bf16[480,2048]{1,0:T(8,128)(2,1)} %get-tuple-element.26), channel_id=1, source_target_pairs={{0,31},{1,13},{2,29},{3,15},{4,0},{5,16},{6,2},{7,18},{8,23},{9,5}... | collective-permute-start | bytes 5898248 | tf_op jit(solution)/shard_map/ppermute | solution.py:506
  11.8 78.6 %collective-permute-start.2 = (bf16[480,2048]{1,0:T(8,128)(2,1)}, bf16[480,2048]{1,0:T(8,128)(2,1)}, u32[]{:S(2)}, u32[]{:S(2)}) collective-permute-start(bf16[480,2048]{1,0:T(8,128)(2,1)} %get-tuple-element.25), channel_id=1, source_target_pairs={{0,16},{1,2},{2,18},{3,0},{4,5},{5,21},{6,7},{7,23},{8,24},{9,10},... | collective-permute-start | bytes 5898248 | tf_op jit(solution)/shard_map/ppermute | solution.py:506
  13.7 80.0 %collective-permute-start.3 = (bf16[480,2048]{1,0:T(8,128)(2,1)}, bf16[480,2048]{1,0:T(8,128)(2,1)}, u32[]{:S(2)}, u32[]{:S(2)}) collective-permute-start(bf16[480,2048]{1,0:T(8,128)(2,1)} %get-tuple-element.26), channel_id=1, source_target_pairs={{0,16},{1,0},{2,18},{3,2},{4,7},{5,21},{6,5},{7,23},{8,24},{9,8},{... | collective-permute-start | bytes 5898248 | tf_op jit(solution)/shard_map/ppermute | solution.py:506
  15.7 53.6 %copy-start = (bf16[2048,128]{1,0:T(8,128)(2,1)S(1)}, bf16[2048,128]{1,0:T(8,128)(2,1)}, u32[]{:S(2)}) copy-start(bf16[2048,128]{1,0:T(8,128)(2,1)} %weight.1) | copy-start | bytes 1572868
  17.1 8.4 %collective-permute-start = (bf16[128,128]{1,0:T(8,128)(2,1)S(1)}, bf16[128,128]{1,0:T(8,128)(2,1)S(1)}, u32[]{:S(2)}, u32[]{:S(2)}) collective-permute-start(bf16[128,128]{1,0:T(8,128)(2,1)S(1)} %get-tuple-element.18), channel_id=1, source_target_pairs={{0,16},{16,32},{32,48},{48,64},{64,80},{80,96},{96,112},{112,128},... | collective-permute-start | bytes 98312 | tf_op jit(solution)/shard_map/ppermute | solution.py:514
  25.5 3.5 %collective-permute-start.1 = (bf16[128,128]{1,0:T(8,128)(2,1)S(1)}, bf16[128,128]{1,0:T(8,128)(2,1)S(1)}, u32[]{:S(2)}, u32[]{:S(2)}) collective-permute-start(bf16[128,128]{1,0:T(8,128)(2,1)S(1)} %get-tuple-element.20), channel_id=1, source_target_pairs={{16,0},{32,16},{48,32},{64,48},{80,64},{96,80},{112,96},{128,112},... | collective-permute-start | bytes 98312 | tf_op jit(solution)/shard_map/ppermute | solution.py:515
  70.7 57.6 %copy-start.1 = (f32[2048]{0:T(1024)S(1)}, f32[2048]{0:T(1024)}, u32[]{:S(2)}) copy-start(f32[2048]{0:T(1024)} %param.18) | copy-start | bytes 24580
  70.7 32.9 %all-to-all-start.1 = ((bf16[16,64,128]{2,1,0:T(8,128)(2,1)}), bf16[16,64,128]{2,1,0:T(8,128)(2,1)S(1)}, u32[]{:S(2)}, u32[]{:S(2)}) async-start(bf16[16,64,128]{2,1,0:T(8,128)(2,1)} %get-tuple-element.23), calls=%async_computation.1 | async-start | bytes 524288 | tf_op jit(solution)/shard_map/all_to_all | solution.py:260
  86.1 42.2 %copy-start.2 = (bf16[480,2048]{1,0:T(8,128)(2,1)}, bf16[480,2048]{1,0:T(8,128)(2,1)S(1)}, u32[]{:S(2)}) copy-start(bf16[480,2048]{1,0:T(8,128)(2,1)S(1)} %collective-permute-done.4.got_2) | copy-start | bytes 5898244
  86.1 42.2 %collective-permute-start.6 = (bf16[480,2048]{1,0:T(8,128)(2,1)S(1)}, bf16[480,2048]{1,0:T(8,128)(2,1)}, u32[]{:S(2)}, u32[]{:S(2)}) collective-permute-start(bf16[480,2048]{1,0:T(8,128)(2,1)S(1)} %collective-permute-done.4.got_2), channel_id=1, source_target_pairs={{0,16},{1,17},{2,18},{3,19},{4,20},{5,21},{6,22},{7,23},{8,24},{9,... | collective-permute-start | bytes 5898248 | tf_op jit(solution)/shard_map/ppermute | solution.py:507
  88.0 40.3 %collective-permute-start.7 = (bf16[480,2048]{1,0:T(8,128)(2,1)}, bf16[480,2048]{1,0:T(8,128)(2,1)}, u32[]{:S(2)}, u32[]{:S(2)}) collective-permute-start(bf16[480,2048]{1,0:T(8,128)(2,1)} %collective-permute-done.5.got_3), channel_id=1, source_target_pairs={{0,16},{1,17},{2,18},{3,19},{4,20},{5,21},{6,22},{7,23},{8,24},{9,... | collective-permute-start | bytes 5898248 | tf_op jit(solution)/shard_map/ppermute | solution.py:507
  90.4 37.9 %collective-permute-start.8 = (bf16[480,2048]{1,0:T(8,128)(2,1)}, bf16[480,2048]{1,0:T(8,128)(2,1)}, u32[]{:S(2)}, u32[]{:S(2)}) collective-permute-start(bf16[480,2048]{1,0:T(8,128)(2,1)} %collective-permute-done.2.got_0), channel_id=1, source_target_pairs={{0,16},{2,18},{5,21},{7,23},{8,24},{10,26},{13,29},{15,31},{17,1},... | collective-permute-start | bytes 5898248 | tf_op jit(solution)/shard_map/ppermute | solution.py:507
  93.7 34.6 %collective-permute-start.9 = (bf16[480,2048]{1,0:T(8,128)(2,1)}, bf16[480,2048]{1,0:T(8,128)(2,1)}, u32[]{:S(2)}, u32[]{:S(2)}) collective-permute-start(bf16[480,2048]{1,0:T(8,128)(2,1)} %collective-permute-done.3.got_1), channel_id=1, source_target_pairs={{0,16},{2,18},{5,21},{7,23},{8,24},{10,26},{13,29},{15,31},{17,1},... | collective-permute-start | bytes 5898248 | tf_op jit(solution)/shard_map/ppermute | solution.py:507
  104.9 23.4 %all-to-all-start.2 = ((bf16[16,256,128]{2,1,0:T(8,128)(2,1)}), bf16[16,256,128]{2,1,0:T(8,128)(2,1)S(1)}, u32[]{:S(2)}, u32[]{:S(2)}) async-start(bf16[16,256,128]{2,1,0:T(8,128)(2,1)} %spread.1), calls=%async_computation.2 | async-start | bytes 2097152 | tf_op jit(solution)/shard_map/all_to_all | solution.py:260
  135.7 28.4 %copy-start.4 = (f32[16,2]{0,1:T(2,128)S(1)}, f32[16,2]{0,1:T(2,128)}, u32[]{:S(2)}) copy-start(f32[16,2]{0,1:T(2,128)} %param.20) | copy-start | bytes 388
  155.9 26.0 %copy-start.3 = (bf16[16,2048]{1,0:T(8,128)(2,1)S(1)}, bf16[16,2048]{1,0:T(8,128)(2,1)}, u32[]{:S(2)}) copy-start(bf16[16,2048]{1,0:T(8,128)(2,1)} %residual.1) | copy-start | bytes 196612
  156.9 24.7 %all-to-all-start.4 = ((bf16[16,64,128]{2,1,0:T(8,128)(2,1)}), bf16[16,64,128]{2,1,0:T(8,128)(2,1)S(1)}, u32[]{:S(2)}, u32[]{:S(2)}) async-start(bf16[16,64,128]{2,1,0:T(8,128)(2,1)} %shares.1), calls=%async_computation.4 | async-start | bytes 524288 | tf_op jit(solution)/shard_map/all_to_all | solution.py:260
